TPU v7x, 32 devices: a whole 2x2x4 slice. The times are simulated.
32 devices in a mesh: sp: 8 (over z, x), tp: 4 (over y, core).
Axes of the slice: x: 2, y: 2, z: 4, core: 2. Of those that a mesh axis runs over, the one named last changes fastest.
Arguments:
- queries: bfloat16 [1024, 2048], P('sp', 'tp'), may hold values from -15 to 15
- key_rows: bfloat16 [1024, 2048], P('sp', 'tp'), may hold values from -6 to 6
- value_rows: bfloat16 [1024, 2048], P('sp', 'tp'), may hold values from -6 to 6
- break_bias: bfloat16 [1024, 16], P('sp', 'tp'), may hold values from -14 to 1
- stream: bfloat16 [1024, 4096], P('sp', 'tp'), may hold values from -24 to 24
- out_proj: bfloat16 [2048, 4096], P(None, 'tp'), may hold values from -0.5 to 0.5
- norm_gain: float32 [4096], P('tp'), may hold values from 0.1 to 1.9
- expert_ids: int32 [1024, 2], P('sp'), may hold values from 0 to 15, all different within a row; in each aligned block of 128 rows (0 to 127, 128 to 255, ...) at most 32 rows name the same one
- route_weights: float32 [1024, 2], P('sp'), may hold values from 0.1 to 2.5
- gate_proj: bfloat16 [16, 4096, 384], P('sp', 'tp'), may hold values from -0.09375 to 0.09375
- up_proj: bfloat16 [16, 4096, 384], P('sp', 'tp'), may hold values from -0.09375 to 0.09375
- down_proj: bfloat16 [16, 384, 4096], P('sp', None, 'tp'), may hold values from -0.3125 to 0.3125
- shared_gate: bfloat16 [4096, 384], P('tp'), may hold values from -0.09375 to 0.09375
- shared_up: bfloat16 [4096, 384], P('tp'), may hold values from -0.09375 to 0.09375
- shared_down: bfloat16 [384, 4096], P(None, 'tp'), may hold values from -0.3125 to 0.3125
Outputs:
- result: bfloat16 [1024, 4096], P('sp', 'tp')
Inputs may be any that keep to these rules, and one draw needn't show every extreme that they name: `expert_ids`: each row names 2 different experts; within the rows of one index of sp no expert is named by more than 32 rows, a bound that some block reaches of them.
All inputs are finite; a program needn't handle non-finite values.
Results may differ from a plain program's by a relative error of at most 0.022.
Values may be sent and summed in bfloat16 or wider, within the bound.
No kernel may reach another device: no remote copies, remote signals or barrier semaphores. Data moves between devices by JAX's collectives and lax.ppermute only.
A program may use at most 64 MiB of HBM per device.

v0:
```python
import jax
import jax.numpy as jnp
from jax import lax
from jax.sharding import PartitionSpec as P

D = 4096


EPS = 1e-06
row_block_size = 32


def block_terms(query_heads, key_piece, value_piece, bias_piece, query_pos):
    heads_local = query_heads.shape[1]
    head_dim = query_heads.shape[2]
    key_count = key_piece.shape[0]
    key_heads = key_piece.reshape(key_count, heads_local, head_dim)
    value_heads = value_piece.reshape(key_count, heads_local, head_dim).astype(jnp.float32)
    logits = jnp.einsum("thd,shd->hts", query_heads, key_heads, preferred_element_type=jnp.float32)
    logits = logits * head_dim ** (-0.5) + bias_piece.astype(jnp.float32).T[:, None, :]
    key_pos = jnp.arange(key_count, dtype=jnp.int32)
    before = (key_pos[None, :] < query_pos[:, None])[None]
    log_fail = jnp.where(before, jax.nn.log_sigmoid(-logits), 0.0)
    tail_sum = lax.cumsum(log_fail, axis=2, reverse=True) - log_fail
    weights = jnp.where(before, jnp.exp(jax.nn.log_sigmoid(logits) + tail_sum), 0.0)
    summary = jnp.einsum("hts,shd->thd", weights, value_heads)
    return (summary, jnp.sum(log_fail, axis=2).T)


def body(
    queries,
    key_rows,
    value_rows,
    break_bias,
    stream,
    out_proj,
    norm_gain,
    expert_ids,
    route_weights,
    gate_proj,
    up_proj,
    down_proj,
    shared_gate,
    shared_up,
    shared_down,
):
    tok_dev = queries.shape[0]
    heads_local = break_bias.shape[1]
    head_dim = queries.shape[1] // heads_local
    blocks_all = lax.axis_size("sp")
    own_block = lax.axis_index("sp")
    own_start = own_block * tok_dev
    query_pos = own_start + jnp.arange(tok_dev, dtype=jnp.int32)
    query_heads = queries.reshape(tok_dev, heads_local, head_dim)
    row_step = min(row_block_size, tok_dev)
    row_turns = tok_dev // row_step
    empty_sums = jnp.zeros((blocks_all, tok_dev, heads_local, head_dim), jnp.float32)
    empty_fails = jnp.zeros((blocks_all, tok_dev, heads_local), jnp.float32)
    offset = jnp.int32(0)
    key_piece = lax.all_gather(key_rows, "sp", axis=0, tiled=True)
    value_piece = lax.all_gather(value_rows, "sp", axis=0, tiled=True)
    bias_piece = lax.all_gather(break_bias, "sp", axis=0, tiled=True)
    block_id = offset // tok_dev

    def compute(operand):

        def rows_part(turn):
            row_start = turn * row_step
            part_q = lax.dynamic_slice_in_dim(query_heads, row_start, row_step, 0)
            part_pos = lax.dynamic_slice_in_dim(query_pos, row_start, row_step, 0)
            return block_terms(part_q, key_piece, value_piece, bias_piece, part_pos)

        summary, fail_sum = lax.map(rows_part, jnp.arange(row_turns, dtype=jnp.int32))
        return (
            summary.reshape(tok_dev, heads_local, head_dim),
            fail_sum.reshape(tok_dev, heads_local),
        )

    def skip(operand):
        return (
            jnp.zeros((tok_dev, heads_local, head_dim), jnp.float32),
            jnp.zeros((tok_dev, heads_local), jnp.float32),
        )

    summary, fail_sum = lax.cond(offset < own_start + tok_dev, compute, skip, 0)
    sums_in = empty_sums
    fails_in = empty_fails
    sums_in = lax.dynamic_update_index_in_dim(sums_in, summary, block_id, 0)
    fails_in = lax.dynamic_update_index_in_dim(fails_in, fail_sum, block_id, 0)
    later_fail = jnp.cumsum(fails_in[::-1], axis=0)[::-1] - fails_in
    attended = jnp.sum(jnp.exp(later_fail)[..., None] * sums_in, axis=0)
    attended = attended.reshape(tok_dev, heads_local * head_dim).astype(jnp.bfloat16)
    projected = jnp.dot(
        lax.all_gather(attended, "tp", axis=1, tiled=True),
        out_proj,
        preferred_element_type=jnp.float32,
    )
    mixed = (stream.astype(jnp.float32) + projected).astype(jnp.bfloat16)
    mixed = lax.optimization_barrier(mixed)
    mixed_f = mixed.astype(jnp.float32)
    square_sum = lax.psum(jnp.sum(mixed_f * mixed_f, axis=1), "tp")
    inv_rms = lax.rsqrt(square_sum / D + EPS)
    normed = (mixed_f * inv_rms[:, None] * norm_gain[None, :]).astype(jnp.bfloat16)
    experts_local = gate_proj.shape[0]
    experts_all = experts_local * blocks_all
    top_k = expert_ids.shape[1]
    capacity = 2 * top_k * tok_dev // experts_all
    flat_ids = expert_ids.reshape(-1)
    one_hot = (flat_ids[:, None] == jnp.arange(experts_all, dtype=jnp.int32)[None, :]).astype(
        jnp.int32
    )
    ranks = jnp.sum((jnp.cumsum(one_hot, axis=0) - one_hot) * one_hot, axis=1)
    owner = flat_ids // experts_local
    local_id = flat_ids % experts_local
    slot_index = local_id * (blocks_all * capacity) + owner * capacity + ranks
    token_index = jnp.arange(tok_dev * top_k, dtype=jnp.int32) // top_k
    token_of_slot = (
        jnp.full((experts_all * capacity,), tok_dev, jnp.int32).at[slot_index].set(token_index)
    )
    padded_rows = jnp.concatenate([normed, jnp.zeros((1, normed.shape[1]), jnp.bfloat16)], 0)
    send_rows = padded_rows[token_of_slot].reshape(
        experts_local, blocks_all * capacity, normed.shape[1]
    )
    arrived = lax.all_to_all(send_rows, "sp", split_axis=1, concat_axis=1, tiled=True)
    gate_part = jnp.einsum("erd,edf->erf", arrived, gate_proj, preferred_element_type=jnp.float32)
    up_part = jnp.einsum("erd,edf->erf", arrived, up_proj, preferred_element_type=jnp.float32)
    routed_rows = experts_local * blocks_all * capacity
    gate_part = gate_part.reshape(routed_rows, -1)
    up_part = up_part.reshape(routed_rows, -1)
    shared_gate_part = jnp.dot(normed, shared_gate, preferred_element_type=jnp.float32)
    shared_up_part = jnp.dot(normed, shared_up, preferred_element_type=jnp.float32)
    gate_sum, up_sum, sgate_sum, sup_sum = (
        lax.psum(gate_part.astype(jnp.bfloat16), "tp").astype(jnp.float32),
        lax.psum(up_part.astype(jnp.bfloat16), "tp").astype(jnp.float32),
        lax.psum(shared_gate_part.astype(jnp.bfloat16), "tp").astype(jnp.float32),
        lax.psum(shared_up_part.astype(jnp.bfloat16), "tp").astype(jnp.float32),
    )
    hidden = (jax.nn.silu(gate_sum) * up_sum).astype(jnp.bfloat16)
    shared_hidden = (jax.nn.silu(sgate_sum) * sup_sum).astype(jnp.bfloat16)
    hidden = hidden.reshape(experts_local, blocks_all * capacity, -1)
    expert_out = jnp.einsum(
        "erf,efd->erd", hidden, down_proj, preferred_element_type=jnp.float32
    ).astype(jnp.bfloat16)
    returned = lax.all_to_all(expert_out, "sp", split_axis=1, concat_axis=1, tiled=True)
    flat_back = returned.reshape(experts_all * capacity, -1)
    picked = flat_back[slot_index.reshape(tok_dev, top_k)]
    routed = jnp.einsum("tk,tkd->td", route_weights, picked.astype(jnp.float32))
    shared_out = jnp.dot(shared_hidden, shared_down, preferred_element_type=jnp.float32)
    return (mixed_f + shared_out + routed).astype(jnp.bfloat16)


def solution(mesh):
    in_specs = (
        P("sp", "tp"),
        P("sp", "tp"),
        P("sp", "tp"),
        P("sp", "tp"),
        P("sp", "tp"),
        P(None, "tp"),
        P("tp"),
        P("sp", None),
        P("sp", None),
        P("sp", "tp", None),
        P("sp", "tp", None),
        P("sp", None, "tp"),
        P("tp", None),
        P("tp", None),
        P(None, "tp"),
    )
    out_specs = P("sp", "tp")
    return jax.shard_map(body, mesh=mesh, in_specs=in_specs, out_specs=out_specs, check_vma=False)
```

profile of v0, /device:TPU:0, one launch (start us, length us, event | category | flops | bytes accessed | tf_op | source)
XLA Modules:
  0.0 900.8 jit_solution(6103857424751520015)
XLA Ops:
  6.5 0.7 all-gather.3.cloned.1.call-update
  7.3 0.7 all-gather.5.cloned.1.call-update
  8.0 0.8 copy.48
  10.2 1.4 scatter_custom_fusion
  11.6 22.5 %all_gather.13 = bf16[1024,4]{0,1:T(4,128)(2,1)S(1)} all-gather(bf16[128,4]{0,1:T(4,128)(2,1)} %param.22), channel_id=1, replica_groups=mesh['sp'=8,'tp'=4] {'sp'}, dimensions={0}, use_global_device_ids=true | all-gather | bytes 9216 | tf_op jit(solution)/shard_map/all_gather | solution.py:62
  34.1 18.3 %all-gather.3.cloned.1.call-done = bf16[1024,512]{1,0:T(8,128)(2,1)} async-done(((bf16[128,512]{1,0:T(8,128)(2,1)}), bf16[1024,512]{1,0:T(8,128)(2,1)}) %all-gather.3.cloned.1.call-update) | async-done | bytes 1048592 | tf_op jit(solution)/shard_map/all_gather | solution.py:60
  52.5 41.1 %all-gather.5.cloned.1.call-done = bf16[1024,512]{1,0:T(8,128)(2,1)} async-done(((bf16[128,512]{1,0:T(8,128)(2,1)}), bf16[1024,512]{1,0:T(8,128)(2,1)}) %all-gather.5.cloned.1.call-update) | async-done | bytes 1048592 | tf_op jit(solution)/shard_map/all_gather | solution.py:61
  93.6 668.0 %conditional.1 = (f32[8,128,4,128]{3,2,1,0:T(4,128)}, f32[8,128,4]{2,1,0:T(8,128)}) conditional(s32[]{:T(128)} %convert_element_type.80, () %tuple.25, (bf16[128,512]{1,0:T(8,128)(2,1)}, s32[]{:T(128)}, s32[128]{0:T(128)S(1)}, bf16[1024,512]{1,0:T(8,128)(2,1)}, bf16[1024,4]{0,1:T(4,128)(2,1)S(1)}, /*index=5*/bf16[1024,512]{1,0:T(8,128)(2,1)}) %tuple.26), branch_computations={%region_0.1_spmd, %region_1.7_spmd} | conditional | flops 89272192 | bytes 12330231 | solution.py:85
  93.6 1.0 copy.47
  94.7 0.8 copy.44
  95.4 662.7 %while.11 = (s32[]{:T(128)}, f32[4,32,4,128]{3,2,1,0:T(4,128)}, f32[4,32,4]{1,2,0:T(4,128)S(1)}, s32[4]{0:T(128)S(1)}, s32[128]{0:T(128)S(1)}, /*index=5*/bf16[1...) while((s32[]{:T(128)}, f32[4,32,4,128]{3,2,1,0:T(4,128)}, ...), condition=%wide.region_6.6_spmd, body=%wide.region_2.5_spmd.sunk | while | flops 89272064 | bytes 9422931 | solution.py:73
  96.7 1.7 fusion.91
  99.1 158.4 %reduce-window.24 = f32[4,32,8,128]{3,2,1,0:T(8,128)S(1)} reduce-window(f32[4,32,8,128]{3,2,1,0:T(8,128)S(1)} %bitcast.111, f32[]{:T(128)} %constant.126.clone..sunk), window={size=1x1x1x128 pad=0_0x0_0x0_0x0_127}, to_apply=%region_3.2 | reduce-window | flops 16646144 | bytes 1048580 | tf_op jit(solution)/shard_map/reduce-window
  258.3 2.1 convolution_bitcast_fusion.2
  262.3 1.7 fusion.91
  264.8 158.4 %reduce-window.24 = f32[4,32,8,128]{3,2,1,0:T(8,128)S(1)} reduce-window(f32[4,32,8,128]{3,2,1,0:T(8,128)S(1)} %bitcast.111, f32[]{:T(128)} %constant.126.clone..sunk), window={size=1x1x1x128 pad=0_0x0_0x0_0x0_127}, to_apply=%region_3.2 | reduce-window | flops 16646144 | bytes 1048580 | tf_op jit(solution)/shard_map/reduce-window
  423.9 2.1 convolution_bitcast_fusion.2
  428.0 1.7 fusion.91
  430.5 158.4 %reduce-window.24 = f32[4,32,8,128]{3,2,1,0:T(8,128)S(1)} reduce-window(f32[4,32,8,128]{3,2,1,0:T(8,128)S(1)} %bitcast.111, f32[]{:T(128)} %constant.126.clone..sunk), window={size=1x1x1x128 pad=0_0x0_0x0_0x0_127}, to_apply=%region_3.2 | reduce-window | flops 16646144 | bytes 1048580 | tf_op jit(solution)/shard_map/reduce-window
  589.6 2.1 convolution_bitcast_fusion.2
  593.6 1.7 fusion.91
  596.1 158.4 %reduce-window.24 = f32[4,32,8,128]{3,2,1,0:T(8,128)S(1)} reduce-window(f32[4,32,8,128]{3,2,1,0:T(8,128)S(1)} %bitcast.111, f32[]{:T(128)} %constant.126.clone..sunk), window={size=1x1x1x128 pad=0_0x0_0x0_0x0_127}, to_apply=%region_3.2 | reduce-window | flops 16646144 | bytes 1048580 | tf_op jit(solution)/shard_map/reduce-window
  755.3 2.1 convolution_bitcast_fusion.2
  758.1 2.6 dynamic_update_slice.18
  760.8 0.8 dynamic_update_slice.19
  761.6 1.1 rev.6
  763.2 1.3 subtract_exponential_fusion
  764.4 2.8 multiply_reduce_fusion
  767.2 7.2 all_gather.15
  774.4 0.7 fusion.27
  775.3 6.4 psum.35
  781.9 2.1 gather_fusion
  783.9 2.1 copy.52
  786.0 3.6 all-to-all-start
  789.8 2.1 convolution_convert_fusion.3
  791.9 2.1 convolution_convert_fusion.4
  793.9 21.1 %all-to-all-done = bf16[2,256,1024]{2,0,1:T(2,128)(2,1)S(1)} async-done(((bf16[2,256,1024]{2,0,1:T(2,128)(2,1)}), bf16[2,256,1024]{2,0,1:T(2,128)(2,1)S(1)}, u32[]{:S(2)}, u32[]{:S(2)}) %all-to-all-start) | async-done | bytes 1048608 | tf_op jit(solution)/shard_map/all_to_all | solution.py:124
  815.0 3.0 convolution_convert_fusion.2
  818.0 1.5 convolution_convert_fusion.1
  819.5 34.3 %all-reduce.6.cloned.1.call-done = (bf16[512,384]{1,0:T(8,128)(2,1)}, bf16[512,384]{1,0:T(8,128)(2,1)}, bf16[128,384]{1,0:T(8,128)(2,1)}, bf16[128,384]{1,0:T(8,128)(2,1)}) async-done(((bf16[512,384]{1,0:T(8,128)(2,1)}, bf16[512,384]{1,0:T(8,128)(2,1)}, bf16[128,384]{1,0:T(8,128)(2,1)}, bf16[128,384]{1,0:T(8,128)(2,1)}), (bf16[512,384]{1,0:T(8,128)(2,1)}, bf16[512,384]{1,0:T(8,128)(2,1)}, ...) | async-done | bytes 983056 | tf_op jit(solution)/shard_map/psum | solution.py:134
  853.8 1.4 fusion.34
  855.2 0.7 convolution_convert_fusion
  855.9 2.1 copy.55
  858.0 5.6 all-to-all-start.1
  864.4 24.8 %all-to-all-done.1 = bf16[2,256,1024]{2,0,1:T(2,128)(2,1)} async-done(((bf16[2,256,1024]{2,0,1:T(2,128)(2,1)}), bf16[2,256,1024]{2,0,1:T(2,128)(2,1)}, u32[]{:S(2)}, u32[]{:S(2)}) %all-to-all-start.1) | async-done | bytes 1048608 | tf_op jit(solution)/shard_map/all_to_all | solution.py:144
  889.2 1.5 copy.56
  890.7 1.2 gather_fusion.1
  893.2 1.1 fusion.26
  (114 shorter events, 15.3 us)
Async XLA Ops:
  6.5 848.6 %copy-start = (bf16[2,384,1024]{2,1,0:T(8,128)(2,1)S(1)}, bf16[2,384,1024]{2,1,0:T(8,128)(2,1)}, u32[]{:S(2)}) copy-start(bf16[2,384,1024]{2,1,0:T(8,128)(2,1)} %param.30) | copy-start | bytes 4718596
  6.5 45.9 %all-gather.3.cloned.1.call-start = ((), (), s32[]{:S(2)}) async-start(), calls=%async_computation.2 | async-start | bytes 1179648 | tf_op jit(solution)/shard_map/all_gather | solution.py:60
  7.3 86.4 %all-gather.5.cloned.1.call-start = ((), (), s32[]{:S(2)}) async-start(), calls=%async_computation.3 | async-start | bytes 1179648 | tf_op jit(solution)/shard_map/all_gather | solution.py:61
  763.1 11.3 %copy-start.1 = (bf16[2048,1024]{1,0:T(8,128)(2,1)S(1)}, bf16[2048,1024]{1,0:T(8,128)(2,1)}, u32[]{:S(2)}) copy-start(bf16[2048,1024]{1,0:T(8,128)(2,1)} %param.24) | copy-start | bytes 12582916
  764.4 10.0 %copy-start.2 = (bf16[128,1024]{1,0:T(8,128)(2,1)S(1)}, bf16[128,1024]{1,0:T(8,128)(2,1)}, u32[]{:S(2)}) copy-start(bf16[128,1024]{1,0:T(8,128)(2,1)} %param.23) | copy-start | bytes 786436
  774.4 7.3 copy-start.3
  786.0 29.0 %all-to-all-start = ((bf16[2,256,1024]{2,0,1:T(2,128)(2,1)}), bf16[2,256,1024]{2,0,1:T(2,128)(2,1)S(1)}, u32[]{:S(2)}, u32[]{:S(2)}) async-start(bf16[2,256,1024]{2,0,1:T(2,128)(2,1)} %copy.52), calls=%async_computation | async-start | bytes 2097152 | tf_op jit(solution)/shard_map/all_to_all | solution.py:124
  789.6 64.2 %all-reduce.6.cloned.1.call-start = ((), (), s32[]{:S(2)}) async-start(), calls=%async_computation.4 | async-start | bytes 1966080 | tf_op jit(solution)/shard_map/psum | solution.py:134
  815.0 3.0 copy-start.6
  858.0 5.8 copy-start.4
  858.0 6.2 copy-start.5
  858.0 31.2 %all-to-all-start.1 = ((bf16[2,256,1024]{2,0,1:T(2,128)(2,1)}), bf16[2,256,1024]{2,0,1:T(2,128)(2,1)}, u32[]{:S(2)}, u32[]{:S(2)}) async-start(bf16[2,256,1024]{2,0,1:T(2,128)(2,1)} %copy.55), calls=%async_computation.1 | async-start | bytes 2097152 | tf_op jit(solution)/shard_map/all_to_all | solution.py:144
  892.0 1.1 copy-start.7
  892.1 1.1 copy-start.8
  892.1 1.1 copy-start.9
Sparse Core Ops, SparseCore 0:
  9.5 42.9 all-gather.2
  54.6 38.9 all-gather.4
  819.6 34.1 all-reduce.5
where the time goes:
time: 902 us; the launch traced here: 901 us
  other arithmetic  644 us (71%)
  waiting for transfers between devices  141 us (16%)
  blocking collectives  36.1 us (4%)
  matrix products  27.2 us (3%)
  local copies, waits for them, and re-layouts  26.9 us (3%)
  between operations  13.4 us (1%)
  starting transfers between devices  9.46 us (1%)
    another operation x12, other arithmetic  634 us
    all_gather x1, waiting for transfers between devices, body(): value_piece = lax.all_gather(value_rows, 'sp', axis=0, tiled=True)  41.1 us
    psum x1, waiting for transfers between devices, body(): lax.psum(up_part.astype(jnp.bfloat16), 'tp').astype(jnp.float32)  34.3 us
    all_to_all x1, waiting for transfers between devices, body(): lax.all_to_all(expert_out, 'sp', split_axis=1, concat_axis=1, tiled=True)  24.8 us
    all_gather x1, blocking collectives, body(): bias_piece = lax.all_gather(break_bias, 'sp', axis=0, tiled=True)  22.5 us
    all_to_all x1, waiting for transfers between devices, body(): lax.all_to_all(send_rows, 'sp', split_axis=1, concat_axis=1, tiled=True)  21.1 us
    all_gather x1, waiting for transfers between devices, body(): key_piece = lax.all_gather(key_rows, 'sp', axis=0, tiled=True)  18.3 us
  transfers between devices with their start and end apart: 5, of which 5 were waited for; matrix products, arithmetic and copies ran while one was open for 1% of the time, Pallas kernels for 0%

commit v1 on v0

v1 whole, which is shorter than its diff:
```python
import functools

import jax
import jax.numpy as jnp
from jax import lax
from jax.experimental import pallas as pl
from jax.experimental.pallas import tpu as pltpu
from jax.sharding import PartitionSpec as P

EPS = 1e-06
LANES = 128
BIAS_ROWS = 16
BF = jnp.bfloat16
F32 = jnp.float32


def vmem():
    return pl.BlockSpec(memory_space=pltpu.VMEM)


def smem():
    return pl.BlockSpec(memory_space=pltpu.SMEM)


def call(kernel, out_shape, in_specs, name, scratch=()):
    many = isinstance(out_shape, (tuple, list))
    return pl.pallas_call(
        kernel,
        out_shape=out_shape,
        in_specs=in_specs,
        out_specs=tuple(vmem() for _ in out_shape) if many else vmem(),
        scratch_shapes=list(scratch),
        name=name,
    )


def iota(shape, dim):
    return lax.broadcasted_iota(jnp.int32, shape, dim)


def dot(a, b):
    return jnp.dot(a, b, preferred_element_type=F32)


def split_pair(x):
    high = x.astype(BF)
    return high, (x - high.astype(F32)).astype(BF)


def pack_kernel(q_ref, k_ref, v_ref, b_ref, out_ref, *, heads, group, rows, hd):
    tok = k_ref.shape[0]
    bias_t = jnp.transpose(b_ref[...].astype(F32))
    for h in range(heads):
        cols = slice(h * hd, (h + 1) * hd)
        bias = jnp.broadcast_to(bias_t[h : h + 1, :], (BIAS_ROWS, tok)).astype(BF)
        for p in range(group):
            s = h * group + p
            out_ref[s, 0:tok] = k_ref[:, cols]
            out_ref[s, tok : 2 * tok] = v_ref[:, cols]
            out_ref[s, 2 * tok : 2 * tok + BIAS_ROWS] = bias
            out_ref[s, 2 * tok + BIAS_ROWS :] = q_ref[p * rows : (p + 1) * rows, cols]


def pack_plain(q, k, v, b, heads, group, rows, padded_rows, hd):
    tok = k.shape[0]
    kh = k.reshape(tok, heads, hd).transpose(1, 0, 2)
    vh = v.reshape(tok, heads, hd).transpose(1, 0, 2)
    bh = jnp.broadcast_to(b.T[:, None, :], (heads, BIAS_ROWS, tok))
    both = jnp.concatenate([kh, vh, bh], axis=1)
    both = jnp.broadcast_to(both[:, None], (heads, group) + both.shape[1:])
    qh = q.reshape(group, rows, heads, hd).transpose(2, 0, 1, 3)
    qh = jnp.pad(qh, ((0, 0), (0, 0), (0, padded_rows - rows), (0, 0)))
    return jnp.concatenate([both, qh], axis=2).reshape(heads * group, -1, hd)


def attention_kernel(p_ref, x_ref, out_ref, acc_ref, carry_ref, *, rows, padded, hd, tok):
    blocks = x_ref.shape[0]
    q0 = 2 * tok + BIAS_ROWS
    queries = jnp.concatenate([x_ref[i, q0 : q0 + padded] for i in range(blocks)], axis=0)
    acc_ref[...] = jnp.zeros_like(acc_ref)
    carry_ref[...] = jnp.zeros_like(carry_ref)
    src = iota((2 * tok, 2 * tok), 0)
    src = jnp.where(src >= tok, src - tok, src)
    dst = iota((2 * tok, 2 * tok), 1)
    tri = jnp.where((dst >= tok) | (src > dst), 1.0, 0.0).astype(BF)
    first = p_ref[0] * rows
    scale = hd ** (-0.5)
    for j in reversed(range(blocks)):
        r0 = j * padded
        n = blocks * padded - r0
        keys = x_ref[j, 0:tok]
        values = x_ref[j, tok : 2 * tok]
        bias = x_ref[j, 2 * tok : 2 * tok + BIAS_ROWS].astype(F32)[0:1, :]
        raw = lax.dot_general(
            queries[r0:, :], keys, (((1,), (1,)), ((), ())), preferred_element_type=F32
        )
        logits = raw * scale + bias
        soft = jnp.log(1.0 + jnp.exp(-jnp.abs(logits)))
        fail = -(jnp.maximum(logits, 0.0) + soft)
        row = iota((n, tok), 0)
        before = (row >= padded) | (iota((n, tok), 1) < row + first)
        stay = logits + fail
        fail = jnp.where(before, fail, 0.0)
        high, low = split_pair(fail)
        sums = dot(jnp.concatenate([high, low], axis=1), tri)
        carry = carry_ref[r0:, :]
        weights = jnp.where(before, jnp.exp(stay + sums[:, :tok] + carry), 0.0)
        carry_ref[r0:, :] = carry + sums[:, tok:]
        acc_ref[r0:, :] += dot(weights.astype(BF), values)
    out_ref[...] = acc_ref[...].astype(BF).reshape(out_ref.shape)


def project_kernel(t_ref, ids_ref, *refs, masks, heads, group, rows, cap, arranged):
    count = len(masks)
    pieces = refs[:count]
    w_ref, stream_ref, mixed_ref, send_ref = refs[count:]
    t = t_ref[0]
    total = stream_ref[...].astype(F32)
    for mask, piece in zip(masks, pieces):
        if arranged:
            part = piece[...]
        else:
            part = jnp.concatenate(
                [
                    jnp.concatenate([piece[h * group + p] for p in range(group)], axis=0)
                    for h in range(heads)
                ],
                axis=1,
            )
        total = total + dot(part, w_ref[jnp.bitwise_xor(t, mask)])
    mixed = total.astype(BF)
    mixed_ref[...] = mixed
    tok = mixed.shape[0]
    experts = send_ref.shape[0] // cap
    named = [iota((experts, tok), 0) == ids_ref[k : k + 1, :] for k in range(ids_ref.shape[0])]
    hit = functools.reduce(jnp.logical_or, named)
    order = jnp.where(iota((tok, tok), 0) < iota((tok, tok), 1), 1.0, 0.0).astype(BF)
    rank = dot(jnp.where(hit, 1.0, 0.0).astype(BF), order)
    rank = jnp.where(hit, rank, -1.0)
    slot = iota((cap, tok), 0).astype(F32)
    pick = jnp.concatenate(
        [jnp.where(slot == rank[e : e + 1, :], 1.0, 0.0) for e in range(experts)], axis=0
    )
    send_ref[...] = dot(pick.astype(BF), mixed).astype(BF)


def partials(x, gain, gate, up):
    scaled = (x * gain).astype(BF)
    square = jnp.sum(x * x, axis=1, keepdims=True)
    high, low = split_pair(square)
    lane = iota((x.shape[0], LANES), 1)
    tail = jnp.where(lane == 0, high.astype(F32), jnp.where(lane == 1, low.astype(F32), 0.0))
    return jnp.concatenate(
        [dot(scaled, gate).astype(BF), dot(scaled, up).astype(BF), tail.astype(BF)], axis=1
    )


def shared_kernel(mixed_ref, gain_ref, gate_ref, up_ref, out_ref):
    out_ref[...] = partials(
        mixed_ref[...].astype(F32), gain_ref[...], gate_ref[...], up_ref[...]
    )


def routed_kernel(e_ref, x_ref, gain_ref, gate_ref, up_ref, out_ref):
    x = x_ref[...].astype(F32)
    x = x.reshape(-1, x.shape[-1])
    out_ref[...] = partials(x, gain_ref[...], gate_ref[0], up_ref[0])


def add_partials(a_ref, b_ref, width):
    a = a_ref[...].astype(F32)
    b = b_ref[...].astype(F32)
    body = a[:, :width] + b[:, :width]
    square = a[:, width : width + 1] + b[:, width : width + 1]
    square = square + (a[:, width + 1 : width + 2] + b[:, width + 1 : width + 2])
    return body, square


def add_kernel(a_ref, b_ref, out_ref, *, width):
    body, square = add_partials(a_ref, b_ref, width)
    high, low = split_pair(square)
    lane = iota((body.shape[0], LANES), 1)
    tail = jnp.where(lane == 0, high.astype(F32), jnp.where(lane == 1, low.astype(F32), 0.0))
    out_ref[...] = jnp.concatenate([body.astype(BF), tail.astype(BF)], axis=1)


def hidden_kernel(a_ref, b_ref, out_ref, *, width, features):
    body, square = add_partials(a_ref, b_ref, width)
    inv = lax.rsqrt(square / features + EPS)
    gate = body[:, : width // 2] * inv
    up = body[:, width // 2 :] * inv
    out_ref[...] = (gate * jax.nn.sigmoid(gate) * up).astype(BF)


def down_kernel(c_ref, own_ref, other_ref, w_ref, out_ref):
    c = c_ref[0]
    blocks, _, cap, feats = out_ref.shape
    out_ref[:, pl.ds(c, 1)] = dot(own_ref[...], w_ref[c]).reshape(blocks, 1, cap, feats).astype(BF)
    d = 1 - c
    out_ref[:, pl.ds(d, 1)] = (
        dot(other_ref[...], w_ref[d]).reshape(blocks, 1, cap, feats).astype(BF)
    )


def combine_kernel(ids_ref, rw_ref, back_ref, mixed_ref, hid_ref, down_ref, out_ref, *, cap):
    tok, choices = ids_ref.shape
    slots = back_ref.shape[0]
    experts = slots // cap
    ids = ids_ref[...]
    named = [iota((tok, experts), 1) == ids[:, k : k + 1] for k in range(choices)]
    hit = functools.reduce(jnp.logical_or, named)
    order = jnp.where(iota((tok, tok), 1) < iota((tok, tok), 0), 1.0, 0.0).astype(BF)
    rank = dot(order, jnp.where(hit, 1.0, 0.0).astype(BF))
    place = rank + (iota((tok, experts), 1) * cap).astype(F32)
    lane = iota((tok, slots), 1).astype(F32)
    pick = jnp.zeros((tok, slots), F32)
    for k in range(choices):
        at = jnp.sum(jnp.where(named[k], place, 0.0), axis=1, keepdims=True)
        pick = pick + jnp.where(lane == at, rw_ref[:, k : k + 1], 0.0)
    high, low = split_pair(pick)
    back = back_ref[...]
    total = mixed_ref[...].astype(F32) + dot(hid_ref[...], down_ref[...])
    total = total + (dot(high, back) + dot(low, back))
    out_ref[...] = total.astype(BF)


def swap(x, axis, bit):
    count = lax.axis_size(axis)
    return lax.ppermute(x, axis, [(i, i ^ bit) for i in range(count)])


def body(
    queries,
    key_rows,
    value_rows,
    break_bias,
    stream,
    out_proj,
    norm_gain,
    expert_ids,
    route_weights,
    gate_proj,
    up_proj,
    down_proj,
    shared_gate,
    shared_up,
    shared_down,
):
    tok = queries.shape[0]
    heads = break_bias.shape[1]
    hd = queries.shape[1] // heads
    blocks = lax.axis_size("sp")
    tp = lax.axis_size("tp")
    feats = stream.shape[1]
    features = feats * tp
    s_index = lax.axis_index("sp")
    t_index = lax.axis_index("tp")
    group = blocks // heads
    rows = tok // group
    padded = max(rows, 16)
    aligned = rows % 16 == 0

    if aligned:
        packed = call(
            functools.partial(pack_kernel, heads=heads, group=group, rows=rows, hd=hd),
            jax.ShapeDtypeStruct((blocks, 2 * tok + BIAS_ROWS + padded, hd), BF),
            [vmem()] * 4,
            "pack",
        )(queries, key_rows, value_rows, break_bias)
    else:
        packed = pack_plain(
            queries, key_rows, value_rows, break_bias, heads, group, rows, padded, hd
        )
    moved = lax.all_to_all(packed, "sp", 0, 0, tiled=True)
    part_index = (s_index % group).astype(jnp.int32).reshape(1)
    attended = call(
        functools.partial(attention_kernel, rows=rows, padded=padded, hd=hd, tok=tok),
        jax.ShapeDtypeStruct((blocks, padded, hd), BF),
        [smem(), vmem()],
        "attention",
        [pltpu.VMEM((blocks * padded, hd), F32), pltpu.VMEM((blocks * padded, tok), F32)],
    )(part_index, moved)
    piece = lax.all_to_all(attended, "sp", 0, 0, tiled=True)
    if not aligned:
        piece = piece.reshape(heads, group, padded, hd)[:, :, :rows]
        piece = piece.transpose(1, 2, 0, 3).reshape(tok, heads * hd)
    bits = [1 << i for i in range(tp.bit_length() - 1)]
    pieces, masks = [piece], [0]
    for bit in reversed(bits):
        pieces = pieces + [swap(x, "tp", bit) for x in pieces]
        masks = masks + [m ^ bit for m in masks]

    experts_local = gate_proj.shape[0]
    experts = experts_local * blocks
    choices = expert_ids.shape[1]
    cap = 2 * choices * tok // experts
    t_array = t_index.astype(jnp.int32).reshape(1)
    mixed, send = call(
        functools.partial(
            project_kernel,
            masks=tuple(masks),
            heads=heads,
            group=group,
            rows=rows,
            cap=cap,
            arranged=not aligned,
        ),
        (
            jax.ShapeDtypeStruct((tok, feats), BF),
            jax.ShapeDtypeStruct((experts * cap, feats), BF),
        ),
        [smem()] + [vmem()] * (len(pieces) + 3),
        "project",
    )(t_array, expert_ids.T, *pieces, out_proj.reshape(tp, -1, feats), stream)
    arrived = lax.all_to_all(
        send.reshape(blocks, experts_local, cap, feats), "sp", 0, 0, tiled=True
    )

    gain = norm_gain.reshape(1, feats)
    hid_s = shared_gate.shape[1]
    shared_sum = call(
        shared_kernel,
        jax.ShapeDtypeStruct((tok, 2 * hid_s + LANES), BF),
        [vmem()] * 4,
        "shared",
    )(mixed, gain, shared_gate, shared_up)

    def add(a, b, width):
        return call(
            functools.partial(add_kernel, width=width),
            jax.ShapeDtypeStruct(a.shape, BF),
            [vmem()] * 2,
            "add",
        )(a, b)

    def hidden(a, b, width):
        return call(
            functools.partial(hidden_kernel, width=width, features=features),
            jax.ShapeDtypeStruct((a.shape[0], width // 2), BF),
            [vmem()] * 2,
            "hidden",
        )(a, b)

    for bit in bits[:-1]:
        shared_sum = add(shared_sum, swap(shared_sum, "tp", bit), 2 * hid_s)
    shared_hidden = hidden(shared_sum, swap(shared_sum, "tp", bits[-1]), 2 * hid_s)

    hid_r = gate_proj.shape[2]
    expert_rows = blocks * cap

    def routed(e):
        spec = pltpu.PrefetchScalarGridSpec(
            num_scalar_prefetch=1,
            grid=(1,),
            in_specs=[
                pl.BlockSpec((blocks, 1, cap, feats), lambda i, e: (0, e[0], 0, 0)),
                pl.BlockSpec((1, feats), lambda i, e: (0, 0)),
                pl.BlockSpec((1, feats, hid_r), lambda i, e: (e[0], 0, 0)),
                pl.BlockSpec((1, feats, hid_r), lambda i, e: (e[0], 0, 0)),
            ],
            out_specs=pl.BlockSpec((expert_rows, 2 * hid_r + LANES), lambda i, e: (0, 0)),
        )
        return pl.pallas_call(
            routed_kernel,
            out_shape=jax.ShapeDtypeStruct((expert_rows, 2 * hid_r + LANES), BF),
            grid_spec=spec,
            name="routed",
        )(e, arrived, gain, gate_proj, up_proj)

    core = t_array % 2
    away = routed(1 - core)
    came = swap(away, "tp", 1)
    total = add(routed(core), came, 2 * hid_r)
    for bit in bits[1:-1]:
        total = add(total, swap(total, "tp", bit), 2 * hid_r)
    hid_own = hidden(total, swap(total, "tp", bits[-1]), 2 * hid_r)
    hid_other = swap(hid_own, "tp", 1)
    outs = call(
        down_kernel,
        jax.ShapeDtypeStruct((blocks, experts_local, cap, feats), BF),
        [smem()] + [vmem()] * 3,
        "down",
    )(core, hid_own, hid_other, down_proj)
    back = lax.all_to_all(outs, "sp", 0, 0, tiled=True).reshape(experts * cap, feats)
    return call(
        functools.partial(combine_kernel, cap=cap),
        jax.ShapeDtypeStruct((tok, feats), BF),
        [vmem()] * 6,
        "combine",
    )(expert_ids, route_weights, back, mixed, shared_hidden, shared_down)


def solution(mesh):
    in_specs = (
        P("sp", "tp"),
        P("sp", "tp"),
        P("sp", "tp"),
        P("sp", "tp"),
        P("sp", "tp"),
        P(None, "tp"),
        P("tp"),
        P("sp", None),
        P("sp", None),
        P("sp", "tp", None),
        P("sp", "tp", None),
        P("sp", None, "tp"),
        P("tp", None),
        P("tp", None),
        P(None, "tp"),
    )
    out_specs = P("sp", "tp")
    return jax.shard_map(body, mesh=mesh, in_specs=in_specs, out_specs=out_specs, check_vma=False)
```

time: 902 us -> 153 us (0.17)
  other arithmetic: 644 us -> 0 us
  waiting for transfers between devices: 141 us -> 77.6 us
  Pallas kernels: 0 us -> 34.3 us
  matrix products: 27.2 us -> 0 us
  blocking collectives: 36.1 us -> 11 us
  local copies, waits for them, and re-layouts: 26.9 us -> 10 us
  between operations: 13.4 us -> 0.08 us
  starting transfers between devices: 9.46 us -> 19.1 us
    another operation x17 -> x0, other arithmetic: 636 us -> none
    all_gather x2 -> x0, waiting for transfers between devices: 59.5 us -> none  [the longest x1 41.1 us: body(): value_piece = lax.all_gather(value_rows, 'sp', axis=0, tiled=True)]
    psum x1 -> x0, waiting for transfers between devices: 34.3 us -> none  [body(): lax.psum(up_part.astype(jnp.bfloat16), 'tp').astype(jnp.float32)]
    pallas_call x0 -> x12, Pallas kernels: none -> 34.3 us  [the longest x2 6.08 us: routed(): pl.pallas_call(routed_kernel, out_shape=jax.ShapeDtypeStruct((expert_rows...]
    all_gather x2 -> x0, blocking collectives: 29.7 us -> none  [the longest x1 22.5 us: body(): bias_piece = lax.all_gather(break_bias, 'sp', axis=0, tiled=True)]
    dot_general x16 -> x0, matrix products: 27.2 us -> none  [the longest x4 8.52 us: block_terms(): summary = jnp.einsum('hts,shd->thd', weights, value_heads)]
    ppermute x0 -> x8, waiting for transfers between devices: none -> 24.5 us  [swap(): return lax.ppermute(x, axis, [(i, i ^ bit) for i in range(count)])]
    all_to_all x0 -> x1, blocking collectives: none -> 11 us  [body(): piece = lax.all_to_all(attended, 'sp', 0, 0, tiled=True)]
  transfers between devices with their start and end apart: 5 -> 11, of which waited for: 5 -> 9; matrix products, arithmetic and copies ran while one was open for 1% -> 1% of each run, Pallas kernels for 0% -> 6%
where the time goes in v1:
time: 153 us; the launch traced here: 152 us
  waiting for transfers between devices  77.6 us (51%)
  Pallas kernels  34.3 us (22%)
  starting transfers between devices  19.1 us (12%)
  blocking collectives  11 us (7%)
  local copies, waits for them, and re-layouts  10 us (7%)
    all_to_all x1, waiting for transfers between devices, body(): lax.all_to_all(send.reshape(blocks, experts_local, cap, feats), 'sp', 0,...  26.3 us
    ppermute x8, waiting for transfers between devices, swap(): return lax.ppermute(x, axis, [(i, i ^ bit) for i in range(count)])  24.5 us
    all_to_all x1, waiting for transfers between devices, body(): moved = lax.all_to_all(packed, 'sp', 0, 0, tiled=True)  18 us
    all_to_all x1, blocking collectives, body(): piece = lax.all_to_all(attended, 'sp', 0, 0, tiled=True)  11 us
    unnamed x31, local copies, waits for them, and re-layouts  10 us
    all_to_all x1, waiting for transfers between devices, body(): lax.all_to_all(outs, 'sp', 0, 0, tiled=True).reshape(experts * cap, feats)  8.86 us
    all_to_all x1, starting transfers between devices, body(): moved = lax.all_to_all(packed, 'sp', 0, 0, tiled=True)  7.28 us
    pallas_call x2, Pallas kernels, routed(): pl.pallas_call(routed_kernel, out_shape=jax.ShapeDtypeStruct((expert_rows...  6.08 us
  transfers between devices with their start and end apart: 11, of which 9 were waited for; matrix products, arithmetic and copies ran while one was open for 1% of the time, Pallas kernels for 6%

profile of v1, /device:TPU:0, one launch (start us, length us, event | category | flops | bytes accessed | tf_op | source)
XLA Modules:
  0.0 152.1 jit_solution(7647013956024721129)
XLA Ops:
  0.0 1.4 copy.16.b_ref
  1.4 2.0 %pack.1 = bf16[8,336,128]{2,1,0:T(8,128)(2,1)} custom-call(bf16[128,512]{1,0:T(8,128)(2,1)} %q_ref.1, bf16[128,512]{1,0:T(8,128)(2,1)} %k_ref.1, bf16[128,512]{1,0:T(8,128)(2,1)} %v_ref.1, bf16[128,4]{1,0:T(8,128)(2,1)} %copy.16.b_ref), custom_call_target="tpu_custom_call" | custom-call | tf_op jit(solution)/shard_map/pack/pallas_call | solution.py:264
  3.4 7.3 %all-to-all-start = ((bf16[8,336,128]{2,1,0:T(8,128)(2,1)}), bf16[8,336,128]{2,1,0:T(8,128)(2,1)S(1)}, u32[]{:S(2)}, u32[]{:S(2)}) async-start(bf16[8,336,128]{2,1,0:T(8,128)(2,1)} %pack.1), calls=%async_computation | async-start | bytes 1376256 | tf_op jit(solution)/shard_map/all_to_all | solution.py:274
  10.7 18.0 %all-to-all-done.x_ref = bf16[8,336,128]{2,1,0:T(8,128)(2,1)S(1)} async-done(((bf16[8,336,128]{2,1,0:T(8,128)(2,1)}), bf16[8,336,128]{2,1,0:T(8,128)(2,1)S(1)}, u32[]{:S(2)}, u32[]{:S(2)}) %all-to-all-start) | async-done | bytes 688160 | tf_op jit(solution)/shard_map/all_to_all | solution.py:274
  28.7 0.9 copy-done.2
  29.6 4.3 %attention.1 = bf16[8,64,128]{2,1,0:T(8,128)(2,1)} custom-call(s32[1]{0:T(128)} %bitcast.2.p_ref, bf16[8,336,128]{2,1,0:T(8,128)(2,1)} %copy-done.2), custom_call_target="tpu_custom_call" | custom-call | tf_op jit(solution)/shard_map/attention/pallas_call | solution.py:276
  33.9 11.0 %all_to_all.20.refs_0_ = bf16[8,64,128]{2,1,0:T(8,128)(2,1)S(1)} all-to-all(bf16[8,64,128]{2,1,0:T(8,128)(2,1)} %attention.1), channel_id=1, replica_groups=mesh['sp'=8,'tp'=4] {'sp'}, dimensions={0} | all-to-all | bytes 262144 | tf_op jit(solution)/shard_map/all_to_all | solution.py:283
  44.9 1.5 collective-permute-start
  46.4 0.0 collective-permute-start.1
  46.4 3.4 %collective-permute-done.refs_1_ = bf16[8,64,128]{2,1,0:T(8,128)(2,1)S(1)} collective-permute-done((bf16[8,64,128]{2,1,0:T(8,128)(2,1)S(1)}, bf16[8,64,128]{2,1,0:T(8,128)(2,1)S(1)}, u32[]{:S(2)}, u32[]{:S(2)}) %collective-permute-start) | collective-permute-done | bytes 131104 | tf_op jit(solution)/shard_map/ppermute | solution.py:229
  49.8 0.0 collective-permute-start.2
  49.8 0.0 collective-permute-done.1.refs_2_
  49.9 1.3 collective-permute-done.2.refs_3_
  51.2 0.6 copy-done.11
  51.8 4.6 %project.1 = (bf16[128,1024]{1,0:T(8,128)(2,1)}, bf16[512,1024]{1,0:T(8,128)(2,1)}) custom-call(s32[1]{0:T(128)} %bitcast.t_ref, s32[2,128]{1,0:T(2,128)} %bitcast.13, bf16[8,64,128]{2,1,0:T(8,128)(2,1)} %copy-done.3, bf16[8,64,128]{2,1,0:T(8,128)(2,1)} %copy-done.9, bf16[8,64,128]{2,1,0:T(8,128)(2,1)} %copy-done.10, bf16[8,64,128]{2,1,0:T(8,128)(2,1)} %copy-done.11, ...), custom_call_target="tpu_custom_call" | custom-call | tf_op jit(solution)/shard_map/project/pallas_call | solution.py:298
  56.4 3.6 %all-to-all-start.2 = ((bf16[8,2,32,1024]{3,2,1,0:T(8,128)(2,1)}), bf16[8,2,32,1024]{3,2,1,0:T(8,128)(2,1)S(1)}, u32[]{:S(2)}, u32[]{:S(2)}) async-start(bf16[8,2,32,1024]{3,2,1,0:T(8,128)(2,1)} %bitcast.9), calls=%async_computation.2 | async-start | bytes 2097152 | tf_op jit(solution)/shard_map/all_to_all | solution.py:315
  60.0 26.3 %all-to-all-done.2.x_ref = bf16[8,2,32,1024]{3,2,1,0:T(8,128)(2,1)S(1)} async-done(((bf16[8,2,32,1024]{3,2,1,0:T(8,128)(2,1)}), bf16[8,2,32,1024]{3,2,1,0:T(8,128)(2,1)S(1)}, u32[]{:S(2)}, u32[]{:S(2)}) %all-to-all-start.2) | async-done | bytes 1048608 | tf_op jit(solution)/shard_map/all_to_all | solution.py:315
  86.3 1.0 copy-done
  87.3 3.1 %routed.3 = bf16[256,896]{1,0:T(8,128)(2,1)} custom-call(s32[1]{0:T(128)S(6)} %sub.3.e_ref, bf16[8,2,32,1024]{3,2,1,0:T(8,128)(2,1)} %copy-done, f32[1,1024]{1,0:T(1,128)} %bitcast.10, bf16[2,1024,384]{2,1,0:T(8,128)(2,1)} %gate_ref.4, bf16[2,1024,384]{2,1,0:T(8,128)(2,1)} %up_ref.4), custom_call_target="tpu_custom_call" | custom-call | tf_op jit(solution)/shard_map/routed/pallas_call | solution.py:363
  90.3 0.0 collective-permute-start.3
  90.3 3.0 %routed.2.a_ref = bf16[256,896]{1,0:T(8,128)(2,1)} custom-call(s32[1]{0:T(128)S(6)} %select_n.13.e_ref.c_ref, bf16[8,2,32,1024]{3,2,1,0:T(8,128)(2,1)} %copy-done, f32[1,1024]{1,0:T(1,128)} %bitcast.11, bf16[2,1024,384]{2,1,0:T(8,128)(2,1)} %gate_ref.4, bf16[2,1024,384]{2,1,0:T(8,128)(2,1)} %up_ref.4), custom_call_target="tpu_custom_call" | custom-call | tf_op jit(solution)/shard_map/routed/pallas_call | solution.py:363
  93.4 0.0 collective-permute-done.3.b_ref
  93.4 0.8 copy-done.5
  94.1 2.3 %add.14.a_ref = bf16[256,896]{1,0:T(8,128)(2,1)} custom-call(bf16[256,896]{1,0:T(8,128)(2,1)} %routed.2.a_ref, bf16[256,896]{1,0:T(8,128)(2,1)} %copy-done.5), custom_call_target="tpu_custom_call" | custom-call | tf_op jit(solution)/shard_map/add/pallas_call | solution.py:329
  96.4 1.5 collective-permute-start.4
  97.9 11.6 %collective-permute-done.4.b_ref = bf16[256,896]{1,0:T(8,128)(2,1)S(1)} collective-permute-done((bf16[256,896]{1,0:T(8,128)(2,1)}, bf16[256,896]{1,0:T(8,128)(2,1)S(1)}, u32[]{:S(2)}, u32[]{:S(2)}) %collective-permute-start.4) | collective-permute-done | bytes 458784 | tf_op jit(solution)/shard_map/ppermute | solution.py:229
  109.6 0.8 copy-done.4
  110.3 2.1 %hidden.2.own_ref = bf16[256,384]{1,0:T(8,128)(2,1)} custom-call(bf16[256,896]{1,0:T(8,128)(2,1)} %add.14.a_ref, bf16[256,896]{1,0:T(8,128)(2,1)} %copy-done.4), custom_call_target="tpu_custom_call" | custom-call | tf_op jit(solution)/shard_map/hidden/pallas_call | solution.py:337
  112.4 0.0 collective-permute-start.5
  112.4 1.6 %collective-permute-done.5.other_ref = bf16[256,384]{1,0:T(8,128)(2,1)S(1)} collective-permute-done((bf16[256,384]{1,0:T(8,128)(2,1)}, bf16[256,384]{1,0:T(8,128)(2,1)S(1)}, u32[]{:S(2)}, u32[]{:S(2)}) %collective-permute-start.5) | collective-permute-done | bytes 196640 | tf_op jit(solution)/shard_map/ppermute | solution.py:229
  114.1 0.7 copy-done.8
  114.8 3.3 %down.1 = bf16[8,2,32,1024]{3,2,1,0:T(8,128)(2,1)} custom-call(s32[1]{0:T(128)S(6)} %select_n.13.e_ref.c_ref, bf16[256,384]{1,0:T(8,128)(2,1)} %hidden.2.own_ref, bf16[256,384]{1,0:T(8,128)(2,1)} %copy-done.8, bf16[2,384,1024]{2,1,0:T(8,128)(2,1)} %w_ref.1), custom_call_target="tpu_custom_call" | custom-call | tf_op jit(solution)/shard_map/down/pallas_call | solution.py:378
  118.1 3.6 %all-to-all-start.3 = ((bf16[8,2,32,1024]{3,2,1,0:T(8,128)(2,1)}), bf16[8,2,32,1024]{3,2,1,0:T(8,128)(2,1)S(1)}, u32[]{:S(2)}, u32[]{:S(2)}) async-start(bf16[8,2,32,1024]{3,2,1,0:T(8,128)(2,1)} %down.1), calls=%async_computation.3 | async-start | bytes 2097152 | tf_op jit(solution)/shard_map/all_to_all | solution.py:384
  121.7 0.0 copy-start.13
  121.7 2.6 %shared.1.a_ref = bf16[128,896]{1,0:T(8,128)(2,1)} custom-call(bf16[128,1024]{1,0:T(8,128)(2,1)} %get-tuple-element.8.mixed_ref, f32[1,1024]{1,0:T(1,128)} %bitcast.12, bf16[1024,384]{1,0:T(8,128)(2,1)} %gate_ref.5, bf16[1024,384]{1,0:T(8,128)(2,1)} %up_ref.5), custom_call_target="tpu_custom_call" | custom-call | tf_op jit(solution)/shard_map/shared/pallas_call | solution.py:321
  124.3 0.1 collective-permute-start.6
  124.4 1.6 %collective-permute-done.6.b_ref = bf16[128,896]{1,0:T(8,128)(2,1)S(1)} collective-permute-done((bf16[128,896]{1,0:T(8,128)(2,1)}, bf16[128,896]{1,0:T(8,128)(2,1)S(1)}, u32[]{:S(2)}, u32[]{:S(2)}) %collective-permute-start.6) | collective-permute-done | bytes 229408 | tf_op jit(solution)/shard_map/ppermute | solution.py:229
  126.0 0.7 copy-done.7
  126.7 1.9 %add.15.a_ref = bf16[128,896]{1,0:T(8,128)(2,1)} custom-call(bf16[128,896]{1,0:T(8,128)(2,1)} %shared.1.a_ref, bf16[128,896]{1,0:T(8,128)(2,1)} %copy-done.7), custom_call_target="tpu_custom_call" | custom-call | tf_op jit(solution)/shard_map/add/pallas_call | solution.py:329
  128.6 1.5 collective-permute-start.7
  130.1 0.7 copy.17.ids_ref
  130.9 0.7 copy.18.rw_ref
  131.6 4.9 %collective-permute-done.7.b_ref = bf16[128,896]{1,0:T(8,128)(2,1)S(1)} collective-permute-done((bf16[128,896]{1,0:T(8,128)(2,1)}, bf16[128,896]{1,0:T(8,128)(2,1)S(1)}, u32[]{:S(2)}, u32[]{:S(2)}) %collective-permute-start.7) | collective-permute-done | bytes 229408 | tf_op jit(solution)/shard_map/ppermute | solution.py:229
  136.5 0.7 copy-done.6
  137.2 1.9 %hidden.3.hid_ref = bf16[128,384]{1,0:T(8,128)(2,1)} custom-call(bf16[128,896]{1,0:T(8,128)(2,1)} %add.15.a_ref, bf16[128,896]{1,0:T(8,128)(2,1)} %copy-done.6), custom_call_target="tpu_custom_call" | custom-call | tf_op jit(solution)/shard_map/hidden/pallas_call | solution.py:337
  139.1 8.9 %all-to-all-done.3 = bf16[8,2,32,1024]{3,2,1,0:T(8,128)(2,1)S(1)} async-done(((bf16[8,2,32,1024]{3,2,1,0:T(8,128)(2,1)}), bf16[8,2,32,1024]{3,2,1,0:T(8,128)(2,1)S(1)}, u32[]{:S(2)}, u32[]{:S(2)}) %all-to-all-start.3) | async-done | bytes 1048608 | tf_op jit(solution)/shard_map/all_to_all | solution.py:384
  147.9 1.0 copy-done.1
  148.9 3.1 %combine.1 = bf16[128,1024]{1,0:T(8,128)(2,1)} custom-call(s32[128,2]{1,0:T(8,128)} %copy.17.ids_ref, f32[128,2]{1,0:T(8,128)} %copy.18.rw_ref, bf16[512,1024]{1,0:T(8,128)(2,1)} %bitcast.8, bf16[128,1024]{1,0:T(8,128)(2,1)} %get-tuple-element.8.mixed_ref, bf16[128,384]{1,0:T(8,128)(2,1)} %hidden.3.hid_ref, bf16[384,1024]{1,0:T(8,128)(2,1)} %down_ref.1), custom_call_target="tpu_custom_call" | custom-call | tf_op jit(solution)/shard_map/combine/pallas_call | solution.py:385
  (18 shorter events, 0.0 us)
Async XLA Ops:
  3.4 25.3 %all-to-all-start = ((bf16[8,336,128]{2,1,0:T(8,128)(2,1)}), bf16[8,336,128]{2,1,0:T(8,128)(2,1)S(1)}, u32[]{:S(2)}, u32[]{:S(2)}) async-start(bf16[8,336,128]{2,1,0:T(8,128)(2,1)} %pack.1), calls=%async_computation | async-start | bytes 1376256 | tf_op jit(solution)/shard_map/all_to_all | solution.py:274
  28.7 0.9 copy-start.2
  44.9 6.3 %copy-start.3 = (bf16[8,64,128]{2,1,0:T(8,128)(2,1)}, bf16[8,64,128]{2,1,0:T(8,128)(2,1)S(1)}, u32[]{:S(2)}) copy-start(bf16[8,64,128]{2,1,0:T(8,128)(2,1)S(1)} %all_to_all.20.refs_0_) | copy-start | bytes 393220
  44.9 5.0 %collective-permute-start = (bf16[8,64,128]{2,1,0:T(8,128)(2,1)S(1)}, bf16[8,64,128]{2,1,0:T(8,128)(2,1)S(1)}, u32[]{:S(2)}, u32[]{:S(2)}) collective-permute-start(bf16[8,64,128]{2,1,0:T(8,128)(2,1)S(1)} %all_to_all.20.refs_0_), channel_id=1, source_target_pairs={{0,2},{1,3},{2,0},{3,1},{4,6},{5,7},{6,4},{7,5},{8,10},{9,11},{10,... | collective-permute-start | bytes 393224 | tf_op jit(solution)/shard_map/ppermute | solution.py:229
  46.4 3.5 %collective-permute-start.1 = (bf16[8,64,128]{2,1,0:T(8,128)(2,1)S(1)}, bf16[8,64,128]{2,1,0:T(8,128)(2,1)S(1)}, u32[]{:S(2)}, u32[]{:S(2)}) collective-permute-start(bf16[8,64,128]{2,1,0:T(8,128)(2,1)S(1)} %all_to_all.20.refs_0_), channel_id=1, source_target_pairs={{0,1},{1,0},{2,3},{3,2},{4,5},{5,4},{6,7},{7,6},{8,9},{9,8},{10,11... | collective-permute-start | bytes 393224 | tf_op jit(solution)/shard_map/ppermute | solution.py:229
  49.8 1.4 copy-start.9
  49.8 1.3 collective-permute-start.2
  49.9 1.3 copy-start.10
  51.2 0.6 copy-start.11
  56.4 29.8 %all-to-all-start.2 = ((bf16[8,2,32,1024]{3,2,1,0:T(8,128)(2,1)}), bf16[8,2,32,1024]{3,2,1,0:T(8,128)(2,1)S(1)}, u32[]{:S(2)}, u32[]{:S(2)}) async-start(bf16[8,2,32,1024]{3,2,1,0:T(8,128)(2,1)} %bitcast.9), calls=%async_computation.2 | async-start | bytes 2097152 | tf_op jit(solution)/shard_map/all_to_all | solution.py:315
  86.3 1.0 copy-start
  90.3 3.0 %collective-permute-start.3 = (bf16[256,896]{1,0:T(8,128)(2,1)}, bf16[256,896]{1,0:T(8,128)(2,1)S(1)}, u32[]{:S(2)}, u32[]{:S(2)}) collective-permute-start(bf16[256,896]{1,0:T(8,128)(2,1)} %routed.3), channel_id=1, source_target_pairs={{0,1},{1,0},{2,3},{3,2},{4,5},{5,4},{6,7},{7,6},{8,9},{9,8},{10,11... | collective-permute-start | bytes 1376264 | tf_op jit(solution)/shard_map/ppermute | solution.py:229
  93.4 0.8 copy-start.5
  96.4 13.1 %collective-permute-start.4 = (bf16[256,896]{1,0:T(8,128)(2,1)}, bf16[256,896]{1,0:T(8,128)(2,1)S(1)}, u32[]{:S(2)}, u32[]{:S(2)}) collective-permute-start(bf16[256,896]{1,0:T(8,128)(2,1)} %add.14.a_ref), channel_id=1, source_target_pairs={{0,2},{1,3},{2,0},{3,1},{4,6},{5,7},{6,4},{7,5},{8,10},{9,11},{10,... | collective-permute-start | bytes 1376264 | tf_op jit(solution)/shard_map/ppermute | solution.py:229
  109.6 0.8 copy-start.4
  112.4 1.7 %collective-permute-start.5 = (bf16[256,384]{1,0:T(8,128)(2,1)}, bf16[256,384]{1,0:T(8,128)(2,1)S(1)}, u32[]{:S(2)}, u32[]{:S(2)}) collective-permute-start(bf16[256,384]{1,0:T(8,128)(2,1)} %hidden.2.own_ref), channel_id=1, source_target_pairs={{0,1},{1,0},{2,3},{3,2},{4,5},{5,4},{6,7},{7,6},{8,9},{9,8},{10,11... | collective-permute-start | bytes 589832 | tf_op jit(solution)/shard_map/ppermute | solution.py:229
  114.1 0.7 copy-start.8
  118.1 29.8 %all-to-all-start.3 = ((bf16[8,2,32,1024]{3,2,1,0:T(8,128)(2,1)}), bf16[8,2,32,1024]{3,2,1,0:T(8,128)(2,1)S(1)}, u32[]{:S(2)}, u32[]{:S(2)}) async-start(bf16[8,2,32,1024]{3,2,1,0:T(8,128)(2,1)} %down.1), calls=%async_computation.3 | async-start | bytes 2097152 | tf_op jit(solution)/shard_map/all_to_all | solution.py:384
  121.7 8.4 %copy-start.12 = (s32[128,2]{0,1:T(2,128)S(1)}, s32[128,2]{0,1:T(2,128)}, u32[]{:S(2)}) copy-start(s32[128,2]{0,1:T(2,128)} %param.22) | copy-start | bytes 3076
  121.7 9.2 %copy-start.13 = (f32[128,2]{0,1:T(2,128)S(1)}, f32[128,2]{0,1:T(2,128)}, u32[]{:S(2)}) copy-start(f32[128,2]{0,1:T(2,128)} %param.23) | copy-start | bytes 3076
  124.3 1.7 %collective-permute-start.6 = (bf16[128,896]{1,0:T(8,128)(2,1)}, bf16[128,896]{1,0:T(8,128)(2,1)S(1)}, u32[]{:S(2)}, u32[]{:S(2)}) collective-permute-start(bf16[128,896]{1,0:T(8,128)(2,1)} %shared.1.a_ref), channel_id=1, source_target_pairs={{0,1},{1,0},{2,3},{3,2},{4,5},{5,4},{6,7},{7,6},{8,9},{9,8},{10,11... | collective-permute-start | bytes 688136 | tf_op jit(solution)/shard_map/ppermute | solution.py:229
  126.0 0.7 copy-start.7
  128.6 7.9 %collective-permute-start.7 = (bf16[128,896]{1,0:T(8,128)(2,1)}, bf16[128,896]{1,0:T(8,128)(2,1)S(1)}, u32[]{:S(2)}, u32[]{:S(2)}) collective-permute-start(bf16[128,896]{1,0:T(8,128)(2,1)} %add.15.a_ref), channel_id=1, source_target_pairs={{0,2},{1,3},{2,0},{3,1},{4,6},{5,7},{6,4},{7,5},{8,10},{9,11},{10,... | collective-permute-start | bytes 688136 | tf_op jit(solution)/shard_map/ppermute | solution.py:229
  136.5 0.7 copy-start.6
  147.9 1.0 copy-start.1

commit v2 on v0

v2 whole, which is shorter than its diff:
```python
import functools

import jax
import jax.numpy as jnp
from jax import lax
from jax.experimental import pallas as pl
from jax.experimental.pallas import tpu as pltpu
from jax.sharding import PartitionSpec as P


EPS = 1e-06
LANES = 128
BIAS_ROWS = 16
VMEM_LIMIT = 16 * 1024 * 1024
BF = jnp.bfloat16
F32 = jnp.float32


def vmem():
    return pl.BlockSpec(memory_space=pltpu.VMEM)


def hbm():
    return pl.BlockSpec(memory_space=pltpu.HBM)


def in_hbm(x):
    return pltpu.with_memory_space_constraint(x, pltpu.HBM)


def smem():
    return pl.BlockSpec(memory_space=pltpu.SMEM)


def call(kernel, out_shape, in_specs, scratch=()):
    many = isinstance(out_shape, (tuple, list))
    return pl.pallas_call(
        kernel,
        out_shape=out_shape,
        in_specs=in_specs,
        out_specs=tuple(vmem() for _ in out_shape) if many else vmem(),
        scratch_shapes=list(scratch),
        compiler_params=pltpu.CompilerParams(vmem_limit_bytes=VMEM_LIMIT),
    )


def iota(shape, dim):
    return lax.broadcasted_iota(jnp.int32, shape, dim)


def dot(a, b):
    return jnp.dot(a, b, preferred_element_type=F32)


def split_pair(x):
    high = x.astype(BF)
    return high, (x - high.astype(F32)).astype(BF)


def pack_kernel(at_ref, q_ref, k_ref, v_ref, b_ref, *refs, hd):
    outs, sems = refs[:-1], refs[-1]
    tok = k_ref.shape[0]
    copies = []
    for mh, out in enumerate(outs):
        head = jnp.bitwise_xor(at_ref[0], mh)
        cols = pl.ds(pl.multiple_of(head * hd, hd), hd)
        for i, (src, start) in enumerate(
            ((k_ref, 0), (v_ref, tok), (q_ref, 2 * tok + BIAS_ROWS))
        ):
            copy = pltpu.make_async_copy(
                src.at[:, cols], out.at[pl.ds(start, tok)], sems.at[3 * mh + i]
            )
            copy.start()
            copies.append(copy)
    bias = b_ref[...].astype(F32)
    for mh, out in enumerate(outs):
        head = jnp.bitwise_xor(at_ref[0], mh)
        row = jnp.where(iota(bias.shape, 0) == head, bias, 0.0)
        row = jnp.sum(row, axis=0, keepdims=True)
        out[2 * tok : 2 * tok + BIAS_ROWS] = jnp.broadcast_to(row, (BIAS_ROWS, tok)).astype(BF)
    for copy in copies:
        copy.wait()


def attention_kernel(at_ref, w_hbm, *refs, heads, group):
    blocks = heads * group
    ins, outs = refs[:blocks], refs[blocks : blocks + heads]
    w_ref, kv_ref, q_ref, acc_ref, carry_ref, sem = refs[blocks + heads :]
    fetch = pltpu.make_async_copy(w_hbm, w_ref, sem)
    fetch.start()
    rows, hd = ins[0].shape
    kv_rows = kv_ref.shape[1]
    tok = rows - kv_rows
    h, p = at_ref[0], at_ref[1]
    for mh in range(heads):
        g = jnp.bitwise_xor(h, mh)
        q_ref[pl.ds(pl.multiple_of(g * tok, tok), tok)] = ins[mh * group][kv_rows:]
        for mp in range(group):
            kv_ref[g * group + jnp.bitwise_xor(p, mp)] = ins[mh * group + mp][:kv_rows]
    acc_ref[...] = jnp.zeros_like(acc_ref)
    carry_ref[...] = jnp.zeros_like(carry_ref)
    src = iota((2 * tok, 2 * tok), 0)
    src = jnp.where(src >= tok, src - tok, src)
    dst = iota((2 * tok, 2 * tok), 1)
    tri = jnp.where((dst >= tok) | (src > dst), 1.0, 0.0).astype(BF)
    scale = hd ** (-0.5)
    for j in reversed(range(blocks)):
        r0 = (j // group) * tok
        n = heads * tok - r0
        keys = kv_ref[j, 0:tok]
        values = kv_ref[j, tok : 2 * tok]
        bias = kv_ref[j, 2 * tok : 2 * tok + BIAS_ROWS].astype(F32)[0:1, :]
        raw = lax.dot_general(
            q_ref[r0:], keys, (((1,), (1,)), ((), ())), preferred_element_type=F32
        )
        logits = raw * scale + bias
        soft = jnp.log(1.0 + jnp.exp(-jnp.abs(logits)))
        fail = -(jnp.maximum(logits, 0.0) + soft)
        row = iota((n, tok), 0)
        before = (row >= tok) | (iota((n, tok), 1) < row + (p - j % group) * tok)
        stay = logits + fail
        fail = jnp.where(before, fail, 0.0)
        high, low = split_pair(fail)
        sums = dot(jnp.concatenate([high, low], axis=1), tri)
        carry = carry_ref[r0:]
        weights = jnp.where(before, jnp.exp(stay + sums[:, :tok] + carry), 0.0)
        carry_ref[r0:] = carry + sums[:, tok:]
        acc_ref[r0:] += dot(weights.astype(BF), values)
    for mh in range(heads):
        g = jnp.bitwise_xor(h, mh)
        outs[mh][...] = acc_ref[pl.ds(pl.multiple_of(g * tok, tok), tok)].astype(BF)
    fetch.wait()


def stack_kernel(*refs):
    for i, ref in enumerate(refs[:-1]):
        refs[-1][i] = ref[...]


def slots_of(ids_ref, s, c, local, blocks):
    tok = ids_ref.shape[1]
    expert = jnp.bitwise_xor(iota((blocks, tok), 0), s) * local + c
    named = [expert == ids_ref[k : k + 1, :] for k in range(ids_ref.shape[0])]
    hit = functools.reduce(jnp.logical_or, named)
    order = jnp.where(iota((tok, tok), 0) < iota((tok, tok), 1), 1.0, 0.0).astype(BF)
    rank = dot(jnp.where(hit, 1.0, 0.0).astype(BF), order)
    return named, jnp.where(hit, rank, -1.0)


def spread(rank, values, cap):
    slot = iota((cap, rank.shape[1]), 0).astype(F32)
    return jnp.concatenate(
        [
            jnp.where(slot == rank[e : e + 1, :], values[e : e + 1, :], 0.0)
            for e in range(rank.shape[0])
        ],
        axis=0,
    )


def project_kernel(at_ref, *refs, masks, heads):
    count = len(masks)
    pieces = refs[:count]
    w_ref, stream_ref, mixed_ref, rows_ref = refs[count:]
    h, t = at_ref[0], at_ref[2]
    for mask, piece in zip(masks, pieces):
        hd = piece.shape[2]
        for mh in range(heads):
            head = jnp.bitwise_xor(t, mask) * heads + jnp.bitwise_xor(h, mh)
            rows_ref[:, pl.ds(pl.multiple_of(head * hd, hd), hd)] = piece[mh]
    total = stream_ref[...].astype(F32) + dot(rows_ref[...], w_ref[...])
    mixed_ref[...] = total.astype(BF)


def dispatch_kernel(at_ref, ids_ref, own_ref, other_ref, *sends, local):
    cap = sends[0].shape[1]
    _, rank = slots_of(ids_ref, at_ref[3], at_ref[4], local, len(sends))
    pick = spread(rank, jnp.ones_like(rank), cap).astype(BF)
    for side, ref in enumerate((own_ref, other_ref)):
        rows = dot(pick, ref[...]).astype(BF)
        for m, send in enumerate(sends):
            send[side] = rows[m * cap : (m + 1) * cap]


def square_lanes(square):
    high, low = split_pair(square)
    lane = iota((square.shape[0], LANES), 1)
    tail = jnp.where(lane == 0, high.astype(F32), jnp.where(lane == 1, low.astype(F32), 0.0))
    return tail.astype(BF)


def partials(sides):
    gate_sum, up_sum, square = 0.0, 0.0, 0.0
    for x, gain, gate, up in sides:
        scaled = (x * gain).astype(BF)
        square = square + jnp.sum(x * x, axis=1, keepdims=True)
        gate_sum = gate_sum + dot(scaled, gate).astype(BF).astype(F32)
        up_sum = up_sum + dot(scaled, up).astype(BF).astype(F32)
    return jnp.concatenate(
        [gate_sum.astype(BF), up_sum.astype(BF), square_lanes(square)], axis=1
    )


def shared_kernel(mixed_ref, gain_ref, gate_ref, up_ref, out_ref):
    out_ref[...] = partials(
        [(mixed_ref[...].astype(F32), gain_ref[...], gate_ref[...], up_ref[...])]
    )


def routed_kernel(at_ref, *refs):
    e = at_ref[4]
    weights, out_ref = refs[-7:-1], refs[-1]
    sides = []
    for side in range(2):
        x = jnp.concatenate([ref[side].astype(F32) for ref in refs[:-7]], axis=0)
        gain_ref, gate_ref, up_ref = weights[3 * side : 3 * side + 3]
        sides.append((x, gain_ref[...], gate_ref[e], up_ref[e]))
    out_ref[...] = partials(sides)


def add_partials(a_ref, b_ref, width):
    a = a_ref[...].astype(F32)
    b = b_ref[...].astype(F32)
    body = a[:, :width] + b[:, :width]
    square = a[:, width : width + 1] + b[:, width : width + 1]
    square = square + (a[:, width + 1 : width + 2] + b[:, width + 1 : width + 2])
    return body, square


def add_kernel(a_ref, b_ref, out_ref, *, width):
    body, square = add_partials(a_ref, b_ref, width)
    out_ref[...] = jnp.concatenate([body.astype(BF), square_lanes(square)], axis=1)


def hidden_of(a_ref, b_ref, width, features):
    body, square = add_partials(a_ref, b_ref, width)
    inv = lax.rsqrt(square / features + EPS)
    gate = body[:, : width // 2] * inv
    up = body[:, width // 2 :] * inv
    return (gate * jax.nn.sigmoid(gate) * up).astype(BF)


def hidden_kernel(a_ref, b_ref, out_ref, *, width, features):
    out_ref[...] = hidden_of(a_ref, b_ref, width, features)


def down_kernel(at_ref, a_ref, b_ref, own_ref, other_ref, *outs, width, features):
    hidden = hidden_of(a_ref, b_ref, width, features)
    cap = outs[0].shape[1]
    for side, w_ref in enumerate((own_ref, other_ref)):
        rows = dot(hidden, w_ref[at_ref[4]]).astype(BF)
        for i, out in enumerate(outs):
            out[side] = rows[i * cap : (i + 1) * cap]


def base_kernel(at_ref, ids_ref, rw_ref, mixed_ref, hid_ref, down_ref, base_ref, *picks, local, cap):
    blocks = sum(pick.shape[1] for pick in picks) // (2 * cap)
    named, rank = slots_of(ids_ref, at_ref[3], at_ref[4], local, blocks)
    weight = functools.reduce(
        jnp.add,
        [jnp.where(hit, rw_ref[k : k + 1, :], 0.0) for k, hit in enumerate(named)],
    )
    high, low = split_pair(jnp.transpose(spread(rank, weight, cap)))
    start = 0
    for pick in picks:
        width = pick.shape[1] // 2
        pick[:, :width] = high[:, start : start + width]
        pick[:, width:] = low[:, start : start + width]
        start += width
    base_ref[0] = mixed_ref[...].astype(F32) + dot(hid_ref[...], down_ref[...])
    base_ref[1] = jnp.zeros_like(base_ref[1])


def combine_kernel(base_ref, pick_ref, *refs, outs):
    backs, out_refs = refs[:-outs], refs[-outs:]
    for side in range(2):
        rows = jnp.concatenate([ref[side] for ref in backs], axis=0)
        rows = jnp.concatenate([rows, rows], axis=0)
        total = base_ref[side] + dot(pick_ref[...], rows)
        if outs == 1:
            out_refs[0][side] = total
        else:
            out_refs[side][...] = total


def final_kernel(a_ref, b_ref, out_ref):
    out_ref[...] = (a_ref[...] + b_ref[...]).astype(BF)


def swap(x, axis, bit):
    if bit == 0:
        return x
    count = lax.axis_size(axis)
    return lax.ppermute(x, axis, [(i, i ^ bit) for i in range(count)])


def layer(
    queries,
    key_rows,
    value_rows,
    break_bias,
    stream,
    out_proj,
    norm_gain,
    expert_ids,
    route_weights,
    gate_proj,
    up_proj,
    down_proj,
    shared_gate,
    shared_up,
    shared_down,
):
    tok = queries.shape[0]
    heads = break_bias.shape[1]
    hd = queries.shape[1] // heads
    blocks = lax.axis_size("sp")
    tp = lax.axis_size("tp")
    feats = stream.shape[1]
    features = feats * tp
    s_index = lax.axis_index("sp").astype(jnp.int32)
    t_index = lax.axis_index("tp").astype(jnp.int32)
    group = blocks // heads
    h_index, p_index = s_index // group, s_index % group

    def array(*shape):
        return jax.ShapeDtypeStruct(shape, BF)

    at = jnp.stack([h_index, p_index, t_index, s_index, t_index % 2])
    rows = 3 * tok + BIAS_ROWS
    gain = norm_gain.reshape(1, feats)
    others = [swap(x, "tp", 1) for x in (gain, gate_proj, up_proj, down_proj)]
    packed = call(
        functools.partial(pack_kernel, hd=hd),
        (array(rows, hd),) * heads,
        [smem()] + [hbm()] * 3 + [vmem()],
        [pltpu.SemaphoreType.DMA((3 * heads,))],
    )(at, in_hbm(queries), in_hbm(key_rows), in_hbm(value_rows), break_bias.T)
    qkv = [swap(packed[mh], "sp", mh * group) for mh in range(heads)]
    qkv = [swap(qkv[mh], "sp", mp) for mh in range(heads) for mp in range(group)]
    *attended, out_w = call(
        functools.partial(attention_kernel, heads=heads, group=group),
        (array(tok, hd),) * heads + (array(*out_proj.shape),),
        [smem(), hbm()] + [vmem()] * blocks,
        [
            pltpu.VMEM((blocks, rows - tok, hd), BF),
            pltpu.VMEM((heads * tok, hd), BF),
            pltpu.VMEM((heads * tok, hd), F32),
            pltpu.VMEM((heads * tok, tok), F32),
            pltpu.SemaphoreType.DMA,
        ],
    )(at, in_hbm(out_proj), *qkv)
    piece = call(stack_kernel, array(heads, tok, hd), [vmem()] * heads)(
        *[swap(attended[mh], "sp", mh * group) for mh in range(heads)]
    )
    bits = [1 << i for i in range(tp.bit_length() - 1)]
    pieces, masks = [piece], [0]
    for bit in reversed(bits):
        pieces = pieces + [swap(x, "tp", bit) for x in pieces]
        masks = masks + [m ^ bit for m in masks]

    local = gate_proj.shape[0]
    experts = local * blocks
    choices = expert_ids.shape[1]
    cap = 2 * choices * tok // experts
    mixed = call(
        functools.partial(project_kernel, masks=tuple(masks), heads=heads),
        array(tok, feats),
        [smem()] + [vmem()] * (len(pieces) + 2),
        [pltpu.VMEM((tok, out_proj.shape[0]), BF)],
    )(at, *pieces, out_w, stream)
    mixed_other = swap(mixed, "tp", 1)
    sends = call(
        functools.partial(dispatch_kernel, local=local),
        (array(2, cap, feats),) * blocks,
        [smem()] + [vmem()] * 3,
    )(at, expert_ids.T, mixed, mixed_other)

    half = blocks // 2
    quarter = half + half // 2
    groups = [range(half), range(half, quarter), range(quarter, blocks)]
    arrived = {m: swap(sends[m], "sp", m) for m in range(blocks)}

    hid_s = shared_gate.shape[1]
    shared_sum = call(
        shared_kernel, array(tok, 2 * hid_s + LANES), [vmem()] * 4
    )(mixed, gain, shared_gate, shared_up)

    def add(a, b, width):
        return call(functools.partial(add_kernel, width=width), array(*a.shape), [vmem()] * 2)(a, b)

    def hidden(a, b, width):
        return call(
            functools.partial(hidden_kernel, width=width, features=features),
            array(a.shape[0], width // 2),
            [vmem()] * 2,
        )(a, b)

    for bit in bits[:-1]:
        shared_sum = add(shared_sum, swap(shared_sum, "tp", bit), 2 * hid_s)
    other = swap(shared_sum, "tp", bits[-1])
    shared_hidden = hidden(shared_sum, other, 2 * hid_s)

    width = 2 * gate_proj.shape[2]
    weights = [gain, gate_proj, up_proj] + others[:3]
    back = {}
    for ms in groups:
        total = call(
            routed_kernel, array(len(ms) * cap, width + LANES), [smem()] + [vmem()] * (len(ms) + 6)
        )(at, *[arrived[m] for m in ms], *weights)
        for bit in bits[1:-1]:
            total = add(total, swap(total, "tp", bit), width)
        came = swap(total, "tp", bits[-1])
        outs = call(
            functools.partial(down_kernel, width=width, features=features),
            (array(2, cap, feats),) * len(ms),
            [smem()] + [vmem()] * 4,
        )(at, total, came, down_proj, others[3])
        for m, out in zip(ms, outs):
            back[m] = swap(out, "sp", m)
    total, *picks = call(
        functools.partial(base_kernel, local=local, cap=cap),
        (jax.ShapeDtypeStruct((2, tok, feats), F32),)
        + tuple(array(tok, 2 * len(ms) * cap) for ms in groups),
        [smem()] + [vmem()] * 5,
    )(at, expert_ids.T, route_weights.T, mixed, shared_hidden, shared_down)
    for i in (1, 0, 2):
        ms, last = groups[i], i == 2
        one = jax.ShapeDtypeStruct((tok, feats), F32)
        total = call(
            functools.partial(combine_kernel, outs=2 if last else 1),
            (one, one) if last else jax.ShapeDtypeStruct((2, tok, feats), F32),
            [vmem()] * (2 + len(ms)),
        )(total, picks[i], *[back[m] for m in ms])
    return call(final_kernel, array(tok, feats), [vmem()] * 2)(total[0], swap(total[1], "tp", 1))


def solution(mesh):
    in_specs = (
        P("sp", "tp"),
        P("sp", "tp"),
        P("sp", "tp"),
        P("sp", "tp"),
        P("sp", "tp"),
        P(None, "tp"),
        P("tp"),
        P("sp", None),
        P("sp", None),
        P("sp", "tp", None),
        P("sp", "tp", None),
        P("sp", None, "tp"),
        P("tp", None),
        P("tp", None),
        P(None, "tp"),
    )
    out_specs = P("sp", "tp")
    return jax.shard_map(layer, mesh=mesh, in_specs=in_specs, out_specs=out_specs, check_vma=False)
```

time: 902 us -> 119 us (0.13)
  other arithmetic: 644 us -> 0 us
  waiting for transfers between devices: 141 us -> 47.6 us
  starting transfers between devices: 9.46 us -> 49.5 us
  blocking collectives: 36.1 us -> 0 us
  matrix products: 27.2 us -> 0 us
  local copies, waits for them, and re-layouts: 26.9 us -> 0.81 us
  Pallas kernels: 0 us -> 20.1 us
  between operations: 13.4 us -> 0.32 us
    another operation x17 -> x0, other arithmetic: 636 us -> none
    all_gather x2 -> x0, waiting for transfers between devices: 59.5 us -> none  [the longest x1 41.1 us: body(): value_piece = lax.all_gather(value_rows, 'sp', axis=0, tiled=True)]
    ppermute x0 -> x38, starting transfers between devices: none -> 49.5 us  [swap(): return lax.ppermute(x, axis, [(i, i ^ bit) for i in range(count)])]
    ppermute x0 -> x38, waiting for transfers between devices: none -> 47.6 us  [swap(): return lax.ppermute(x, axis, [(i, i ^ bit) for i in range(count)])]
    all_to_all x2 -> x0, waiting for transfers between devices: 45.9 us -> none  [the longest x1 24.8 us: body(): lax.all_to_all(expert_out, 'sp', split_axis=1, concat_axis=1, tiled=True)]
    psum x1 -> x0, waiting for transfers between devices: 34.3 us -> none  [body(): lax.psum(up_part.astype(jnp.bfloat16), 'tp').astype(jnp.float32)]
    all_gather x2 -> x0, blocking collectives: 29.7 us -> none  [the longest x1 22.5 us: body(): bias_piece = lax.all_gather(break_bias, 'sp', axis=0, tiled=True)]
    dot_general x16 -> x0, matrix products: 27.2 us -> none  [the longest x4 8.52 us: block_terms(): summary = jnp.einsum('hts,shd->thd', weights, value_heads)]
  transfers between devices with their start and end apart: 5 -> 38, of which waited for: 5 -> 21; matrix products, arithmetic and copies ran while one was open for 1% -> 0% of each run, Pallas kernels for 0% -> 16%
where the time goes in v2:
time: 119 us; the launch traced here: 118 us
  starting transfers between devices  49.5 us (42%)
  waiting for transfers between devices  47.6 us (40%)
  Pallas kernels  20.1 us (17%)
    ppermute x38, starting transfers between devices, swap(): return lax.ppermute(x, axis, [(i, i ^ bit) for i in range(count)])  49.5 us
    ppermute x38, waiting for transfers between devices, swap(): return lax.ppermute(x, axis, [(i, i ^ bit) for i in range(count)])  47.6 us
    pallas_call x3, Pallas kernels, layer(): call(routed_kernel, array(len(ms) * cap, width + LANES), [smem()] + [vmem...  6.4 us
    pallas_call x3, Pallas kernels, layer(): call(functools.partial(down_kernel, width=width, features=features), (arr...  3.28 us
    pallas_call x1, Pallas kernels, layer(): call(functools.partial(attention_kernel, heads=heads, group=group), (arra...  2.97 us
  transfers between devices with their start and end apart: 38, of which 21 were waited for; matrix products, arithmetic and copies ran while one was open for 0% of the time, Pallas kernels for 16%

profile of v2, /device:TPU:0, one launch (start us, length us, event | category | flops | bytes accessed | tf_op | source)
XLA Modules:
  0.0 118.3 jit_solution(6633139266089719338)
XLA Ops:
  1.8 1.6 %shard_map.145 = (bf16[400,128]{1,0:T(8,128)(2,1)S(1)}, bf16[400,128]{1,0:T(8,128)(2,1)S(1)}, bf16[400,128]{1,0:T(8,128)(2,1)S(1)}, bf16[400,128]{1,0:T(8,128)(2,1)S(1)}) custom-call(s32[5]{0:T(128)S(1)} %stack.23.at_ref, bf16[128,512]{1,0:T(8,128)(2,1)} %q_ref.1, bf16[128,512]{1,0:T(8,128)(2,1)} %k_ref.1, bf16[128,512]{1,0:T(8,128)(2,1)} %v_ref.1, ...), custom_call_target="tpu_custom_call" | custom-call | tf_op jit(solution)/shard_map/pallas_call | solution.py:333
  3.4 2.6 %collective-permute-start.1 = (bf16[400,128]{1,0:T(8,128)(2,1)S(1)}, bf16[400,128]{1,0:T(8,128)(2,1)S(1)}, u32[]{:S(2)}, u32[]{:S(2)}) collective-permute-start(bf16[400,128]{1,0:T(8,128)(2,1)S(1)} %get-tuple-element.37), channel_id=1, source_target_pairs={{0,8},{4,12},{8,0},{12,4},{16,24},{20,28},{24,16},{28,20},{1,9},{5... | collective-permute-start | bytes 307208 | tf_op jit(solution)/shard_map/ppermute | solution.py:294
  6.0 2.6 %collective-permute-start.3 = (bf16[400,128]{1,0:T(8,128)(2,1)S(1)}, bf16[400,128]{1,0:T(8,128)(2,1)S(1)}, u32[]{:S(2)}, u32[]{:S(2)}) collective-permute-start(bf16[400,128]{1,0:T(8,128)(2,1)S(1)} %get-tuple-element.38), channel_id=1, source_target_pairs={{0,16},{4,20},{8,24},{12,28},{16,0},{20,4},{24,8},{28,12},{1,17},{... | collective-permute-start | bytes 307208 | tf_op jit(solution)/shard_map/ppermute | solution.py:294
  9.6 4.8 %collective-permute-start.5 = (bf16[400,128]{1,0:T(8,128)(2,1)S(1)}, bf16[400,128]{1,0:T(8,128)(2,1)S(1)}, u32[]{:S(2)}, u32[]{:S(2)}) collective-permute-start(bf16[400,128]{1,0:T(8,128)(2,1)S(1)} %get-tuple-element.39), channel_id=1, source_target_pairs={{0,24},{4,28},{8,16},{12,20},{16,8},{20,12},{24,0},{28,4},{1,25},{... | collective-permute-start | bytes 307208 | tf_op jit(solution)/shard_map/ppermute | solution.py:294
  14.4 1.5 %collective-permute-start = (bf16[400,128]{1,0:T(8,128)(2,1)S(1)}, bf16[400,128]{1,0:T(8,128)(2,1)S(1)}, u32[]{:S(2)}, u32[]{:S(2)}) collective-permute-start(bf16[400,128]{1,0:T(8,128)(2,1)S(1)} %get-tuple-element.36.refs_0_), channel_id=1, source_target_pairs={{0,4},{4,0},{8,12},{12,8},{16,20},{20,16},{24,28},{28,24},{1,5},{5... | collective-permute-start | bytes 307208 | tf_op jit(solution)/shard_map/ppermute | solution.py:294
  15.9 1.3 %collective-permute-done.5.refs_6_ = bf16[400,128]{1,0:T(8,128)(2,1)S(1)} collective-permute-done((bf16[400,128]{1,0:T(8,128)(2,1)S(1)}, bf16[400,128]{1,0:T(8,128)(2,1)S(1)}, u32[]{:S(2)}, u32[]{:S(2)}) %collective-permute-start.5) | collective-permute-done | bytes 102432 | tf_op jit(solution)/shard_map/ppermute | solution.py:294
  17.2 1.5 %collective-permute-start.2 = (bf16[400,128]{1,0:T(8,128)(2,1)S(1)}, bf16[400,128]{1,0:T(8,128)(2,1)S(1)}, u32[]{:S(2)}, u32[]{:S(2)}) collective-permute-start(bf16[400,128]{1,0:T(8,128)(2,1)S(1)} %collective-permute-done.1.refs_2_), channel_id=1, source_target_pairs={{0,4},{4,0},{8,12},{12,8},{16,20},{20,16},{24,28},{28,24},{1,5},{5... | collective-permute-start | bytes 307208 | tf_op jit(solution)/shard_map/ppermute | solution.py:294
  19.3 1.5 %collective-permute-start.4 = (bf16[400,128]{1,0:T(8,128)(2,1)S(1)}, bf16[400,128]{1,0:T(8,128)(2,1)S(1)}, u32[]{:S(2)}, u32[]{:S(2)}) collective-permute-start(bf16[400,128]{1,0:T(8,128)(2,1)S(1)} %collective-permute-done.3.refs_4_), channel_id=1, source_target_pairs={{0,4},{4,0},{8,12},{12,8},{16,20},{20,16},{24,28},{28,24},{1,5},{5... | collective-permute-start | bytes 307208 | tf_op jit(solution)/shard_map/ppermute | solution.py:294
  20.8 1.6 %collective-permute-done.2.refs_3_ = bf16[400,128]{1,0:T(8,128)(2,1)S(1)} collective-permute-done((bf16[400,128]{1,0:T(8,128)(2,1)S(1)}, bf16[400,128]{1,0:T(8,128)(2,1)S(1)}, u32[]{:S(2)}, u32[]{:S(2)}) %collective-permute-start.2) | collective-permute-done | bytes 102432 | tf_op jit(solution)/shard_map/ppermute | solution.py:294
  22.3 1.5 %collective-permute-start.6 = (bf16[400,128]{1,0:T(8,128)(2,1)S(1)}, bf16[400,128]{1,0:T(8,128)(2,1)S(1)}, u32[]{:S(2)}, u32[]{:S(2)}) collective-permute-start(bf16[400,128]{1,0:T(8,128)(2,1)S(1)} %collective-permute-done.5.refs_6_), channel_id=1, source_target_pairs={{0,4},{4,0},{8,12},{12,8},{16,20},{20,16},{24,28},{28,24},{1,5},{5... | collective-permute-start | bytes 307208 | tf_op jit(solution)/shard_map/ppermute | solution.py:294
  24.8 2.2 %collective-permute-done.6.refs_7_ = bf16[400,128]{1,0:T(8,128)(2,1)S(1)} collective-permute-done((bf16[400,128]{1,0:T(8,128)(2,1)S(1)}, bf16[400,128]{1,0:T(8,128)(2,1)S(1)}, u32[]{:S(2)}, u32[]{:S(2)}) %collective-permute-start.6) | collective-permute-done | bytes 102432 | tf_op jit(solution)/shard_map/ppermute | solution.py:294
  27.0 3.0 %shard_map.146 = (bf16[128,128]{1,0:T(8,128)(2,1)S(1)}, bf16[128,128]{1,0:T(8,128)(2,1)S(1)}, bf16[128,128]{1,0:T(8,128)(2,1)S(1)}, bf16[128,128]{1,0:T(8,128)(2,1)S(1)}, bf16[2048,1024]{1,0:T(8,128)(2,1)S(1)}) custom-call(s32[5]{0:T(128)S(1)} %stack.23.at_ref, bf16[2048,1024]{1,0:T(8,128)(2,1)} %w_hbm.1, bf16[400,128]{1,0:T(8,128)(2,1)S(1)} %get-tuple-element.36.refs_0_, ...), custom_call_target="tpu_custom_call" | custom-call | tf_op jit(solution)/shard_map/pallas_call | solution.py:341
  30.0 2.5 %collective-permute-start.7 = (bf16[128,128]{1,0:T(8,128)(2,1)S(1)}, bf16[128,128]{1,0:T(8,128)(2,1)S(1)}, u32[]{:S(2)}, u32[]{:S(2)}) collective-permute-start(bf16[128,128]{1,0:T(8,128)(2,1)S(1)} %get-tuple-element.41), channel_id=1, source_target_pairs={{0,8},{4,12},{8,0},{12,4},{16,24},{20,28},{24,16},{28,20},{1,9},{5... | collective-permute-start | bytes 98312 | tf_op jit(solution)/shard_map/ppermute | solution.py:294
  32.4 1.3 %collective-permute-start.8 = (bf16[128,128]{1,0:T(8,128)(2,1)S(1)}, bf16[128,128]{1,0:T(8,128)(2,1)S(1)}, u32[]{:S(2)}, u32[]{:S(2)}) collective-permute-start(bf16[128,128]{1,0:T(8,128)(2,1)S(1)} %get-tuple-element.42), channel_id=1, source_target_pairs={{0,16},{4,20},{8,24},{12,28},{16,0},{20,4},{24,8},{28,12},{1,17},{... | collective-permute-start | bytes 98312 | tf_op jit(solution)/shard_map/ppermute | solution.py:294
  34.3 2.8 %collective-permute-start.9 = (bf16[128,128]{1,0:T(8,128)(2,1)S(1)}, bf16[128,128]{1,0:T(8,128)(2,1)S(1)}, u32[]{:S(2)}, u32[]{:S(2)}) collective-permute-start(bf16[128,128]{1,0:T(8,128)(2,1)S(1)} %get-tuple-element.43), channel_id=1, source_target_pairs={{0,24},{4,28},{8,16},{12,20},{16,8},{20,12},{24,0},{28,4},{1,25},{... | collective-permute-start | bytes 98312 | tf_op jit(solution)/shard_map/ppermute | solution.py:294
  37.3 2.9 %collective-permute-done.9.refs_3_ = bf16[128,128]{1,0:T(8,128)(2,1)S(1)} collective-permute-done((bf16[128,128]{1,0:T(8,128)(2,1)S(1)}, bf16[128,128]{1,0:T(8,128)(2,1)S(1)}, u32[]{:S(2)}, u32[]{:S(2)}) %collective-permute-start.9) | collective-permute-done | bytes 32800 | tf_op jit(solution)/shard_map/ppermute | solution.py:294
  40.2 1.6 %collective-permute-start.10 = (bf16[4,128,128]{2,1,0:T(8,128)(2,1)S(1)}, bf16[4,128,128]{2,1,0:T(8,128)(2,1)S(1)}, u32[]{:S(2)}, u32[]{:S(2)}) collective-permute-start(bf16[4,128,128]{2,1,0:T(8,128)(2,1)S(1)} %shard_map.147.refs_0_), channel_id=1, source_target_pairs={{0,2},{1,3},{2,0},{3,1},{4,6},{5,7},{6,4},{7,5},{8,10},{9,11},{10,... | collective-permute-start | bytes 393224 | tf_op jit(solution)/shard_map/ppermute | solution.py:294
  41.8 3.4 %collective-permute-done.10.refs_1_ = bf16[4,128,128]{2,1,0:T(8,128)(2,1)S(1)} collective-permute-done((bf16[4,128,128]{2,1,0:T(8,128)(2,1)S(1)}, bf16[4,128,128]{2,1,0:T(8,128)(2,1)S(1)}, u32[]{:S(2)}, u32[]{:S(2)}) %collective-permute-start.10) | collective-permute-done | bytes 131104 | tf_op jit(solution)/shard_map/ppermute | solution.py:294
  45.2 1.3 %collective-permute-done.12.refs_3_ = bf16[4,128,128]{2,1,0:T(8,128)(2,1)S(1)} collective-permute-done((bf16[4,128,128]{2,1,0:T(8,128)(2,1)S(1)}, bf16[4,128,128]{2,1,0:T(8,128)(2,1)S(1)}, u32[]{:S(2)}, u32[]{:S(2)}) %collective-permute-start.12) | collective-permute-done | bytes 131104 | tf_op jit(solution)/shard_map/ppermute | solution.py:294
  46.6 1.4 %shard_map.148.mixed_ref.own_ref = bf16[128,1024]{1,0:T(8,128)(2,1)S(1)} custom-call(s32[5]{0:T(128)S(1)} %stack.23.at_ref, bf16[4,128,128]{2,1,0:T(8,128)(2,1)S(1)} %shard_map.147.refs_0_, bf16[4,128,128]{2,1,0:T(8,128)(2,1)S(1)} %collective-permute-done.10.refs_1_, bf16[4,128,128]{2,1,0:T(8,128)(2,1)S(1)} %collective-permute-done.11.refs_2_, ...), custom_call_target="tpu_custom_call" | custom-call | tf_op jit(solution)/shard_map/pallas_call | solution.py:366
  48.2 1.4 %collective-permute-done.15.other_ref = bf16[128,1024]{1,0:T(8,128)(2,1)S(1)} collective-permute-done((bf16[128,1024]{1,0:T(8,128)(2,1)S(1)}, bf16[128,1024]{1,0:T(8,128)(2,1)S(1)}, u32[]{:S(2)}, u32[]{:S(2)}) %collective-permute-start.15) | collective-permute-done | bytes 262176 | tf_op jit(solution)/shard_map/ppermute | solution.py:294
  49.6 1.1 shard_map.153
  50.7 1.6 %collective-permute-start.25 = (bf16[2,32,1024]{2,1,0:T(8,128)(2,1)S(1)}, bf16[2,32,1024]{2,1,0:T(8,128)(2,1)S(1)}, u32[]{:S(2)}, u32[]{:S(2)}) collective-permute-start(bf16[2,32,1024]{2,1,0:T(8,128)(2,1)S(1)} %get-tuple-element.53), channel_id=1, source_target_pairs={{0,4},{4,0},{8,12},{12,8},{16,20},{20,16},{24,28},{28,24},{1,5},{5... | collective-permute-start | bytes 393224 | tf_op jit(solution)/shard_map/ppermute | solution.py:294
  52.3 1.2 collective-permute-done.18.refs_5_.refs_7_
  54.2 2.1 %collective-permute-done.25.refs_1_ = bf16[2,32,1024]{2,1,0:T(8,128)(2,1)S(1)} collective-permute-done((bf16[2,32,1024]{2,1,0:T(8,128)(2,1)S(1)}, bf16[2,32,1024]{2,1,0:T(8,128)(2,1)S(1)}, u32[]{:S(2)}, u32[]{:S(2)}) %collective-permute-start.25) | collective-permute-done | bytes 131104 | tf_op jit(solution)/shard_map/ppermute | solution.py:294
  57.2 1.9 %collective-permute-done.26.refs_2_ = bf16[2,32,1024]{2,1,0:T(8,128)(2,1)S(1)} collective-permute-done((bf16[2,32,1024]{2,1,0:T(8,128)(2,1)S(1)}, bf16[2,32,1024]{2,1,0:T(8,128)(2,1)S(1)}, u32[]{:S(2)}, u32[]{:S(2)}) %collective-permute-start.26) | collective-permute-done | bytes 131104 | tf_op jit(solution)/shard_map/ppermute | solution.py:294
  59.1 1.4 %collective-permute-start.17 = (bf16[2,32,1024]{2,1,0:T(8,128)(2,1)S(1)}, bf16[2,32,1024]{2,1,0:T(8,128)(2,1)S(1)}, u32[]{:S(2)}, u32[]{:S(2)}) collective-permute-start(bf16[2,32,1024]{2,1,0:T(8,128)(2,1)S(1)} %get-tuple-element.48), channel_id=1, source_target_pairs={{0,20},{4,16},{8,28},{12,24},{16,4},{20,0},{24,12},{28,8},{1,21},{... | collective-permute-start | bytes 393224 | tf_op jit(solution)/shard_map/ppermute | solution.py:294
  60.9 7.5 %collective-permute-done.16.refs_0_ = bf16[2,32,1024]{2,1,0:T(8,128)(2,1)S(1)} collective-permute-done((bf16[2,32,1024]{2,1,0:T(8,128)(2,1)S(1)}, bf16[2,32,1024]{2,1,0:T(8,128)(2,1)S(1)}, u32[]{:S(2)}, u32[]{:S(2)}) %collective-permute-start.16) | collective-permute-done | bytes 131104 | tf_op jit(solution)/shard_map/ppermute | solution.py:294
  68.5 2.9 %collective-permute-done.17.refs_1_ = bf16[2,32,1024]{2,1,0:T(8,128)(2,1)S(1)} collective-permute-done((bf16[2,32,1024]{2,1,0:T(8,128)(2,1)S(1)}, bf16[2,32,1024]{2,1,0:T(8,128)(2,1)S(1)}, u32[]{:S(2)}, u32[]{:S(2)}) %collective-permute-start.17) | collective-permute-done | bytes 131104 | tf_op jit(solution)/shard_map/ppermute | solution.py:294
  71.4 1.7 %collective-permute-start.32 = (bf16[2,32,1024]{2,1,0:T(8,128)(2,1)S(1)}, bf16[2,32,1024]{2,1,0:T(8,128)(2,1)S(1)}, u32[]{:S(2)}, u32[]{:S(2)}) collective-permute-start(bf16[2,32,1024]{2,1,0:T(8,128)(2,1)S(1)} %get-tuple-element.61), channel_id=1, source_target_pairs={{0,24},{4,28},{8,16},{12,20},{16,8},{20,12},{24,0},{28,4},{1,25},{... | collective-permute-start | bytes 393224 | tf_op jit(solution)/shard_map/ppermute | solution.py:294
  73.0 2.0 %collective-permute-start.33 = (bf16[2,32,1024]{2,1,0:T(8,128)(2,1)S(1)}, bf16[2,32,1024]{2,1,0:T(8,128)(2,1)S(1)}, u32[]{:S(2)}, u32[]{:S(2)}) collective-permute-start(bf16[2,32,1024]{2,1,0:T(8,128)(2,1)S(1)} %get-tuple-element.62), channel_id=1, source_target_pairs={{0,28},{4,24},{8,20},{12,16},{16,12},{20,8},{24,4},{28,0},{1,29},{... | collective-permute-start | bytes 393224 | tf_op jit(solution)/shard_map/ppermute | solution.py:294
  75.1 2.1 %shard_map.154.a_ref = bf16[64,896]{1,0:T(8,128)(2,1)S(1)} custom-call(s32[5]{0:T(128)S(1)} %stack.23.at_ref, bf16[2,32,1024]{2,1,0:T(8,128)(2,1)S(1)} %collective-permute-done.16.refs_0_, bf16[2,32,1024]{2,1,0:T(8,128)(2,1)S(1)} %collective-permute-done.17.refs_1_, f32[1,1024]{1,0:T(1,128)S(1)} %bitcast.11, bf16[2,1024,384]{2,1,0:T(8,128)(2,1)S(1)} %copy-done.1, ...), custom_call_target="tpu_custom_call" | custom-call | tf_op jit(solution)/shard_map/pallas_call | solution.py:408
  77.1 6.0 %collective-permute-done.27.refs_3_ = bf16[2,32,1024]{2,1,0:T(8,128)(2,1)S(1)} collective-permute-done((bf16[2,32,1024]{2,1,0:T(8,128)(2,1)S(1)}, bf16[2,32,1024]{2,1,0:T(8,128)(2,1)S(1)}, u32[]{:S(2)}, u32[]{:S(2)}) %collective-permute-start.27) | collective-permute-done | bytes 131104 | tf_op jit(solution)/shard_map/ppermute | solution.py:294
  83.1 1.5 %collective-permute-start.21 = (bf16[64,896]{1,0:T(8,128)(2,1)S(1)}, bf16[64,896]{1,0:T(8,128)(2,1)S(1)}, u32[]{:S(2)}, u32[]{:S(2)}) collective-permute-start(bf16[64,896]{1,0:T(8,128)(2,1)S(1)} %shard_map.154.a_ref), channel_id=1, source_target_pairs={{0,2},{1,3},{2,0},{3,1},{4,6},{5,7},{6,4},{7,5},{8,10},{9,11},{10,... | collective-permute-start | bytes 344072 | tf_op jit(solution)/shard_map/ppermute | solution.py:294
  84.6 2.3 %shard_map.157.a_ref = bf16[128,896]{1,0:T(8,128)(2,1)S(1)} custom-call(s32[5]{0:T(128)S(1)} %stack.23.at_ref, bf16[2,32,1024]{2,1,0:T(8,128)(2,1)S(1)} %get-tuple-element.52.refs_0_, bf16[2,32,1024]{2,1,0:T(8,128)(2,1)S(1)} %collective-permute-done.25.refs_1_, bf16[2,32,1024]{2,1,0:T(8,128)(2,1)S(1)} %collective-permute-done.26.refs_2_, ...), custom_call_target="tpu_custom_call" | custom-call | tf_op jit(solution)/shard_map/pallas_call | solution.py:408
  87.7 1.6 %collective-permute-start.14 = (bf16[128,896]{1,0:T(8,128)(2,1)S(1)}, bf16[128,896]{1,0:T(8,128)(2,1)S(1)}, u32[]{:S(2)}, u32[]{:S(2)}) collective-permute-start(bf16[128,896]{1,0:T(8,128)(2,1)S(1)} %shard_map.150.a_ref), channel_id=1, source_target_pairs={{0,2},{1,3},{2,0},{3,1},{4,6},{5,7},{6,4},{7,5},{8,10},{9,11},{10,... | collective-permute-start | bytes 688136 | tf_op jit(solution)/shard_map/ppermute | solution.py:294
  89.3 1.1 shard_map.155
  90.6 2.1 %shard_map.160.a_ref = bf16[64,896]{1,0:T(8,128)(2,1)S(1)} custom-call(s32[5]{0:T(128)S(1)} %stack.23.at_ref, bf16[2,32,1024]{2,1,0:T(8,128)(2,1)S(1)} %collective-permute-done.32.refs_0_, bf16[2,32,1024]{2,1,0:T(8,128)(2,1)S(1)} %collective-permute-done.33.refs_1_, f32[1,1024]{1,0:T(1,128)S(1)} %bitcast.13, bf16[2,1024,384]{2,1,0:T(8,128)(2,1)S(1)} %copy-done.1, ...), custom_call_target="tpu_custom_call" | custom-call | tf_op jit(solution)/shard_map/pallas_call | solution.py:408
  92.7 1.1 collective-permute-start.34
  93.8 4.1 %collective-permute-done.34.b_ref = bf16[64,896]{1,0:T(8,128)(2,1)S(1)} collective-permute-done((bf16[64,896]{1,0:T(8,128)(2,1)S(1)}, bf16[64,896]{1,0:T(8,128)(2,1)S(1)}, u32[]{:S(2)}, u32[]{:S(2)}) %collective-permute-start.34) | collective-permute-done | bytes 114720 | tf_op jit(solution)/shard_map/ppermute | solution.py:294
  97.9 1.1 shard_map.161
  99.0 1.1 shard_map.158
  100.2 4.0 %collective-permute-start.29 = (bf16[2,32,1024]{2,1,0:T(8,128)(2,1)S(1)}, bf16[2,32,1024]{2,1,0:T(8,128)(2,1)S(1)}, u32[]{:S(2)}, u32[]{:S(2)}) collective-permute-start(bf16[2,32,1024]{2,1,0:T(8,128)(2,1)S(1)} %get-tuple-element.57), channel_id=1, source_target_pairs={{0,4},{4,0},{8,12},{12,8},{16,20},{20,16},{24,28},{28,24},{1,5},{5... | collective-permute-start | bytes 393224 | tf_op jit(solution)/shard_map/ppermute | solution.py:294
  104.1 1.5 %collective-permute-start.31 = (bf16[2,32,1024]{2,1,0:T(8,128)(2,1)S(1)}, bf16[2,32,1024]{2,1,0:T(8,128)(2,1)S(1)}, u32[]{:S(2)}, u32[]{:S(2)}) collective-permute-start(bf16[2,32,1024]{2,1,0:T(8,128)(2,1)S(1)} %get-tuple-element.59), channel_id=1, source_target_pairs={{0,12},{4,8},{8,4},{12,0},{16,28},{20,24},{24,20},{28,16},{1,13},{... | collective-permute-start | bytes 393224 | tf_op jit(solution)/shard_map/ppermute | solution.py:294
  105.7 1.7 %collective-permute-start.35 = (bf16[2,32,1024]{2,1,0:T(8,128)(2,1)S(1)}, bf16[2,32,1024]{2,1,0:T(8,128)(2,1)S(1)}, u32[]{:S(2)}, u32[]{:S(2)}) collective-permute-start(bf16[2,32,1024]{2,1,0:T(8,128)(2,1)S(1)} %get-tuple-element.63), channel_id=1, source_target_pairs={{0,24},{4,28},{8,16},{12,20},{16,8},{20,12},{24,0},{28,4},{1,25},{... | collective-permute-start | bytes 393224 | tf_op jit(solution)/shard_map/ppermute | solution.py:294
  107.4 3.5 %collective-permute-start.36 = (bf16[2,32,1024]{2,1,0:T(8,128)(2,1)S(1)}, bf16[2,32,1024]{2,1,0:T(8,128)(2,1)S(1)}, u32[]{:S(2)}, u32[]{:S(2)}) collective-permute-start(bf16[2,32,1024]{2,1,0:T(8,128)(2,1)S(1)} %get-tuple-element.64), channel_id=1, source_target_pairs={{0,28},{4,24},{8,20},{12,16},{16,12},{20,8},{24,4},{28,0},{1,29},{... | collective-permute-start | bytes 393224 | tf_op jit(solution)/shard_map/ppermute | solution.py:294
  112.7 2.7 %collective-permute-done.36.refs_1_ = bf16[2,32,1024]{2,1,0:T(8,128)(2,1)S(1)} collective-permute-done((bf16[2,32,1024]{2,1,0:T(8,128)(2,1)S(1)}, bf16[2,32,1024]{2,1,0:T(8,128)(2,1)S(1)}, u32[]{:S(2)}, u32[]{:S(2)}) %collective-permute-start.36) | collective-permute-done | bytes 131104 | tf_op jit(solution)/shard_map/ppermute | solution.py:294
  115.7 1.9 %collective-permute-done.37.b_ref = f32[128,1024]{1,0:T(8,128)S(1)} collective-permute-done((f32[128,1024]{1,0:T(8,128)S(1)}, f32[128,1024]{1,0:T(8,128)S(1)}, u32[]{:S(2)}, u32[]{:S(2)}) %collective-permute-start.37) | collective-permute-done | bytes 524320 | tf_op jit(solution)/shard_map/ppermute | solution.py:294
  (70 shorter events, 11.0 us)
Async XLA Ops:
  0.0 71.4 %collective-permute-start.19 = (bf16[2,1024,384]{2,1,0:T(8,128)(2,1)}, bf16[2,1024,384]{2,1,0:T(8,128)(2,1)S(1)}, u32[]{:S(2)}, u32[]{:S(2)}) collective-permute-start(bf16[2,1024,384]{2,1,0:T(8,128)(2,1)} %refs_3_.3), channel_id=1, source_target_pairs={{0,1},{1,0},{2,3},{3,2},{4,5},{5,4},{6,7},{7,6},{8,9},{9,8},{10,11... | collective-permute-start | bytes 4718600 | tf_op jit(solution)/shard_map/ppermute | solution.py:294
  0.5 72.5 %collective-permute-start.20 = (bf16[2,1024,384]{2,1,0:T(8,128)(2,1)}, bf16[2,1024,384]{2,1,0:T(8,128)(2,1)}, u32[]{:S(2)}, u32[]{:S(2)}) collective-permute-start(bf16[2,1024,384]{2,1,0:T(8,128)(2,1)} %refs_4_.3), channel_id=1, source_target_pairs={{0,1},{1,0},{2,3},{3,2},{4,5},{5,4},{6,7},{7,6},{8,9},{9,8},{10,11... | collective-permute-start | bytes 4718600 | tf_op jit(solution)/shard_map/ppermute | solution.py:294
  0.5 87.2 %collective-permute-start.22 = (bf16[2,384,1024]{2,1,0:T(8,128)(2,1)}, bf16[2,384,1024]{2,1,0:T(8,128)(2,1)S(1)}, u32[]{:S(2)}, u32[]{:S(2)}) collective-permute-start(bf16[2,384,1024]{2,1,0:T(8,128)(2,1)} %own_ref.5), channel_id=1, source_target_pairs={{0,1},{1,0},{2,3},{3,2},{4,5},{5,4},{6,7},{7,6},{8,9},{9,8},{10,11... | collective-permute-start | bytes 4718600 | tf_op jit(solution)/shard_map/ppermute | solution.py:294
  3.4 6.2 %collective-permute-start.1 = (bf16[400,128]{1,0:T(8,128)(2,1)S(1)}, bf16[400,128]{1,0:T(8,128)(2,1)S(1)}, u32[]{:S(2)}, u32[]{:S(2)}) collective-permute-start(bf16[400,128]{1,0:T(8,128)(2,1)S(1)} %get-tuple-element.37), channel_id=1, source_target_pairs={{0,8},{4,12},{8,0},{12,4},{16,24},{20,28},{24,16},{28,20},{1,9},{5... | collective-permute-start | bytes 307208 | tf_op jit(solution)/shard_map/ppermute | solution.py:294
  6.0 8.4 %collective-permute-start.3 = (bf16[400,128]{1,0:T(8,128)(2,1)S(1)}, bf16[400,128]{1,0:T(8,128)(2,1)S(1)}, u32[]{:S(2)}, u32[]{:S(2)}) collective-permute-start(bf16[400,128]{1,0:T(8,128)(2,1)S(1)} %get-tuple-element.38), channel_id=1, source_target_pairs={{0,16},{4,20},{8,24},{12,28},{16,0},{20,4},{24,8},{28,12},{1,17},{... | collective-permute-start | bytes 307208 | tf_op jit(solution)/shard_map/ppermute | solution.py:294
  9.6 7.6 %collective-permute-start.5 = (bf16[400,128]{1,0:T(8,128)(2,1)S(1)}, bf16[400,128]{1,0:T(8,128)(2,1)S(1)}, u32[]{:S(2)}, u32[]{:S(2)}) collective-permute-start(bf16[400,128]{1,0:T(8,128)(2,1)S(1)} %get-tuple-element.39), channel_id=1, source_target_pairs={{0,24},{4,28},{8,16},{12,20},{16,8},{20,12},{24,0},{28,4},{1,25},{... | collective-permute-start | bytes 307208 | tf_op jit(solution)/shard_map/ppermute | solution.py:294
  14.4 32.2 %copy-start.6 = (bf16[128,1024]{1,0:T(8,128)(2,1)S(1)}, bf16[128,1024]{1,0:T(8,128)(2,1)}, u32[]{:S(2)}) copy-start(bf16[128,1024]{1,0:T(8,128)(2,1)} %refs_5_.2) | copy-start | bytes 786436
  14.4 4.9 %collective-permute-start = (bf16[400,128]{1,0:T(8,128)(2,1)S(1)}, bf16[400,128]{1,0:T(8,128)(2,1)S(1)}, u32[]{:S(2)}, u32[]{:S(2)}) collective-permute-start(bf16[400,128]{1,0:T(8,128)(2,1)S(1)} %get-tuple-element.36.refs_0_), channel_id=1, source_target_pairs={{0,4},{4,0},{8,12},{12,8},{16,20},{20,16},{24,28},{28,24},{1,5},{5... | collective-permute-start | bytes 307208 | tf_op jit(solution)/shard_map/ppermute | solution.py:294
  17.2 5.2 %collective-permute-start.2 = (bf16[400,128]{1,0:T(8,128)(2,1)S(1)}, bf16[400,128]{1,0:T(8,128)(2,1)S(1)}, u32[]{:S(2)}, u32[]{:S(2)}) collective-permute-start(bf16[400,128]{1,0:T(8,128)(2,1)S(1)} %collective-permute-done.1.refs_2_), channel_id=1, source_target_pairs={{0,4},{4,0},{8,12},{12,8},{16,20},{20,16},{24,28},{28,24},{1,5},{5... | collective-permute-start | bytes 307208 | tf_op jit(solution)/shard_map/ppermute | solution.py:294
  19.3 5.5 %collective-permute-start.4 = (bf16[400,128]{1,0:T(8,128)(2,1)S(1)}, bf16[400,128]{1,0:T(8,128)(2,1)S(1)}, u32[]{:S(2)}, u32[]{:S(2)}) collective-permute-start(bf16[400,128]{1,0:T(8,128)(2,1)S(1)} %collective-permute-done.3.refs_4_), channel_id=1, source_target_pairs={{0,4},{4,0},{8,12},{12,8},{16,20},{20,16},{24,28},{28,24},{1,5},{5... | collective-permute-start | bytes 307208 | tf_op jit(solution)/shard_map/ppermute | solution.py:294
  22.3 4.7 %collective-permute-start.6 = (bf16[400,128]{1,0:T(8,128)(2,1)S(1)}, bf16[400,128]{1,0:T(8,128)(2,1)S(1)}, u32[]{:S(2)}, u32[]{:S(2)}) collective-permute-start(bf16[400,128]{1,0:T(8,128)(2,1)S(1)} %collective-permute-done.5.refs_6_), channel_id=1, source_target_pairs={{0,4},{4,0},{8,12},{12,8},{16,20},{20,16},{24,28},{28,24},{1,5},{5... | collective-permute-start | bytes 307208 | tf_op jit(solution)/shard_map/ppermute | solution.py:294
  30.0 4.3 %collective-permute-start.7 = (bf16[128,128]{1,0:T(8,128)(2,1)S(1)}, bf16[128,128]{1,0:T(8,128)(2,1)S(1)}, u32[]{:S(2)}, u32[]{:S(2)}) collective-permute-start(bf16[128,128]{1,0:T(8,128)(2,1)S(1)} %get-tuple-element.41), channel_id=1, source_target_pairs={{0,8},{4,12},{8,0},{12,4},{16,24},{20,28},{24,16},{28,20},{1,9},{5... | collective-permute-start | bytes 98312 | tf_op jit(solution)/shard_map/ppermute | solution.py:294
  32.4 4.8 %collective-permute-start.8 = (bf16[128,128]{1,0:T(8,128)(2,1)S(1)}, bf16[128,128]{1,0:T(8,128)(2,1)S(1)}, u32[]{:S(2)}, u32[]{:S(2)}) collective-permute-start(bf16[128,128]{1,0:T(8,128)(2,1)S(1)} %get-tuple-element.42), channel_id=1, source_target_pairs={{0,16},{4,20},{8,24},{12,28},{16,0},{20,4},{24,8},{28,12},{1,17},{... | collective-permute-start | bytes 98312 | tf_op jit(solution)/shard_map/ppermute | solution.py:294
  34.3 5.8 %collective-permute-start.9 = (bf16[128,128]{1,0:T(8,128)(2,1)S(1)}, bf16[128,128]{1,0:T(8,128)(2,1)S(1)}, u32[]{:S(2)}, u32[]{:S(2)}) collective-permute-start(bf16[128,128]{1,0:T(8,128)(2,1)S(1)} %get-tuple-element.43), channel_id=1, source_target_pairs={{0,24},{4,28},{8,16},{12,20},{16,8},{20,12},{24,0},{28,4},{1,25},{... | collective-permute-start | bytes 98312 | tf_op jit(solution)/shard_map/ppermute | solution.py:294
  40.2 5.0 %collective-permute-start.10 = (bf16[4,128,128]{2,1,0:T(8,128)(2,1)S(1)}, bf16[4,128,128]{2,1,0:T(8,128)(2,1)S(1)}, u32[]{:S(2)}, u32[]{:S(2)}) collective-permute-start(bf16[4,128,128]{2,1,0:T(8,128)(2,1)S(1)} %shard_map.147.refs_0_), channel_id=1, source_target_pairs={{0,2},{1,3},{2,0},{3,1},{4,6},{5,7},{6,4},{7,5},{8,10},{9,11},{10,... | collective-permute-start | bytes 393224 | tf_op jit(solution)/shard_map/ppermute | solution.py:294
  41.7 3.5 %collective-permute-start.11 = (bf16[4,128,128]{2,1,0:T(8,128)(2,1)S(1)}, bf16[4,128,128]{2,1,0:T(8,128)(2,1)S(1)}, u32[]{:S(2)}, u32[]{:S(2)}) collective-permute-start(bf16[4,128,128]{2,1,0:T(8,128)(2,1)S(1)} %shard_map.147.refs_0_), channel_id=1, source_target_pairs={{0,1},{1,0},{2,3},{3,2},{4,5},{5,4},{6,7},{7,6},{8,9},{9,8},{10,11... | collective-permute-start | bytes 393224 | tf_op jit(solution)/shard_map/ppermute | solution.py:294
  45.2 1.3 %collective-permute-start.12 = (bf16[4,128,128]{2,1,0:T(8,128)(2,1)S(1)}, bf16[4,128,128]{2,1,0:T(8,128)(2,1)S(1)}, u32[]{:S(2)}, u32[]{:S(2)}) collective-permute-start(bf16[4,128,128]{2,1,0:T(8,128)(2,1)S(1)} %collective-permute-done.10.refs_1_), channel_id=1, source_target_pairs={{0,1},{1,0},{2,3},{3,2},{4,5},{5,4},{6,7},{7,6},{8,9},{9,8},{10,11... | collective-permute-start | bytes 393224 | tf_op jit(solution)/shard_map/ppermute | solution.py:294
  46.5 3.1 %copy-start.8 = (s32[128,2]{0,1:T(2,128)S(1)}, s32[128,2]{0,1:T(2,128)}, u32[]{:S(2)}) copy-start(s32[128,2]{0,1:T(2,128)} %param.22) | copy-start | bytes 3076
  46.5 5.8 %copy-start.7 = (f32[1024]{0:T(1024)S(1)}, f32[1024]{0:T(1024)}, u32[]{:S(2)}) copy-start(f32[1024]{0:T(1024)} %param.21) | copy-start | bytes 12292
  46.6 13.9 %copy-start.4 = (bf16[1024,384]{1,0:T(8,128)(2,1)S(1)}, bf16[1024,384]{1,0:T(8,128)(2,1)}, u32[]{:S(2)}) copy-start(bf16[1024,384]{1,0:T(8,128)(2,1)} %gate_ref.1) | copy-start | bytes 2359300
  46.6 13.9 %copy-start.5 = (bf16[1024,384]{1,0:T(8,128)(2,1)S(1)}, bf16[1024,384]{1,0:T(8,128)(2,1)}, u32[]{:S(2)}) copy-start(bf16[1024,384]{1,0:T(8,128)(2,1)} %up_ref.1) | copy-start | bytes 2359300
  46.6 28.5 %copy-start.2 = (bf16[2,1024,384]{2,1,0:T(8,128)(2,1)S(1)}, bf16[2,1024,384]{2,1,0:T(8,128)(2,1)}, u32[]{:S(2)}) copy-start(bf16[2,1024,384]{2,1,0:T(8,128)(2,1)} %refs_4_.3) | copy-start | bytes 4718596
  48.0 27.1 %copy-start.1 = (bf16[2,1024,384]{2,1,0:T(8,128)(2,1)S(1)}, bf16[2,1024,384]{2,1,0:T(8,128)(2,1)}, u32[]{:S(2)}) copy-start(bf16[2,1024,384]{2,1,0:T(8,128)(2,1)} %refs_3_.3) | copy-start | bytes 4718596
  48.0 1.6 %collective-permute-start.15 = (bf16[128,1024]{1,0:T(8,128)(2,1)S(1)}, bf16[128,1024]{1,0:T(8,128)(2,1)S(1)}, u32[]{:S(2)}, u32[]{:S(2)}) collective-permute-start(bf16[128,1024]{1,0:T(8,128)(2,1)S(1)} %shard_map.148.mixed_ref.own_ref), channel_id=1, source_target_pairs={{0,1},{1,0},{2,3},{3,2},{4,5},{5,4},{6,7},{7,6},{8,9},{9,8},{10,11... | collective-permute-start | bytes 786440 | tf_op jit(solution)/shard_map/ppermute | solution.py:294
  50.7 5.6 %collective-permute-start.25 = (bf16[2,32,1024]{2,1,0:T(8,128)(2,1)S(1)}, bf16[2,32,1024]{2,1,0:T(8,128)(2,1)S(1)}, u32[]{:S(2)}, u32[]{:S(2)}) collective-permute-start(bf16[2,32,1024]{2,1,0:T(8,128)(2,1)S(1)} %get-tuple-element.53), channel_id=1, source_target_pairs={{0,4},{4,0},{8,12},{12,8},{16,20},{20,16},{24,28},{28,24},{1,5},{5... | collective-permute-start | bytes 393224 | tf_op jit(solution)/shard_map/ppermute | solution.py:294
  52.3 1.2 collective-permute-start.18
  53.5 5.6 %collective-permute-start.26 = (bf16[2,32,1024]{2,1,0:T(8,128)(2,1)S(1)}, bf16[2,32,1024]{2,1,0:T(8,128)(2,1)S(1)}, u32[]{:S(2)}, u32[]{:S(2)}) collective-permute-start(bf16[2,32,1024]{2,1,0:T(8,128)(2,1)S(1)} %get-tuple-element.54), channel_id=1, source_target_pairs={{0,8},{4,12},{8,0},{12,4},{16,24},{20,28},{24,16},{28,20},{1,9},{5... | collective-permute-start | bytes 393224 | tf_op jit(solution)/shard_map/ppermute | solution.py:294
  56.3 12.2 %collective-permute-start.16 = (bf16[2,32,1024]{2,1,0:T(8,128)(2,1)S(1)}, bf16[2,32,1024]{2,1,0:T(8,128)(2,1)S(1)}, u32[]{:S(2)}, u32[]{:S(2)}) collective-permute-start(bf16[2,32,1024]{2,1,0:T(8,128)(2,1)S(1)} %get-tuple-element.47), channel_id=1, source_target_pairs={{0,16},{4,20},{8,24},{12,28},{16,0},{20,4},{24,8},{28,12},{1,17},{... | collective-permute-start | bytes 393224 | tf_op jit(solution)/shard_map/ppermute | solution.py:294
  59.1 12.3 %collective-permute-start.17 = (bf16[2,32,1024]{2,1,0:T(8,128)(2,1)S(1)}, bf16[2,32,1024]{2,1,0:T(8,128)(2,1)S(1)}, u32[]{:S(2)}, u32[]{:S(2)}) collective-permute-start(bf16[2,32,1024]{2,1,0:T(8,128)(2,1)S(1)} %get-tuple-element.48), channel_id=1, source_target_pairs={{0,20},{4,16},{8,28},{12,24},{16,4},{20,0},{24,12},{28,8},{1,21},{... | collective-permute-start | bytes 393224 | tf_op jit(solution)/shard_map/ppermute | solution.py:294
  68.5 18.4 %collective-permute-start.13 = (bf16[128,896]{1,0:T(8,128)(2,1)S(1)}, bf16[128,896]{1,0:T(8,128)(2,1)S(1)}, u32[]{:S(2)}, u32[]{:S(2)}) collective-permute-start(bf16[128,896]{1,0:T(8,128)(2,1)S(1)} %shard_map.149.a_ref), channel_id=1, source_target_pairs={{0,1},{1,0},{2,3},{3,2},{4,5},{5,4},{6,7},{7,6},{8,9},{9,8},{10,11... | collective-permute-start | bytes 688136 | tf_op jit(solution)/shard_map/ppermute | solution.py:294
  71.3 11.8 %collective-permute-start.27 = (bf16[2,32,1024]{2,1,0:T(8,128)(2,1)S(1)}, bf16[2,32,1024]{2,1,0:T(8,128)(2,1)S(1)}, u32[]{:S(2)}, u32[]{:S(2)}) collective-permute-start(bf16[2,32,1024]{2,1,0:T(8,128)(2,1)S(1)} %get-tuple-element.55), channel_id=1, source_target_pairs={{0,12},{4,8},{8,4},{12,0},{16,28},{20,24},{24,20},{28,16},{1,13},{... | collective-permute-start | bytes 393224 | tf_op jit(solution)/shard_map/ppermute | solution.py:294
  71.4 19.1 %collective-permute-start.32 = (bf16[2,32,1024]{2,1,0:T(8,128)(2,1)S(1)}, bf16[2,32,1024]{2,1,0:T(8,128)(2,1)S(1)}, u32[]{:S(2)}, u32[]{:S(2)}) collective-permute-start(bf16[2,32,1024]{2,1,0:T(8,128)(2,1)S(1)} %get-tuple-element.61), channel_id=1, source_target_pairs={{0,24},{4,28},{8,16},{12,20},{16,8},{20,12},{24,0},{28,4},{1,25},{... | collective-permute-start | bytes 393224 | tf_op jit(solution)/shard_map/ppermute | solution.py:294
  73.0 17.5 %collective-permute-start.33 = (bf16[2,32,1024]{2,1,0:T(8,128)(2,1)S(1)}, bf16[2,32,1024]{2,1,0:T(8,128)(2,1)S(1)}, u32[]{:S(2)}, u32[]{:S(2)}) collective-permute-start(bf16[2,32,1024]{2,1,0:T(8,128)(2,1)S(1)} %get-tuple-element.62), channel_id=1, source_target_pairs={{0,28},{4,24},{8,20},{12,16},{16,12},{20,8},{24,4},{28,0},{1,29},{... | collective-permute-start | bytes 393224 | tf_op jit(solution)/shard_map/ppermute | solution.py:294
  83.1 6.2 %collective-permute-start.21 = (bf16[64,896]{1,0:T(8,128)(2,1)S(1)}, bf16[64,896]{1,0:T(8,128)(2,1)S(1)}, u32[]{:S(2)}, u32[]{:S(2)}) collective-permute-start(bf16[64,896]{1,0:T(8,128)(2,1)S(1)} %shard_map.154.a_ref), channel_id=1, source_target_pairs={{0,2},{1,3},{2,0},{3,1},{4,6},{5,7},{6,4},{7,5},{8,10},{9,11},{10,... | collective-permute-start | bytes 344072 | tf_op jit(solution)/shard_map/ppermute | solution.py:294
  84.6 4.7 %copy-start = (bf16[2,384,1024]{2,1,0:T(8,128)(2,1)S(1)}, bf16[2,384,1024]{2,1,0:T(8,128)(2,1)}, u32[]{:S(2)}) copy-start(bf16[2,384,1024]{2,1,0:T(8,128)(2,1)} %own_ref.5) | copy-start | bytes 4718596
  86.9 12.1 %collective-permute-start.28 = (bf16[128,896]{1,0:T(8,128)(2,1)S(1)}, bf16[128,896]{1,0:T(8,128)(2,1)S(1)}, u32[]{:S(2)}, u32[]{:S(2)}) collective-permute-start(bf16[128,896]{1,0:T(8,128)(2,1)S(1)} %shard_map.157.a_ref), channel_id=1, source_target_pairs={{0,2},{1,3},{2,0},{3,1},{4,6},{5,7},{6,4},{7,5},{8,10},{9,11},{10,... | collective-permute-start | bytes 688136 | tf_op jit(solution)/shard_map/ppermute | solution.py:294
  87.7 16.4 %collective-permute-start.14 = (bf16[128,896]{1,0:T(8,128)(2,1)S(1)}, bf16[128,896]{1,0:T(8,128)(2,1)S(1)}, u32[]{:S(2)}, u32[]{:S(2)}) collective-permute-start(bf16[128,896]{1,0:T(8,128)(2,1)S(1)} %shard_map.150.a_ref), channel_id=1, source_target_pairs={{0,2},{1,3},{2,0},{3,1},{4,6},{5,7},{6,4},{7,5},{8,10},{9,11},{10,... | collective-permute-start | bytes 688136 | tf_op jit(solution)/shard_map/ppermute | solution.py:294
  90.4 15.3 %collective-permute-start.23 = (bf16[2,32,1024]{2,1,0:T(8,128)(2,1)S(1)}, bf16[2,32,1024]{2,1,0:T(8,128)(2,1)S(1)}, u32[]{:S(2)}, u32[]{:S(2)}) collective-permute-start(bf16[2,32,1024]{2,1,0:T(8,128)(2,1)S(1)} %get-tuple-element.49), channel_id=1, source_target_pairs={{0,16},{4,20},{8,24},{12,28},{16,0},{20,4},{24,8},{28,12},{1,17},{... | collective-permute-start | bytes 393224 | tf_op jit(solution)/shard_map/ppermute | solution.py:294
  90.5 16.9 %collective-permute-start.24 = (bf16[2,32,1024]{2,1,0:T(8,128)(2,1)S(1)}, bf16[2,32,1024]{2,1,0:T(8,128)(2,1)S(1)}, u32[]{:S(2)}, u32[]{:S(2)}) collective-permute-start(bf16[2,32,1024]{2,1,0:T(8,128)(2,1)S(1)} %get-tuple-element.50), channel_id=1, source_target_pairs={{0,20},{4,16},{8,28},{12,24},{16,4},{20,0},{24,12},{28,8},{1,21},{... | collective-permute-start | bytes 393224 | tf_op jit(solution)/shard_map/ppermute | solution.py:294
  92.7 5.3 %collective-permute-start.34 = (bf16[64,896]{1,0:T(8,128)(2,1)S(1)}, bf16[64,896]{1,0:T(8,128)(2,1)S(1)}, u32[]{:S(2)}, u32[]{:S(2)}) collective-permute-start(bf16[64,896]{1,0:T(8,128)(2,1)S(1)} %shard_map.160.a_ref), channel_id=1, source_target_pairs={{0,2},{1,3},{2,0},{3,1},{4,6},{5,7},{6,4},{7,5},{8,10},{9,11},{10,... | collective-permute-start | bytes 344072 | tf_op jit(solution)/shard_map/ppermute | solution.py:294
  99.0 12.1 %copy-start.3 = (bf16[384,1024]{1,0:T(8,128)(2,1)S(1)}, bf16[384,1024]{1,0:T(8,128)(2,1)}, u32[]{:S(2)}) copy-start(bf16[384,1024]{1,0:T(8,128)(2,1)} %down_ref.1) | copy-start | bytes 2359300
  99.0 12.1 %copy-start.10 = (f32[128,2]{0,1:T(2,128)S(1)}, f32[128,2]{0,1:T(2,128)}, u32[]{:S(2)}) copy-start(f32[128,2]{0,1:T(2,128)} %param.23) | copy-start | bytes 3076
  100.2 12.1 %collective-permute-start.29 = (bf16[2,32,1024]{2,1,0:T(8,128)(2,1)S(1)}, bf16[2,32,1024]{2,1,0:T(8,128)(2,1)S(1)}, u32[]{:S(2)}, u32[]{:S(2)}) collective-permute-start(bf16[2,32,1024]{2,1,0:T(8,128)(2,1)S(1)} %get-tuple-element.57), channel_id=1, source_target_pairs={{0,4},{4,0},{8,12},{12,8},{16,20},{20,16},{24,28},{28,24},{1,5},{5... | collective-permute-start | bytes 393224 | tf_op jit(solution)/shard_map/ppermute | solution.py:294
  104.1 8.2 %collective-permute-start.30 = (bf16[2,32,1024]{2,1,0:T(8,128)(2,1)S(1)}, bf16[2,32,1024]{2,1,0:T(8,128)(2,1)S(1)}, u32[]{:S(2)}, u32[]{:S(2)}) collective-permute-start(bf16[2,32,1024]{2,1,0:T(8,128)(2,1)S(1)} %get-tuple-element.58), channel_id=1, source_target_pairs={{0,8},{4,12},{8,0},{12,4},{16,24},{20,28},{24,16},{28,20},{1,9},{5... | collective-permute-start | bytes 393224 | tf_op jit(solution)/shard_map/ppermute | solution.py:294
  104.1 8.2 %collective-permute-start.31 = (bf16[2,32,1024]{2,1,0:T(8,128)(2,1)S(1)}, bf16[2,32,1024]{2,1,0:T(8,128)(2,1)S(1)}, u32[]{:S(2)}, u32[]{:S(2)}) collective-permute-start(bf16[2,32,1024]{2,1,0:T(8,128)(2,1)S(1)} %get-tuple-element.59), channel_id=1, source_target_pairs={{0,12},{4,8},{8,4},{12,0},{16,28},{20,24},{24,20},{28,16},{1,13},{... | collective-permute-start | bytes 393224 | tf_op jit(solution)/shard_map/ppermute | solution.py:294
  105.7 7.0 %collective-permute-start.35 = (bf16[2,32,1024]{2,1,0:T(8,128)(2,1)S(1)}, bf16[2,32,1024]{2,1,0:T(8,128)(2,1)S(1)}, u32[]{:S(2)}, u32[]{:S(2)}) collective-permute-start(bf16[2,32,1024]{2,1,0:T(8,128)(2,1)S(1)} %get-tuple-element.63), channel_id=1, source_target_pairs={{0,24},{4,28},{8,16},{12,20},{16,8},{20,12},{24,0},{28,4},{1,25},{... | collective-permute-start | bytes 393224 | tf_op jit(solution)/shard_map/ppermute | solution.py:294
  107.4 8.0 %collective-permute-start.36 = (bf16[2,32,1024]{2,1,0:T(8,128)(2,1)S(1)}, bf16[2,32,1024]{2,1,0:T(8,128)(2,1)S(1)}, u32[]{:S(2)}, u32[]{:S(2)}) collective-permute-start(bf16[2,32,1024]{2,1,0:T(8,128)(2,1)S(1)} %get-tuple-element.64), channel_id=1, source_target_pairs={{0,28},{4,24},{8,20},{12,16},{16,12},{20,8},{24,4},{28,0},{1,29},{... | collective-permute-start | bytes 393224 | tf_op jit(solution)/shard_map/ppermute | solution.py:294
  115.6 2.0 %collective-permute-start.37 = (f32[128,1024]{1,0:T(8,128)S(1)}, f32[128,1024]{1,0:T(8,128)S(1)}, u32[]{:S(2)}, u32[]{:S(2)}) collective-permute-start(f32[128,1024]{1,0:T(8,128)S(1)} %get-tuple-element.66), channel_id=1, source_target_pairs={{0,1},{1,0},{2,3},{3,2},{4,5},{5,4},{6,7},{7,6},{8,9},{9,8},{10,11... | collective-permute-start | bytes 1572872 | tf_op jit(solution)/shard_map/ppermute | solution.py:294
  (1 other events, 0.7 us)

commit v3 on v2

--- a/solution.py
+++ b/solution.py
@@ -58,21 +58,27 @@
 
 
 def pack_kernel(at_ref, q_ref, k_ref, v_ref, b_ref, *refs, hd):
-    outs, sems = refs[:-1], refs[-1]
+    heads = (len(refs) - 2) // 2
+    outs, queries, bias_ref, sems = refs[:heads], refs[heads:-2], refs[-2], refs[-1]
     tok = k_ref.shape[0]
+    fetch = pltpu.make_async_copy(b_ref, bias_ref, sems.at[3 * heads])
+    fetch.start()
     copies = []
     for mh, out in enumerate(outs):
         head = jnp.bitwise_xor(at_ref[0], mh)
         cols = pl.ds(pl.multiple_of(head * hd, hd), hd)
-        for i, (src, start) in enumerate(
-            ((k_ref, 0), (v_ref, tok), (q_ref, 2 * tok + BIAS_ROWS))
+        for i, (src, target) in enumerate(
+            (
+                (k_ref, out.at[pl.ds(0, tok)]),
+                (v_ref, out.at[pl.ds(tok, tok)]),
+                (q_ref, queries[mh]),
+            )
         ):
-            copy = pltpu.make_async_copy(
-                src.at[:, cols], out.at[pl.ds(start, tok)], sems.at[3 * mh + i]
-            )
+            copy = pltpu.make_async_copy(src.at[:, cols], target, sems.at[3 * mh + i])
             copy.start()
             copies.append(copy)
-    bias = b_ref[...].astype(F32)
+    fetch.wait()
+    bias = bias_ref[...].astype(F32)
     for mh, out in enumerate(outs):
         head = jnp.bitwise_xor(at_ref[0], mh)
         row = jnp.where(iota(bias.shape, 0) == head, bias, 0.0)
@@ -82,54 +88,76 @@
         copy.wait()
 
 
-def attention_kernel(at_ref, w_hbm, *refs, heads, group):
+def lay_kernel(at_ref, *refs):
+    for i, (ref, out) in enumerate(zip(refs[:4], refs[4:5] * 2 + refs[5:6] * 2)):
+        value = ref[at_ref[4]] if i < 2 else ref[...]
+        width = value.shape[1]
+        out[:, i % 2 * width : (i % 2 + 1) * width] = value
+
+
+def attention_kernel(at_ref, *refs, heads, group):
     blocks = heads * group
-    ins, outs = refs[:blocks], refs[blocks : blocks + heads]
-    w_ref, kv_ref, q_ref, acc_ref, carry_ref, sem = refs[blocks + heads :]
-    fetch = pltpu.make_async_copy(w_hbm, w_ref, sem)
-    fetch.start()
-    rows, hd = ins[0].shape
-    kv_rows = kv_ref.shape[1]
-    tok = rows - kv_rows
+    weights, refs = refs[:5], refs[5:]
+    ins, q_ins, outs = refs[:blocks], refs[blocks : blocks + heads], refs[blocks + heads : -8]
+    w_ref, laid_ref, shared_ref, kv_ref, q_ref, acc_ref, carry_ref, sems = refs[-8:]
+    e = at_ref[4]
+    moves = [(weights[0], w_ref)]
+    for i, src in enumerate((weights[1].at[e], weights[2].at[e], *weights[3:])):
+        cols = pl.ds(i % 2 * src.shape[1], src.shape[1])
+        moves.append((src, (laid_ref if i < 2 else shared_ref).at[:, cols]))
+    fetches = [pltpu.make_async_copy(a, b, sems.at[i]) for i, (a, b) in enumerate(moves)]
+    for fetch in fetches:
+        fetch.start()
+    tok, hd = q_ins[0].shape
     h, p = at_ref[0], at_ref[1]
     for mh in range(heads):
         g = jnp.bitwise_xor(h, mh)
-        q_ref[pl.ds(pl.multiple_of(g * tok, tok), tok)] = ins[mh * group][kv_rows:]
+        q_ref[pl.ds(pl.multiple_of(g * tok, tok), tok)] = q_ins[mh][...]
         for mp in range(group):
-            kv_ref[g * group + jnp.bitwise_xor(p, mp)] = ins[mh * group + mp][:kv_rows]
+            kv_ref[g * group + jnp.bitwise_xor(p, mp)] = ins[mh * group + mp][...]
     acc_ref[...] = jnp.zeros_like(acc_ref)
     carry_ref[...] = jnp.zeros_like(carry_ref)
-    src = iota((2 * tok, 2 * tok), 0)
-    src = jnp.where(src >= tok, src - tok, src)
-    dst = iota((2 * tok, 2 * tok), 1)
-    tri = jnp.where((dst >= tok) | (src > dst), 1.0, 0.0).astype(BF)
+    span = 2 if group % 2 == 0 else 1
+    keys_all = span * tok
+    tri = jnp.where(
+        iota((keys_all, keys_all), 0) > iota((keys_all, keys_all), 1), 1.0, 0.0
+    ).astype(BF)
     scale = hd ** (-0.5)
-    for j in reversed(range(blocks)):
+
+    def pair(j, start, stop, axis=0):
+        return jnp.concatenate([kv_ref[j + i, start:stop] for i in range(span)], axis=axis)
+
+    for j in reversed(range(0, blocks, span)):
         r0 = (j // group) * tok
         n = heads * tok - r0
-        keys = kv_ref[j, 0:tok]
-        values = kv_ref[j, tok : 2 * tok]
-        bias = kv_ref[j, 2 * tok : 2 * tok + BIAS_ROWS].astype(F32)[0:1, :]
+        keys, values = pair(j, 0, tok), pair(j, tok, 2 * tok)
+        bias = pair(j, 2 * tok, 2 * tok + BIAS_ROWS, 1).astype(F32)[0:1, :]
         raw = lax.dot_general(
             q_ref[r0:], keys, (((1,), (1,)), ((), ())), preferred_element_type=F32
         )
         logits = raw * scale + bias
         soft = jnp.log(1.0 + jnp.exp(-jnp.abs(logits)))
-        fail = -(jnp.maximum(logits, 0.0) + soft)
-        row = iota((n, tok), 0)
-        before = (row >= tok) | (iota((n, tok), 1) < row + (p - j % group) * tok)
-        stay = logits + fail
-        fail = jnp.where(before, fail, 0.0)
-        high, low = split_pair(fail)
-        sums = dot(jnp.concatenate([high, low], axis=1), tri)
+        stay = jnp.minimum(logits, 0.0) - soft
+        loss = jnp.maximum(logits, 0.0) + soft
+        before = iota((tok, keys_all), 1) < iota((tok, keys_all), 0) + (p - j % group) * tok
+
+        def masked(x):
+            first = jnp.where(before, x[:tok], 0.0)
+            return jnp.concatenate([first, x[tok:]], axis=0) if n > tok else first
+
+        loss = masked(loss)
+        sums = dot(jnp.concatenate(split_pair(loss), axis=0), tri)
+        sums = sums[:n] + sums[n:]
         carry = carry_ref[r0:]
-        weights = jnp.where(before, jnp.exp(stay + sums[:, :tok] + carry), 0.0)
-        carry_ref[r0:] = carry + sums[:, tok:]
+        later = sums + jnp.concatenate([carry] * span, axis=1)
+        weights = masked(jnp.exp(stay - later))
+        carry_ref[r0:] = carry + (sums[:, 0:1] + loss[:, 0:1])
         acc_ref[r0:] += dot(weights.astype(BF), values)
     for mh in range(heads):
         g = jnp.bitwise_xor(h, mh)
         outs[mh][...] = acc_ref[pl.ds(pl.multiple_of(g * tok, tok), tok)].astype(BF)
-    fetch.wait()
+    for fetch in fetches:
+        fetch.wait()
 
 
 def stack_kernel(*refs):
@@ -189,33 +217,29 @@
     return tail.astype(BF)
 
 
-def partials(sides):
-    gate_sum, up_sum, square = 0.0, 0.0, 0.0
-    for x, gain, gate, up in sides:
-        scaled = (x * gain).astype(BF)
+def weighted(xs, gain_refs, w_refs):
+    total, square = 0.0, 0.0
+    for x, gain_ref, w_ref in zip(xs, gain_refs, w_refs):
         square = square + jnp.sum(x * x, axis=1, keepdims=True)
-        gate_sum = gate_sum + dot(scaled, gate).astype(BF).astype(F32)
-        up_sum = up_sum + dot(scaled, up).astype(BF).astype(F32)
-    return jnp.concatenate(
-        [gate_sum.astype(BF), up_sum.astype(BF), square_lanes(square)], axis=1
-    )
-
-
-def shared_kernel(mixed_ref, gain_ref, gate_ref, up_ref, out_ref):
-    out_ref[...] = partials(
-        [(mixed_ref[...].astype(F32), gain_ref[...], gate_ref[...], up_ref[...])]
-    )
-
-
-def routed_kernel(at_ref, *refs):
-    e = at_ref[4]
-    weights, out_ref = refs[-7:-1], refs[-1]
-    sides = []
-    for side in range(2):
-        x = jnp.concatenate([ref[side].astype(F32) for ref in refs[:-7]], axis=0)
-        gain_ref, gate_ref, up_ref = weights[3 * side : 3 * side + 3]
-        sides.append((x, gain_ref[...], gate_ref[e], up_ref[e]))
-    out_ref[...] = partials(sides)
+        scaled = (x * gain_ref[...]).astype(BF)
+        total = total + dot(scaled, w_ref[...]).astype(BF).astype(F32)
+    return jnp.concatenate([total.astype(BF), square_lanes(square)], axis=1)
+
+
+def shared_kernel(at_ref, own_ref, other_ref, *refs):
+    out_ref = refs[-1]
+    count = out_ref.shape[0]
+    part = pl.ds(pl.multiple_of(at_ref[4] * count, count), count)
+    xs = [ref[part].astype(F32) for ref in (own_ref, other_ref)]
+    out_ref[...] = weighted(xs, refs[:2], refs[2:4])
+
+
+def routed_kernel(*refs):
+    xs = [
+        jnp.concatenate([ref[side].astype(F32) for ref in refs[4:-1]], axis=0)
+        for side in range(2)
+    ]
+    refs[-1][...] = weighted(xs, refs[:2], refs[2:4])
 
 
 def add_partials(a_ref, b_ref, width):
@@ -253,7 +277,9 @@
             out[side] = rows[i * cap : (i + 1) * cap]
 
 
-def base_kernel(at_ref, ids_ref, rw_ref, mixed_ref, hid_ref, down_ref, base_ref, *picks, local, cap):
+def base_kernel(
+    at_ref, ids_ref, rw_ref, mixed_ref, mine_ref, theirs_ref, down_ref, base_ref, *picks, local, cap
+):
     blocks = sum(pick.shape[1] for pick in picks) // (2 * cap)
     named, rank = slots_of(ids_ref, at_ref[3], at_ref[4], local, blocks)
     weight = functools.reduce(
@@ -267,7 +293,11 @@
         pick[:, :width] = high[:, start : start + width]
         pick[:, width:] = low[:, start : start + width]
         start += width
-    base_ref[0] = mixed_ref[...].astype(F32) + dot(hid_ref[...], down_ref[...])
+    first = at_ref[4] == 0
+    mine, theirs = mine_ref[...].astype(F32), theirs_ref[...].astype(F32)
+    hid = [jnp.where(first, mine, theirs), jnp.where(first, theirs, mine)]
+    hid = jnp.concatenate(hid, axis=0).astype(BF)
+    base_ref[0] = mixed_ref[...].astype(F32) + dot(hid, down_ref[...])
     base_ref[1] = jnp.zeros_like(base_ref[1])
 
 
@@ -327,29 +357,42 @@
         return jax.ShapeDtypeStruct(shape, BF)
 
     at = jnp.stack([h_index, p_index, t_index, s_index, t_index % 2])
-    rows = 3 * tok + BIAS_ROWS
+    kv_rows = 2 * tok + BIAS_ROWS
     gain = norm_gain.reshape(1, feats)
-    others = [swap(x, "tp", 1) for x in (gain, gate_proj, up_proj, down_proj)]
+    others = [
+        swap(x, "tp", 1)
+        for x in (gain, gate_proj, up_proj, shared_gate, shared_up, down_proj)
+    ]
     packed = call(
         functools.partial(pack_kernel, hd=hd),
-        (array(rows, hd),) * heads,
-        [smem()] + [hbm()] * 3 + [vmem()],
-        [pltpu.SemaphoreType.DMA((3 * heads,))],
-    )(at, in_hbm(queries), in_hbm(key_rows), in_hbm(value_rows), break_bias.T)
-    qkv = [swap(packed[mh], "sp", mh * group) for mh in range(heads)]
-    qkv = [swap(qkv[mh], "sp", mp) for mh in range(heads) for mp in range(group)]
-    *attended, out_w = call(
+        (array(kv_rows, hd),) * heads + (array(tok, hd),) * heads,
+        [smem()] + [hbm()] * 4,
+        [pltpu.VMEM((heads, tok), BF), pltpu.SemaphoreType.DMA((3 * heads + 1,))],
+    )(at, *[in_hbm(x) for x in (queries, key_rows, value_rows, break_bias.T)])
+    kv = [swap(packed[mh], "sp", mh * group) for mh in range(heads)]
+    kv = [swap(kv[mh], "sp", mp) for mh in range(heads) for mp in range(group)]
+    q = [swap(packed[heads + mh], "sp", mh * group) for mh in range(heads)]
+    hid_s = shared_gate.shape[1]
+    width = 2 * gate_proj.shape[2]
+    wide = (array(feats, width), array(feats, 2 * hid_s))
+    laid_other, shared_other = call(lay_kernel, wide, [smem()] + [vmem()] * 4)(at, *others[1:5])
+    *attended, out_w, laid_own, shared_own = call(
         functools.partial(attention_kernel, heads=heads, group=group),
-        (array(tok, hd),) * heads + (array(*out_proj.shape),),
-        [smem(), hbm()] + [vmem()] * blocks,
+        (array(tok, hd),) * heads + (array(*out_proj.shape),) + wide,
+        [smem()] + [hbm()] * 5 + [vmem()] * (blocks + heads),
         [
-            pltpu.VMEM((blocks, rows - tok, hd), BF),
+            pltpu.VMEM((blocks, kv_rows, hd), BF),
             pltpu.VMEM((heads * tok, hd), BF),
             pltpu.VMEM((heads * tok, hd), F32),
             pltpu.VMEM((heads * tok, tok), F32),
-            pltpu.SemaphoreType.DMA,
+            pltpu.SemaphoreType.DMA((5,)),
         ],
-    )(at, in_hbm(out_proj), *qkv)
+    )(
+        at,
+        *[in_hbm(x) for x in (out_proj, gate_proj, up_proj, shared_gate, shared_up)],
+        *kv,
+        *q,
+    )
     piece = call(stack_kernel, array(heads, tok, hd), [vmem()] * heads)(
         *[swap(attended[mh], "sp", mh * group) for mh in range(heads)]
     )
@@ -381,10 +424,9 @@
     groups = [range(half), range(half, quarter), range(quarter, blocks)]
     arrived = {m: swap(sends[m], "sp", m) for m in range(blocks)}
 
-    hid_s = shared_gate.shape[1]
     shared_sum = call(
-        shared_kernel, array(tok, 2 * hid_s + LANES), [vmem()] * 4
-    )(mixed, gain, shared_gate, shared_up)
+        shared_kernel, array(tok // 2, 2 * hid_s + LANES), [smem()] + [vmem()] * 6
+    )(at, mixed, mixed_other, gain, others[0], shared_own, shared_other)
 
     def add(a, b, width):
         return call(functools.partial(add_kernel, width=width), array(*a.shape), [vmem()] * 2)(a, b)
@@ -396,18 +438,18 @@
             [vmem()] * 2,
         )(a, b)
 
-    for bit in bits[:-1]:
-        shared_sum = add(shared_sum, swap(shared_sum, "tp", bit), 2 * hid_s)
+    for bit in bits[1:-1]:
+        other = swap(shared_sum, "tp", bit)
+        shared_sum = add(shared_sum, other, 2 * hid_s)
     other = swap(shared_sum, "tp", bits[-1])
     shared_hidden = hidden(shared_sum, other, 2 * hid_s)
-
-    width = 2 * gate_proj.shape[2]
-    weights = [gain, gate_proj, up_proj] + others[:3]
+    other_hidden = swap(shared_hidden, "tp", 1)
+
     back = {}
     for ms in groups:
         total = call(
-            routed_kernel, array(len(ms) * cap, width + LANES), [smem()] + [vmem()] * (len(ms) + 6)
-        )(at, *[arrived[m] for m in ms], *weights)
+            routed_kernel, array(len(ms) * cap, width + LANES), [vmem()] * (len(ms) + 4)
+        )(gain, others[0], laid_own, laid_other, *[arrived[m] for m in ms])
         for bit in bits[1:-1]:
             total = add(total, swap(total, "tp", bit), width)
         came = swap(total, "tp", bits[-1])
@@ -415,15 +457,15 @@
             functools.partial(down_kernel, width=width, features=features),
             (array(2, cap, feats),) * len(ms),
             [smem()] + [vmem()] * 4,
-        )(at, total, came, down_proj, others[3])
+        )(at, total, came, down_proj, others[5])
         for m, out in zip(ms, outs):
             back[m] = swap(out, "sp", m)
     total, *picks = call(
         functools.partial(base_kernel, local=local, cap=cap),
         (jax.ShapeDtypeStruct((2, tok, feats), F32),)
         + tuple(array(tok, 2 * len(ms) * cap) for ms in groups),
-        [smem()] + [vmem()] * 5,
-    )(at, expert_ids.T, route_weights.T, mixed, shared_hidden, shared_down)
+        [smem()] + [vmem()] * 6,
+    )(at, expert_ids.T, route_weights.T, mixed, shared_hidden, other_hidden, shared_down)
     for i in (1, 0, 2):
         ms, last = groups[i], i == 2
         one = jax.ShapeDtypeStruct((tok, feats), F32)

time: 119 us -> 113 us (0.950)
  waiting for transfers between devices: 47.6 us -> 41.9 us
  starting transfers between devices: 49.5 us -> 52.3 us
  Pallas kernels: 20.1 us -> 18.2 us
    ppermute x38 -> x43, waiting for transfers between devices: 47.6 us -> 41.9 us  [swap(): return lax.ppermute(x, axis, [(i, i ^ bit) for i in range(count)])]
    pallas_call x6, Pallas kernels: 8.66 us -> 5.63 us  [the longest x3 2 us: layer(): call(routed_kernel, array(len(ms) * cap, width + LANES), [vmem()] * (len(...]
    ppermute x38 -> x43, starting transfers between devices: 49.5 us -> 52.3 us  [swap(): return lax.ppermute(x, axis, [(i, i ^ bit) for i in range(count)])]
  transfers between devices with their start and end apart: 38 -> 43, of which waited for: 21 -> 19; matrix products, arithmetic and copies ran while one was open for 0% -> 0% of each run, Pallas kernels for 16% -> 10%
where the time goes in v3:
time: 113 us
  starting transfers between devices  52.3 us (46%)
  waiting for transfers between devices  41.9 us (37%)
  Pallas kernels  18.2 us (16%)
    ppermute x43, starting transfers between devices, swap(): return lax.ppermute(x, axis, [(i, i ^ bit) for i in range(count)])  52.3 us
    ppermute x43, waiting for transfers between devices, swap(): return lax.ppermute(x, axis, [(i, i ^ bit) for i in range(count)])  41.9 us
    pallas_call x1, Pallas kernels, layer(): call(functools.partial(attention_kernel, heads=heads, group=group), (arra...  4.04 us
    pallas_call x3, Pallas kernels, layer(): call(functools.partial(down_kernel, width=width, features=features), (arr...  3.28 us
  transfers between devices with their start and end apart: 43, of which 19 were waited for; matrix products, arithmetic and copies ran while one was open for 0% of the time, Pallas kernels for 10%

profile of v3, /device:TPU:0, one launch (start us, length us, event | category | flops | bytes accessed | tf_op | source)
XLA Modules:
  0.0 112.8 jit_solution(12513525090164519548)
XLA Ops:
  0.1 1.6 %shard_map.145 = (bf16[272,128]{1,0:T(8,128)(2,1)S(1)}, bf16[272,128]{1,0:T(8,128)(2,1)S(1)}, bf16[272,128]{1,0:T(8,128)(2,1)S(1)}, bf16[272,128]{1,0:T(8,128)(2...) custom-call(s32[5]{0:T(128)S(1)} %stack.23.at_ref, ...), custom_call_target="tpu_custom_call" | custom-call | tf_op jit(solution)/shard_map/pallas_call | solution.py:366
  1.7 3.1 %collective-permute-start.1 = (bf16[272,128]{1,0:T(8,128)(2,1)S(1)}, bf16[272,128]{1,0:T(8,128)(2,1)S(1)}, u32[]{:S(2)}, u32[]{:S(2)}) collective-permute-start(bf16[272,128]{1,0:T(8,128)(2,1)S(1)} %get-tuple-element.45), channel_id=1, source_target_pairs={{0,8},{4,12},{8,0},{12,4},{16,24},{20,28},{24,16},{28,20},{1,9},{5... | collective-permute-start | bytes 208904 | tf_op jit(solution)/shard_map/ppermute | solution.py:324
  4.8 2.6 %collective-permute-start.3 = (bf16[272,128]{1,0:T(8,128)(2,1)S(1)}, bf16[272,128]{1,0:T(8,128)(2,1)S(1)}, u32[]{:S(2)}, u32[]{:S(2)}) collective-permute-start(bf16[272,128]{1,0:T(8,128)(2,1)S(1)} %get-tuple-element.46), channel_id=1, source_target_pairs={{0,16},{4,20},{8,24},{12,28},{16,0},{20,4},{24,8},{28,12},{1,17},{... | collective-permute-start | bytes 208904 | tf_op jit(solution)/shard_map/ppermute | solution.py:324
  7.4 0.9 collective-permute-start.7
  8.3 1.5 %collective-permute-start = (bf16[272,128]{1,0:T(8,128)(2,1)S(1)}, bf16[272,128]{1,0:T(8,128)(2,1)S(1)}, u32[]{:S(2)}, u32[]{:S(2)}) collective-permute-start(bf16[272,128]{1,0:T(8,128)(2,1)S(1)} %get-tuple-element.44.refs_5_), channel_id=1, source_target_pairs={{0,4},{4,0},{8,12},{12,8},{16,20},{20,16},{24,28},{28,24},{1,5},{5... | collective-permute-start | bytes 208904 | tf_op jit(solution)/shard_map/ppermute | solution.py:324
  10.3 2.0 %collective-permute-done.3.refs_9_ = bf16[272,128]{1,0:T(8,128)(2,1)S(1)} collective-permute-done((bf16[272,128]{1,0:T(8,128)(2,1)S(1)}, bf16[272,128]{1,0:T(8,128)(2,1)S(1)}, u32[]{:S(2)}, u32[]{:S(2)}) %collective-permute-start.3) | collective-permute-done | bytes 69664 | tf_op jit(solution)/shard_map/ppermute | solution.py:324
  12.3 1.5 %collective-permute-start.4 = (bf16[272,128]{1,0:T(8,128)(2,1)S(1)}, bf16[272,128]{1,0:T(8,128)(2,1)S(1)}, u32[]{:S(2)}, u32[]{:S(2)}) collective-permute-start(bf16[272,128]{1,0:T(8,128)(2,1)S(1)} %collective-permute-done.3.refs_9_), channel_id=1, source_target_pairs={{0,4},{4,0},{8,12},{12,8},{16,20},{20,16},{24,28},{28,24},{1,5},{5... | collective-permute-start | bytes 208904 | tf_op jit(solution)/shard_map/ppermute | solution.py:324
  13.8 1.3 %collective-permute-start.6 = (bf16[272,128]{1,0:T(8,128)(2,1)S(1)}, bf16[272,128]{1,0:T(8,128)(2,1)S(1)}, u32[]{:S(2)}, u32[]{:S(2)}) collective-permute-start(bf16[272,128]{1,0:T(8,128)(2,1)S(1)} %collective-permute-done.5.refs_11_), channel_id=1, source_target_pairs={{0,4},{4,0},{8,12},{12,8},{16,20},{20,16},{24,28},{28,24},{1,5},{5... | collective-permute-start | bytes 208904 | tf_op jit(solution)/shard_map/ppermute | solution.py:324
  15.1 1.8 %collective-permute-start.8 = (bf16[128,128]{1,0:T(8,128)(2,1)S(1)}, bf16[128,128]{1,0:T(8,128)(2,1)S(1)}, u32[]{:S(2)}, u32[]{:S(2)}) collective-permute-start(bf16[128,128]{1,0:T(8,128)(2,1)S(1)} %get-tuple-element.50), channel_id=1, source_target_pairs={{0,16},{4,20},{8,24},{12,28},{16,0},{20,4},{24,8},{28,12},{1,17},{... | collective-permute-start | bytes 98312 | tf_op jit(solution)/shard_map/ppermute | solution.py:324
  16.9 3.4 %collective-permute-done.8.refs_15_ = bf16[128,128]{1,0:T(8,128)(2,1)S(1)} collective-permute-done((bf16[128,128]{1,0:T(8,128)(2,1)S(1)}, bf16[128,128]{1,0:T(8,128)(2,1)S(1)}, u32[]{:S(2)}, u32[]{:S(2)}) %collective-permute-start.8) | collective-permute-done | bytes 32800 | tf_op jit(solution)/shard_map/ppermute | solution.py:324
  20.3 3.2 %collective-permute-start.9 = (bf16[128,128]{1,0:T(8,128)(2,1)S(1)}, bf16[128,128]{1,0:T(8,128)(2,1)S(1)}, u32[]{:S(2)}, u32[]{:S(2)}) collective-permute-start(bf16[128,128]{1,0:T(8,128)(2,1)S(1)} %get-tuple-element.51), channel_id=1, source_target_pairs={{0,24},{4,28},{8,16},{12,20},{16,8},{20,12},{24,0},{28,4},{1,25},{... | collective-permute-start | bytes 98312 | tf_op jit(solution)/shard_map/ppermute | solution.py:324
  23.5 2.5 %collective-permute-done.9.refs_16_ = bf16[128,128]{1,0:T(8,128)(2,1)S(1)} collective-permute-done((bf16[128,128]{1,0:T(8,128)(2,1)S(1)}, bf16[128,128]{1,0:T(8,128)(2,1)S(1)}, u32[]{:S(2)}, u32[]{:S(2)}) %collective-permute-start.9) | collective-permute-done | bytes 32800 | tf_op jit(solution)/shard_map/ppermute | solution.py:324
  26.1 4.0 %shard_map.146 = (bf16[128,128]{1,0:T(8,128)(2,1)S(1)}, bf16[128,128]{1,0:T(8,128)(2,1)S(1)}, bf16[128,128]{1,0:T(8,128)(2,1)S(1)}, bf16[128,128]{1,0:T(8,128)(2...) custom-call(s32[5]{0:T(128)S(1)} %stack.23.at_ref, ...), custom_call_target="tpu_custom_call" | custom-call | tf_op jit(solution)/shard_map/pallas_call | solution.py:379
  30.2 3.8 %collective-permute-start.11 = (bf16[128,128]{1,0:T(8,128)(2,1)S(1)}, bf16[128,128]{1,0:T(8,128)(2,1)S(1)}, u32[]{:S(2)}, u32[]{:S(2)}) collective-permute-start(bf16[128,128]{1,0:T(8,128)(2,1)S(1)} %get-tuple-element.54), channel_id=1, source_target_pairs={{0,16},{4,20},{8,24},{12,28},{16,0},{20,4},{24,8},{28,12},{1,17},{... | collective-permute-start | bytes 98312 | tf_op jit(solution)/shard_map/ppermute | solution.py:324
  35.9 3.8 %collective-permute-done.12.refs_3_ = bf16[128,128]{1,0:T(8,128)(2,1)S(1)} collective-permute-done((bf16[128,128]{1,0:T(8,128)(2,1)S(1)}, bf16[128,128]{1,0:T(8,128)(2,1)S(1)}, u32[]{:S(2)}, u32[]{:S(2)}) %collective-permute-start.12) | collective-permute-done | bytes 32800 | tf_op jit(solution)/shard_map/ppermute | solution.py:324
  39.7 1.6 %collective-permute-start.13 = (bf16[4,128,128]{2,1,0:T(8,128)(2,1)S(1)}, bf16[4,128,128]{2,1,0:T(8,128)(2,1)S(1)}, u32[]{:S(2)}, u32[]{:S(2)}) collective-permute-start(bf16[4,128,128]{2,1,0:T(8,128)(2,1)S(1)} %shard_map.147.refs_0_), channel_id=1, source_target_pairs={{0,2},{1,3},{2,0},{3,1},{4,6},{5,7},{6,4},{7,5},{8,10},{9,11},{10,... | collective-permute-start | bytes 393224 | tf_op jit(solution)/shard_map/ppermute | solution.py:324
  41.8 2.9 %collective-permute-done.13.refs_1_ = bf16[4,128,128]{2,1,0:T(8,128)(2,1)S(1)} collective-permute-done((bf16[4,128,128]{2,1,0:T(8,128)(2,1)S(1)}, bf16[4,128,128]{2,1,0:T(8,128)(2,1)S(1)}, u32[]{:S(2)}, u32[]{:S(2)}) %collective-permute-start.13) | collective-permute-done | bytes 131104 | tf_op jit(solution)/shard_map/ppermute | solution.py:324
  44.9 1.2 %collective-permute-done.15.refs_3_ = bf16[4,128,128]{2,1,0:T(8,128)(2,1)S(1)} collective-permute-done((bf16[4,128,128]{2,1,0:T(8,128)(2,1)S(1)}, bf16[4,128,128]{2,1,0:T(8,128)(2,1)S(1)}, u32[]{:S(2)}, u32[]{:S(2)}) %collective-permute-start.15) | collective-permute-done | bytes 131104 | tf_op jit(solution)/shard_map/ppermute | solution.py:324
  46.1 1.4 %shard_map.148.own_ref.mixed_ref = bf16[128,1024]{1,0:T(8,128)(2,1)S(1)} custom-call(s32[5]{0:T(128)S(1)} %stack.23.at_ref, bf16[4,128,128]{2,1,0:T(8,128)(2,1)S(1)} %shard_map.147.refs_0_, bf16[4,128,128]{2,1,0:T(8,128)(2,1)S(1)} %collective-permute-done.13.refs_1_, bf16[4,128,128]{2,1,0:T(8,128)(2,1)S(1)} %collective-permute-done.14.refs_2_, ...), custom_call_target="tpu_custom_call" | custom-call | tf_op jit(solution)/shard_map/pallas_call | solution.py:409
  48.1 1.0 collective-permute-done.17.refs_1_
  49.6 1.1 shard_map.153
  51.4 1.1 collective-permute-done.21.refs_3_
  52.5 1.9 %collective-permute-start.25 = (bf16[2,32,1024]{2,1,0:T(8,128)(2,1)S(1)}, bf16[2,32,1024]{2,1,0:T(8,128)(2,1)S(1)}, u32[]{:S(2)}, u32[]{:S(2)}) collective-permute-start(bf16[2,32,1024]{2,1,0:T(8,128)(2,1)S(1)} %get-tuple-element.64), channel_id=1, source_target_pairs={{0,20},{4,16},{8,28},{12,24},{16,4},{20,0},{24,12},{28,8},{1,21},{... | collective-permute-start | bytes 393224 | tf_op jit(solution)/shard_map/ppermute | solution.py:324
  54.5 7.0 %collective-permute-done.24.refs_4_ = bf16[2,32,1024]{2,1,0:T(8,128)(2,1)S(1)} collective-permute-done((bf16[2,32,1024]{2,1,0:T(8,128)(2,1)S(1)}, bf16[2,32,1024]{2,1,0:T(8,128)(2,1)S(1)}, u32[]{:S(2)}, u32[]{:S(2)}) %collective-permute-start.24) | collective-permute-done | bytes 131104 | tf_op jit(solution)/shard_map/ppermute | solution.py:324
  62.2 2.0 %collective-permute-done.25.refs_5_ = bf16[2,32,1024]{2,1,0:T(8,128)(2,1)S(1)} collective-permute-done((bf16[2,32,1024]{2,1,0:T(8,128)(2,1)S(1)}, bf16[2,32,1024]{2,1,0:T(8,128)(2,1)S(1)}, u32[]{:S(2)}, u32[]{:S(2)}) %collective-permute-start.25) | collective-permute-done | bytes 131104 | tf_op jit(solution)/shard_map/ppermute | solution.py:324
  64.2 2.8 %collective-permute-done.30.refs_5_ = bf16[2,32,1024]{2,1,0:T(8,128)(2,1)S(1)} collective-permute-done((bf16[2,32,1024]{2,1,0:T(8,128)(2,1)S(1)}, bf16[2,32,1024]{2,1,0:T(8,128)(2,1)S(1)}, u32[]{:S(2)}, u32[]{:S(2)}) %collective-permute-start.30) | collective-permute-done | bytes 131104 | tf_op jit(solution)/shard_map/ppermute | solution.py:324
  67.3 2.6 %collective-permute-start.37 = (bf16[2,32,1024]{2,1,0:T(8,128)(2,1)S(1)}, bf16[2,32,1024]{2,1,0:T(8,128)(2,1)S(1)}, u32[]{:S(2)}, u32[]{:S(2)}) collective-permute-start(bf16[2,32,1024]{2,1,0:T(8,128)(2,1)S(1)} %get-tuple-element.77), channel_id=1, source_target_pairs={{0,24},{4,28},{8,16},{12,20},{16,8},{20,12},{24,0},{28,4},{1,25},{... | collective-permute-start | bytes 393224 | tf_op jit(solution)/shard_map/ppermute | solution.py:324
  69.9 1.9 %collective-permute-start.38 = (bf16[2,32,1024]{2,1,0:T(8,128)(2,1)S(1)}, bf16[2,32,1024]{2,1,0:T(8,128)(2,1)S(1)}, u32[]{:S(2)}, u32[]{:S(2)}) collective-permute-start(bf16[2,32,1024]{2,1,0:T(8,128)(2,1)S(1)} %get-tuple-element.78), channel_id=1, source_target_pairs={{0,28},{4,24},{8,20},{12,16},{16,12},{20,8},{24,4},{28,0},{1,29},{... | collective-permute-start | bytes 393224 | tf_op jit(solution)/shard_map/ppermute | solution.py:324
  71.8 0.8 shard_map.149
  73.3 1.6 %collective-permute-start.26 = (bf16[64,896]{1,0:T(8,128)(2,1)S(1)}, bf16[64,896]{1,0:T(8,128)(2,1)S(1)}, u32[]{:S(2)}, u32[]{:S(2)}) collective-permute-start(bf16[64,896]{1,0:T(8,128)(2,1)S(1)} %shard_map.154.a_ref), channel_id=1, source_target_pairs={{0,2},{1,3},{2,0},{3,1},{4,6},{5,7},{6,4},{7,5},{8,10},{9,11},{10,... | collective-permute-start | bytes 344072 | tf_op jit(solution)/shard_map/ppermute | solution.py:324
  75.6 0.8 collective-permute-start.33
  76.3 1.2 %shard_map.150.a_ref = bf16[64,896]{1,0:T(8,128)(2,1)S(1)} custom-call(s32[5]{0:T(128)S(1)} %stack.23.at_ref, bf16[128,1024]{1,0:T(8,128)(2,1)S(1)} %shard_map.148.own_ref.mixed_ref, bf16[128,1024]{1,0:T(8,128)(2,1)S(1)} %collective-permute-done.16.other_ref, f32[1,1024]{1,0:T(1,128)S(1)} %bitcast.12, f32[1,1024]{1,0:T(1,128)S(1)} %collective-permute-done.17.refs_1_, ...), custom_call_target="tpu_custom_call" | custom-call | tf_op jit(solution)/shard_map/pallas_call | solution.py:427
  77.6 1.4 %collective-permute-start.22 = (bf16[64,896]{1,0:T(8,128)(2,1)S(1)}, bf16[64,896]{1,0:T(8,128)(2,1)S(1)}, u32[]{:S(2)}, u32[]{:S(2)}) collective-permute-start(bf16[64,896]{1,0:T(8,128)(2,1)S(1)} %shard_map.150.a_ref), channel_id=1, source_target_pairs={{0,2},{1,3},{2,0},{3,1},{4,6},{5,7},{6,4},{7,5},{8,10},{9,11},{10,... | collective-permute-start | bytes 344072 | tf_op jit(solution)/shard_map/ppermute | solution.py:324
  79.0 1.1 shard_map.155
  80.1 4.4 %collective-permute-start.28 = (bf16[2,32,1024]{2,1,0:T(8,128)(2,1)S(1)}, bf16[2,32,1024]{2,1,0:T(8,128)(2,1)S(1)}, u32[]{:S(2)}, u32[]{:S(2)}) collective-permute-start(bf16[2,32,1024]{2,1,0:T(8,128)(2,1)S(1)} %get-tuple-element.65), channel_id=1, source_target_pairs={{0,16},{4,20},{8,24},{12,28},{16,0},{20,4},{24,8},{28,12},{1,17},{... | collective-permute-start | bytes 393224 | tf_op jit(solution)/shard_map/ppermute | solution.py:324
  84.5 3.6 %collective-permute-start.29 = (bf16[2,32,1024]{2,1,0:T(8,128)(2,1)S(1)}, bf16[2,32,1024]{2,1,0:T(8,128)(2,1)S(1)}, u32[]{:S(2)}, u32[]{:S(2)}) collective-permute-start(bf16[2,32,1024]{2,1,0:T(8,128)(2,1)S(1)} %get-tuple-element.66), channel_id=1, source_target_pairs={{0,20},{4,16},{8,28},{12,24},{16,4},{20,0},{24,12},{28,8},{1,21},{... | collective-permute-start | bytes 393224 | tf_op jit(solution)/shard_map/ppermute | solution.py:324
  88.7 1.6 %collective-permute-start.39 = (bf16[64,896]{1,0:T(8,128)(2,1)S(1)}, bf16[64,896]{1,0:T(8,128)(2,1)S(1)}, u32[]{:S(2)}, u32[]{:S(2)}) collective-permute-start(bf16[64,896]{1,0:T(8,128)(2,1)S(1)} %shard_map.160.a_ref), channel_id=1, source_target_pairs={{0,2},{1,3},{2,0},{3,1},{4,6},{5,7},{6,4},{7,5},{8,10},{9,11},{10,... | collective-permute-start | bytes 344072 | tf_op jit(solution)/shard_map/ppermute | solution.py:324
  90.6 3.0 %collective-permute-done.39.b_ref = bf16[64,896]{1,0:T(8,128)(2,1)S(1)} collective-permute-done((bf16[64,896]{1,0:T(8,128)(2,1)S(1)}, bf16[64,896]{1,0:T(8,128)(2,1)S(1)}, u32[]{:S(2)}, u32[]{:S(2)}) %collective-permute-start.39) | collective-permute-done | bytes 114720 | tf_op jit(solution)/shard_map/ppermute | solution.py:324
  93.6 1.1 shard_map.161
  94.7 1.1 %shard_map.158 = (bf16[2,32,1024]{2,1,0:T(8,128)(2,1)S(1)}, bf16[2,32,1024]{2,1,0:T(8,128)(2,1)S(1)}, bf16[2,32,1024]{2,1,0:T(8,128)(2,1)S(1)}, bf16[2,32,1024]{2,1,0:T(8,128)(2,1)S(1)}) custom-call(s32[5]{0:T(128)S(1)} %stack.23.at_ref, bf16[128,896]{1,0:T(8,128)(2,1)S(1)} %shard_map.157.a_ref, bf16[128,896]{1,0:T(8,128)(2,1)S(1)} %collective-permute-done.33.b_ref, ...), custom_call_target="tpu_custom_call" | custom-call | tf_op jit(solution)/shard_map/pallas_call | solution.py:456
  96.5 2.9 %collective-permute-start.36 = (bf16[2,32,1024]{2,1,0:T(8,128)(2,1)S(1)}, bf16[2,32,1024]{2,1,0:T(8,128)(2,1)S(1)}, u32[]{:S(2)}, u32[]{:S(2)}) collective-permute-start(bf16[2,32,1024]{2,1,0:T(8,128)(2,1)S(1)} %get-tuple-element.75), channel_id=1, source_target_pairs={{0,12},{4,8},{8,4},{12,0},{16,28},{20,24},{24,20},{28,16},{1,13},{... | collective-permute-start | bytes 393224 | tf_op jit(solution)/shard_map/ppermute | solution.py:324
  99.4 2.2 %collective-permute-start.40 = (bf16[2,32,1024]{2,1,0:T(8,128)(2,1)S(1)}, bf16[2,32,1024]{2,1,0:T(8,128)(2,1)S(1)}, u32[]{:S(2)}, u32[]{:S(2)}) collective-permute-start(bf16[2,32,1024]{2,1,0:T(8,128)(2,1)S(1)} %get-tuple-element.79), channel_id=1, source_target_pairs={{0,24},{4,28},{8,16},{12,20},{16,8},{20,12},{24,0},{28,4},{1,25},{... | collective-permute-start | bytes 393224 | tf_op jit(solution)/shard_map/ppermute | solution.py:324
  101.6 1.2 %collective-permute-start.41 = (bf16[2,32,1024]{2,1,0:T(8,128)(2,1)S(1)}, bf16[2,32,1024]{2,1,0:T(8,128)(2,1)S(1)}, u32[]{:S(2)}, u32[]{:S(2)}) collective-permute-start(bf16[2,32,1024]{2,1,0:T(8,128)(2,1)S(1)} %get-tuple-element.80), channel_id=1, source_target_pairs={{0,28},{4,24},{8,20},{12,16},{16,12},{20,8},{24,4},{28,0},{1,29},{... | collective-permute-start | bytes 393224 | tf_op jit(solution)/shard_map/ppermute | solution.py:324
  102.7 0.9 shard_map.152
  104.0 2.0 %collective-permute-done.36.refs_3_ = bf16[2,32,1024]{2,1,0:T(8,128)(2,1)S(1)} collective-permute-done((bf16[2,32,1024]{2,1,0:T(8,128)(2,1)S(1)}, bf16[2,32,1024]{2,1,0:T(8,128)(2,1)S(1)}, u32[]{:S(2)}, u32[]{:S(2)}) %collective-permute-start.36) | collective-permute-done | bytes 131104 | tf_op jit(solution)/shard_map/ppermute | solution.py:324
  106.3 1.2 %collective-permute-done.40.refs_0_ = bf16[2,32,1024]{2,1,0:T(8,128)(2,1)S(1)} collective-permute-done((bf16[2,32,1024]{2,1,0:T(8,128)(2,1)S(1)}, bf16[2,32,1024]{2,1,0:T(8,128)(2,1)S(1)}, u32[]{:S(2)}, u32[]{:S(2)}) %collective-permute-start.40) | collective-permute-done | bytes 131104 | tf_op jit(solution)/shard_map/ppermute | solution.py:324
  107.5 2.2 %collective-permute-done.41.refs_1_ = bf16[2,32,1024]{2,1,0:T(8,128)(2,1)S(1)} collective-permute-done((bf16[2,32,1024]{2,1,0:T(8,128)(2,1)S(1)}, bf16[2,32,1024]{2,1,0:T(8,128)(2,1)S(1)}, u32[]{:S(2)}, u32[]{:S(2)}) %collective-permute-start.41) | collective-permute-done | bytes 131104 | tf_op jit(solution)/shard_map/ppermute | solution.py:324
  110.2 1.9 %collective-permute-done.42.b_ref = f32[128,1024]{1,0:T(8,128)S(1)} collective-permute-done((f32[128,1024]{1,0:T(8,128)S(1)}, f32[128,1024]{1,0:T(8,128)S(1)}, u32[]{:S(2)}, u32[]{:S(2)}) %collective-permute-start.42) | collective-permute-done | bytes 524320 | tf_op jit(solution)/shard_map/ppermute | solution.py:324
  (78 shorter events, 10.8 us)
Async XLA Ops:
  1.7 8.1 %collective-permute-start.1 = (bf16[272,128]{1,0:T(8,128)(2,1)S(1)}, bf16[272,128]{1,0:T(8,128)(2,1)S(1)}, u32[]{:S(2)}, u32[]{:S(2)}) collective-permute-start(bf16[272,128]{1,0:T(8,128)(2,1)S(1)} %get-tuple-element.45), channel_id=1, source_target_pairs={{0,8},{4,12},{8,0},{12,4},{16,24},{20,28},{24,16},{28,20},{1,9},{5... | collective-permute-start | bytes 208904 | tf_op jit(solution)/shard_map/ppermute | solution.py:324
  4.8 7.5 %collective-permute-start.3 = (bf16[272,128]{1,0:T(8,128)(2,1)S(1)}, bf16[272,128]{1,0:T(8,128)(2,1)S(1)}, u32[]{:S(2)}, u32[]{:S(2)}) collective-permute-start(bf16[272,128]{1,0:T(8,128)(2,1)S(1)} %get-tuple-element.46), channel_id=1, source_target_pairs={{0,16},{4,20},{8,24},{12,28},{16,0},{20,4},{24,8},{28,12},{1,17},{... | collective-permute-start | bytes 208904 | tf_op jit(solution)/shard_map/ppermute | solution.py:324
  7.4 6.4 %collective-permute-start.5 = (bf16[272,128]{1,0:T(8,128)(2,1)S(1)}, bf16[272,128]{1,0:T(8,128)(2,1)S(1)}, u32[]{:S(2)}, u32[]{:S(2)}) collective-permute-start(bf16[272,128]{1,0:T(8,128)(2,1)S(1)} %get-tuple-element.47), channel_id=1, source_target_pairs={{0,24},{4,28},{8,16},{12,20},{16,8},{20,12},{24,0},{28,4},{1,25},{... | collective-permute-start | bytes 208904 | tf_op jit(solution)/shard_map/ppermute | solution.py:324
  7.4 7.7 %collective-permute-start.7 = (bf16[128,128]{1,0:T(8,128)(2,1)S(1)}, bf16[128,128]{1,0:T(8,128)(2,1)S(1)}, u32[]{:S(2)}, u32[]{:S(2)}) collective-permute-start(bf16[128,128]{1,0:T(8,128)(2,1)S(1)} %get-tuple-element.49), channel_id=1, source_target_pairs={{0,8},{4,12},{8,0},{12,4},{16,24},{20,28},{24,16},{28,20},{1,9},{5... | collective-permute-start | bytes 98312 | tf_op jit(solution)/shard_map/ppermute | solution.py:324
  8.3 17.7 %collective-permute-start = (bf16[272,128]{1,0:T(8,128)(2,1)S(1)}, bf16[272,128]{1,0:T(8,128)(2,1)S(1)}, u32[]{:S(2)}, u32[]{:S(2)}) collective-permute-start(bf16[272,128]{1,0:T(8,128)(2,1)S(1)} %get-tuple-element.44.refs_5_), channel_id=1, source_target_pairs={{0,4},{4,0},{8,12},{12,8},{16,20},{20,16},{24,28},{28,24},{1,5},{5... | collective-permute-start | bytes 208904 | tf_op jit(solution)/shard_map/ppermute | solution.py:324
  9.8 16.2 %collective-permute-start.2 = (bf16[272,128]{1,0:T(8,128)(2,1)S(1)}, bf16[272,128]{1,0:T(8,128)(2,1)S(1)}, u32[]{:S(2)}, u32[]{:S(2)}) collective-permute-start(bf16[272,128]{1,0:T(8,128)(2,1)S(1)} %collective-permute-done.1.refs_7_), channel_id=1, source_target_pairs={{0,4},{4,0},{8,12},{12,8},{16,20},{20,16},{24,28},{28,24},{1,5},{5... | collective-permute-start | bytes 208904 | tf_op jit(solution)/shard_map/ppermute | solution.py:324
  12.3 13.7 %collective-permute-start.4 = (bf16[272,128]{1,0:T(8,128)(2,1)S(1)}, bf16[272,128]{1,0:T(8,128)(2,1)S(1)}, u32[]{:S(2)}, u32[]{:S(2)}) collective-permute-start(bf16[272,128]{1,0:T(8,128)(2,1)S(1)} %collective-permute-done.3.refs_9_), channel_id=1, source_target_pairs={{0,4},{4,0},{8,12},{12,8},{16,20},{20,16},{24,28},{28,24},{1,5},{5... | collective-permute-start | bytes 208904 | tf_op jit(solution)/shard_map/ppermute | solution.py:324
  13.8 12.2 %collective-permute-start.6 = (bf16[272,128]{1,0:T(8,128)(2,1)S(1)}, bf16[272,128]{1,0:T(8,128)(2,1)S(1)}, u32[]{:S(2)}, u32[]{:S(2)}) collective-permute-start(bf16[272,128]{1,0:T(8,128)(2,1)S(1)} %collective-permute-done.5.refs_11_), channel_id=1, source_target_pairs={{0,4},{4,0},{8,12},{12,8},{16,20},{20,16},{24,28},{28,24},{1,5},{5... | collective-permute-start | bytes 208904 | tf_op jit(solution)/shard_map/ppermute | solution.py:324
  15.1 5.2 %collective-permute-start.8 = (bf16[128,128]{1,0:T(8,128)(2,1)S(1)}, bf16[128,128]{1,0:T(8,128)(2,1)S(1)}, u32[]{:S(2)}, u32[]{:S(2)}) collective-permute-start(bf16[128,128]{1,0:T(8,128)(2,1)S(1)} %get-tuple-element.50), channel_id=1, source_target_pairs={{0,16},{4,20},{8,24},{12,28},{16,0},{20,4},{24,8},{28,12},{1,17},{... | collective-permute-start | bytes 98312 | tf_op jit(solution)/shard_map/ppermute | solution.py:324
  20.3 5.7 %collective-permute-start.9 = (bf16[128,128]{1,0:T(8,128)(2,1)S(1)}, bf16[128,128]{1,0:T(8,128)(2,1)S(1)}, u32[]{:S(2)}, u32[]{:S(2)}) collective-permute-start(bf16[128,128]{1,0:T(8,128)(2,1)S(1)} %get-tuple-element.51), channel_id=1, source_target_pairs={{0,24},{4,28},{8,16},{12,20},{16,8},{20,12},{24,0},{28,4},{1,25},{... | collective-permute-start | bytes 98312 | tf_op jit(solution)/shard_map/ppermute | solution.py:324
  26.0 8.6 %copy-start.6 = (bf16[2,1024,384]{2,1,0:T(8,128)(2,1)S(1)}, bf16[2,1024,384]{2,1,0:T(8,128)(2,1)}, u32[]{:S(2)}) copy-start(bf16[2,1024,384]{2,1,0:T(8,128)(2,1)} %refs_1_.1) | copy-start | bytes 4718596
  26.1 8.5 %copy-start.7 = (bf16[2,1024,384]{2,1,0:T(8,128)(2,1)S(1)}, bf16[2,1024,384]{2,1,0:T(8,128)(2,1)}, u32[]{:S(2)}) copy-start(bf16[2,1024,384]{2,1,0:T(8,128)(2,1)} %refs_2_.1) | copy-start | bytes 4718596
  26.1 15.2 %copy-start = (bf16[2,384,1024]{2,1,0:T(8,128)(2,1)S(1)}, bf16[2,384,1024]{2,1,0:T(8,128)(2,1)}, u32[]{:S(2)}) copy-start(bf16[2,384,1024]{2,1,0:T(8,128)(2,1)} %own_ref.5) | copy-start | bytes 4718596
  26.1 20.0 %copy-start.2 = (bf16[128,1024]{1,0:T(8,128)(2,1)S(1)}, bf16[128,1024]{1,0:T(8,128)(2,1)}, u32[]{:S(2)}) copy-start(bf16[128,1024]{1,0:T(8,128)(2,1)} %refs_5_.1) | copy-start | bytes 786436
  30.1 5.0 %collective-permute-start.10 = (bf16[128,128]{1,0:T(8,128)(2,1)S(1)}, bf16[128,128]{1,0:T(8,128)(2,1)S(1)}, u32[]{:S(2)}, u32[]{:S(2)}) collective-permute-start(bf16[128,128]{1,0:T(8,128)(2,1)S(1)} %get-tuple-element.53), channel_id=1, source_target_pairs={{0,8},{4,12},{8,0},{12,4},{16,24},{20,28},{24,16},{28,20},{1,9},{5... | collective-permute-start | bytes 98312 | tf_op jit(solution)/shard_map/ppermute | solution.py:324
  30.2 5.6 %collective-permute-start.11 = (bf16[128,128]{1,0:T(8,128)(2,1)S(1)}, bf16[128,128]{1,0:T(8,128)(2,1)S(1)}, u32[]{:S(2)}, u32[]{:S(2)}) collective-permute-start(bf16[128,128]{1,0:T(8,128)(2,1)S(1)} %get-tuple-element.54), channel_id=1, source_target_pairs={{0,16},{4,20},{8,24},{12,28},{16,0},{20,4},{24,8},{28,12},{1,17},{... | collective-permute-start | bytes 98312 | tf_op jit(solution)/shard_map/ppermute | solution.py:324
  34.0 5.7 %collective-permute-start.12 = (bf16[128,128]{1,0:T(8,128)(2,1)S(1)}, bf16[128,128]{1,0:T(8,128)(2,1)S(1)}, u32[]{:S(2)}, u32[]{:S(2)}) collective-permute-start(bf16[128,128]{1,0:T(8,128)(2,1)S(1)} %get-tuple-element.55), channel_id=1, source_target_pairs={{0,24},{4,28},{8,16},{12,20},{16,8},{20,12},{24,0},{28,4},{1,25},{... | collective-permute-start | bytes 98312 | tf_op jit(solution)/shard_map/ppermute | solution.py:324
  34.6 32.7 %collective-permute-start.18 = (bf16[2,1024,384]{2,1,0:T(8,128)(2,1)S(1)}, bf16[2,1024,384]{2,1,0:T(8,128)(2,1)S(1)}, u32[]{:S(2)}, u32[]{:S(2)}) collective-permute-start(bf16[2,1024,384]{2,1,0:T(8,128)(2,1)S(1)} %copy-done.6), channel_id=1, source_target_pairs={{0,1},{1,0},{2,3},{3,2},{4,5},{5,4},{6,7},{7,6},{8,9},{9,8},{10,11... | collective-permute-start | bytes 4718600 | tf_op jit(solution)/shard_map/ppermute | solution.py:324
  34.6 35.3 %collective-permute-start.19 = (bf16[2,1024,384]{2,1,0:T(8,128)(2,1)S(1)}, bf16[2,1024,384]{2,1,0:T(8,128)(2,1)S(1)}, u32[]{:S(2)}, u32[]{:S(2)}) collective-permute-start(bf16[2,1024,384]{2,1,0:T(8,128)(2,1)S(1)} %copy-done.7), channel_id=1, source_target_pairs={{0,1},{1,0},{2,3},{3,2},{4,5},{5,4},{6,7},{7,6},{8,9},{9,8},{10,11... | collective-permute-start | bytes 4718600 | tf_op jit(solution)/shard_map/ppermute | solution.py:324
  39.7 5.0 %collective-permute-start.13 = (bf16[4,128,128]{2,1,0:T(8,128)(2,1)S(1)}, bf16[4,128,128]{2,1,0:T(8,128)(2,1)S(1)}, u32[]{:S(2)}, u32[]{:S(2)}) collective-permute-start(bf16[4,128,128]{2,1,0:T(8,128)(2,1)S(1)} %shard_map.147.refs_0_), channel_id=1, source_target_pairs={{0,2},{1,3},{2,0},{3,1},{4,6},{5,7},{6,4},{7,5},{8,10},{9,11},{10,... | collective-permute-start | bytes 393224 | tf_op jit(solution)/shard_map/ppermute | solution.py:324
  41.3 36.3 %collective-permute-start.27 = (bf16[2,384,1024]{2,1,0:T(8,128)(2,1)S(1)}, bf16[2,384,1024]{2,1,0:T(8,128)(2,1)S(1)}, u32[]{:S(2)}, u32[]{:S(2)}) collective-permute-start(bf16[2,384,1024]{2,1,0:T(8,128)(2,1)S(1)} %copy-done), channel_id=1, source_target_pairs={{0,1},{1,0},{2,3},{3,2},{4,5},{5,4},{6,7},{7,6},{8,9},{9,8},{10,11... | collective-permute-start | bytes 4718600 | tf_op jit(solution)/shard_map/ppermute | solution.py:324
  41.3 3.6 %collective-permute-start.14 = (bf16[4,128,128]{2,1,0:T(8,128)(2,1)S(1)}, bf16[4,128,128]{2,1,0:T(8,128)(2,1)S(1)}, u32[]{:S(2)}, u32[]{:S(2)}) collective-permute-start(bf16[4,128,128]{2,1,0:T(8,128)(2,1)S(1)} %shard_map.147.refs_0_), channel_id=1, source_target_pairs={{0,1},{1,0},{2,3},{3,2},{4,5},{5,4},{6,7},{7,6},{8,9},{9,8},{10,11... | collective-permute-start | bytes 393224 | tf_op jit(solution)/shard_map/ppermute | solution.py:324
  44.7 1.3 %collective-permute-start.15 = (bf16[4,128,128]{2,1,0:T(8,128)(2,1)S(1)}, bf16[4,128,128]{2,1,0:T(8,128)(2,1)S(1)}, u32[]{:S(2)}, u32[]{:S(2)}) collective-permute-start(bf16[4,128,128]{2,1,0:T(8,128)(2,1)S(1)} %collective-permute-done.13.refs_1_), channel_id=1, source_target_pairs={{0,1},{1,0},{2,3},{3,2},{4,5},{5,4},{6,7},{7,6},{8,9},{9,8},{10,11... | collective-permute-start | bytes 393224 | tf_op jit(solution)/shard_map/ppermute | solution.py:324
  47.5 1.8 %collective-permute-start.16 = (bf16[128,1024]{1,0:T(8,128)(2,1)S(1)}, bf16[128,1024]{1,0:T(8,128)(2,1)S(1)}, u32[]{:S(2)}, u32[]{:S(2)}) collective-permute-start(bf16[128,1024]{1,0:T(8,128)(2,1)S(1)} %shard_map.148.own_ref.mixed_ref), channel_id=1, source_target_pairs={{0,1},{1,0},{2,3},{3,2},{4,5},{5,4},{6,7},{7,6},{8,9},{9,8},{10,11... | collective-permute-start | bytes 786440 | tf_op jit(solution)/shard_map/ppermute | solution.py:324
  47.7 1.4 %collective-permute-start.17 = (f32[1,1024]{1,0:T(1,128)S(1)}, f32[1,1024]{1,0:T(1,128)S(1)}, u32[]{:S(2)}, u32[]{:S(2)}) collective-permute-start(f32[1,1024]{1,0:T(1,128)S(1)} %bitcast.9), channel_id=1, source_target_pairs={{0,1},{1,0},{2,3},{3,2},{4,5},{5,4},{6,7},{7,6},{8,9},{9,8},{10,11... | collective-permute-start | bytes 12296 | tf_op jit(solution)/shard_map/ppermute | solution.py:324
  49.1 2.3 %collective-permute-start.20 = (bf16[1024,384]{1,0:T(8,128)(2,1)S(1)}, bf16[1024,384]{1,0:T(8,128)(2,1)S(1)}, u32[]{:S(2)}, u32[]{:S(2)}) collective-permute-start(bf16[1024,384]{1,0:T(8,128)(2,1)S(1)} %copy-done.8), channel_id=1, source_target_pairs={{0,1},{1,0},{2,3},{3,2},{4,5},{5,4},{6,7},{7,6},{8,9},{9,8},{10,11... | collective-permute-start | bytes 2359304 | tf_op jit(solution)/shard_map/ppermute | solution.py:324
  49.3 3.3 %collective-permute-start.21 = (bf16[1024,384]{1,0:T(8,128)(2,1)S(1)}, bf16[1024,384]{1,0:T(8,128)(2,1)S(1)}, u32[]{:S(2)}, u32[]{:S(2)}) collective-permute-start(bf16[1024,384]{1,0:T(8,128)(2,1)S(1)} %copy-done.9), channel_id=1, source_target_pairs={{0,1},{1,0},{2,3},{3,2},{4,5},{5,4},{6,7},{7,6},{8,9},{9,8},{10,11... | collective-permute-start | bytes 2359304 | tf_op jit(solution)/shard_map/ppermute | solution.py:324
  51.4 10.1 %collective-permute-start.24 = (bf16[2,32,1024]{2,1,0:T(8,128)(2,1)S(1)}, bf16[2,32,1024]{2,1,0:T(8,128)(2,1)S(1)}, u32[]{:S(2)}, u32[]{:S(2)}) collective-permute-start(bf16[2,32,1024]{2,1,0:T(8,128)(2,1)S(1)} %get-tuple-element.63), channel_id=1, source_target_pairs={{0,16},{4,20},{8,24},{12,28},{16,0},{20,4},{24,8},{28,12},{1,17},{... | collective-permute-start | bytes 393224 | tf_op jit(solution)/shard_map/ppermute | solution.py:324
  52.5 11.6 %collective-permute-start.25 = (bf16[2,32,1024]{2,1,0:T(8,128)(2,1)S(1)}, bf16[2,32,1024]{2,1,0:T(8,128)(2,1)S(1)}, u32[]{:S(2)}, u32[]{:S(2)}) collective-permute-start(bf16[2,32,1024]{2,1,0:T(8,128)(2,1)S(1)} %get-tuple-element.64), channel_id=1, source_target_pairs={{0,20},{4,16},{8,28},{12,24},{16,4},{20,0},{24,12},{28,8},{1,21},{... | collective-permute-start | bytes 393224 | tf_op jit(solution)/shard_map/ppermute | solution.py:324
  61.5 5.4 %collective-permute-start.30 = (bf16[2,32,1024]{2,1,0:T(8,128)(2,1)S(1)}, bf16[2,32,1024]{2,1,0:T(8,128)(2,1)S(1)}, u32[]{:S(2)}, u32[]{:S(2)}) collective-permute-start(bf16[2,32,1024]{2,1,0:T(8,128)(2,1)S(1)} %get-tuple-element.69), channel_id=1, source_target_pairs={{0,4},{4,0},{8,12},{12,8},{16,20},{20,16},{24,28},{28,24},{1,5},{5... | collective-permute-start | bytes 393224 | tf_op jit(solution)/shard_map/ppermute | solution.py:324
  64.1 9.2 %collective-permute-start.31 = (bf16[2,32,1024]{2,1,0:T(8,128)(2,1)S(1)}, bf16[2,32,1024]{2,1,0:T(8,128)(2,1)S(1)}, u32[]{:S(2)}, u32[]{:S(2)}) collective-permute-start(bf16[2,32,1024]{2,1,0:T(8,128)(2,1)S(1)} %get-tuple-element.70), channel_id=1, source_target_pairs={{0,8},{4,12},{8,0},{12,4},{16,24},{20,28},{24,16},{28,20},{1,9},{5... | collective-permute-start | bytes 393224 | tf_op jit(solution)/shard_map/ppermute | solution.py:324
  67.0 8.0 %collective-permute-start.32 = (bf16[2,32,1024]{2,1,0:T(8,128)(2,1)S(1)}, bf16[2,32,1024]{2,1,0:T(8,128)(2,1)S(1)}, u32[]{:S(2)}, u32[]{:S(2)}) collective-permute-start(bf16[2,32,1024]{2,1,0:T(8,128)(2,1)S(1)} %get-tuple-element.71), channel_id=1, source_target_pairs={{0,12},{4,8},{8,4},{12,0},{16,28},{20,24},{24,20},{28,16},{1,13},{... | collective-permute-start | bytes 393224 | tf_op jit(solution)/shard_map/ppermute | solution.py:324
  67.3 17.2 %collective-permute-start.37 = (bf16[2,32,1024]{2,1,0:T(8,128)(2,1)S(1)}, bf16[2,32,1024]{2,1,0:T(8,128)(2,1)S(1)}, u32[]{:S(2)}, u32[]{:S(2)}) collective-permute-start(bf16[2,32,1024]{2,1,0:T(8,128)(2,1)S(1)} %get-tuple-element.77), channel_id=1, source_target_pairs={{0,24},{4,28},{8,16},{12,20},{16,8},{20,12},{24,0},{28,4},{1,25},{... | collective-permute-start | bytes 393224 | tf_op jit(solution)/shard_map/ppermute | solution.py:324
  69.9 18.1 %collective-permute-start.38 = (bf16[2,32,1024]{2,1,0:T(8,128)(2,1)S(1)}, bf16[2,32,1024]{2,1,0:T(8,128)(2,1)S(1)}, u32[]{:S(2)}, u32[]{:S(2)}) collective-permute-start(bf16[2,32,1024]{2,1,0:T(8,128)(2,1)S(1)} %get-tuple-element.78), channel_id=1, source_target_pairs={{0,28},{4,24},{8,20},{12,16},{16,12},{20,8},{24,4},{28,0},{1,29},{... | collective-permute-start | bytes 393224 | tf_op jit(solution)/shard_map/ppermute | solution.py:324
  73.3 5.7 %collective-permute-start.26 = (bf16[64,896]{1,0:T(8,128)(2,1)S(1)}, bf16[64,896]{1,0:T(8,128)(2,1)S(1)}, u32[]{:S(2)}, u32[]{:S(2)}) collective-permute-start(bf16[64,896]{1,0:T(8,128)(2,1)S(1)} %shard_map.154.a_ref), channel_id=1, source_target_pairs={{0,2},{1,3},{2,0},{3,1},{4,6},{5,7},{6,4},{7,5},{8,10},{9,11},{10,... | collective-permute-start | bytes 344072 | tf_op jit(solution)/shard_map/ppermute | solution.py:324
  75.6 19.1 %collective-permute-start.33 = (bf16[128,896]{1,0:T(8,128)(2,1)S(1)}, bf16[128,896]{1,0:T(8,128)(2,1)S(1)}, u32[]{:S(2)}, u32[]{:S(2)}) collective-permute-start(bf16[128,896]{1,0:T(8,128)(2,1)S(1)} %shard_map.157.a_ref), channel_id=1, source_target_pairs={{0,2},{1,3},{2,0},{3,1},{4,6},{5,7},{6,4},{7,5},{8,10},{9,11},{10,... | collective-permute-start | bytes 688136 | tf_op jit(solution)/shard_map/ppermute | solution.py:324
  77.6 12.7 %collective-permute-start.22 = (bf16[64,896]{1,0:T(8,128)(2,1)S(1)}, bf16[64,896]{1,0:T(8,128)(2,1)S(1)}, u32[]{:S(2)}, u32[]{:S(2)}) collective-permute-start(bf16[64,896]{1,0:T(8,128)(2,1)S(1)} %shard_map.150.a_ref), channel_id=1, source_target_pairs={{0,2},{1,3},{2,0},{3,1},{4,6},{5,7},{6,4},{7,5},{8,10},{9,11},{10,... | collective-permute-start | bytes 344072 | tf_op jit(solution)/shard_map/ppermute | solution.py:324
  80.1 19.3 %collective-permute-start.28 = (bf16[2,32,1024]{2,1,0:T(8,128)(2,1)S(1)}, bf16[2,32,1024]{2,1,0:T(8,128)(2,1)S(1)}, u32[]{:S(2)}, u32[]{:S(2)}) collective-permute-start(bf16[2,32,1024]{2,1,0:T(8,128)(2,1)S(1)} %get-tuple-element.65), channel_id=1, source_target_pairs={{0,16},{4,20},{8,24},{12,28},{16,0},{20,4},{24,8},{28,12},{1,17},{... | collective-permute-start | bytes 393224 | tf_op jit(solution)/shard_map/ppermute | solution.py:324
  84.5 17.1 %collective-permute-start.29 = (bf16[2,32,1024]{2,1,0:T(8,128)(2,1)S(1)}, bf16[2,32,1024]{2,1,0:T(8,128)(2,1)S(1)}, u32[]{:S(2)}, u32[]{:S(2)}) collective-permute-start(bf16[2,32,1024]{2,1,0:T(8,128)(2,1)S(1)} %get-tuple-element.66), channel_id=1, source_target_pairs={{0,20},{4,16},{8,28},{12,24},{16,4},{20,0},{24,12},{28,8},{1,21},{... | collective-permute-start | bytes 393224 | tf_op jit(solution)/shard_map/ppermute | solution.py:324
  88.7 4.9 %collective-permute-start.39 = (bf16[64,896]{1,0:T(8,128)(2,1)S(1)}, bf16[64,896]{1,0:T(8,128)(2,1)S(1)}, u32[]{:S(2)}, u32[]{:S(2)}) collective-permute-start(bf16[64,896]{1,0:T(8,128)(2,1)S(1)} %shard_map.160.a_ref), channel_id=1, source_target_pairs={{0,2},{1,3},{2,0},{3,1},{4,6},{5,7},{6,4},{7,5},{8,10},{9,11},{10,... | collective-permute-start | bytes 344072 | tf_op jit(solution)/shard_map/ppermute | solution.py:324
  90.5 6.0 %collective-permute-start.23 = (bf16[64,384]{1,0:T(8,128)(2,1)S(1)}, bf16[64,384]{1,0:T(8,128)(2,1)S(1)}, u32[]{:S(2)}, u32[]{:S(2)}) collective-permute-start(bf16[64,384]{1,0:T(8,128)(2,1)S(1)} %shard_map.151.mine_ref), channel_id=1, source_target_pairs={{0,1},{1,0},{2,3},{3,2},{4,5},{5,4},{6,7},{7,6},{8,9},{9,8},{10,11... | collective-permute-start | bytes 147464 | tf_op jit(solution)/shard_map/ppermute | solution.py:324
  94.6 8.1 %copy-start.1 = (bf16[384,1024]{1,0:T(8,128)(2,1)S(1)}, bf16[384,1024]{1,0:T(8,128)(2,1)}, u32[]{:S(2)}) copy-start(bf16[384,1024]{1,0:T(8,128)(2,1)} %down_ref.1) | copy-start | bytes 2359300
  95.8 8.1 %collective-permute-start.34 = (bf16[2,32,1024]{2,1,0:T(8,128)(2,1)S(1)}, bf16[2,32,1024]{2,1,0:T(8,128)(2,1)S(1)}, u32[]{:S(2)}, u32[]{:S(2)}) collective-permute-start(bf16[2,32,1024]{2,1,0:T(8,128)(2,1)S(1)} %get-tuple-element.73), channel_id=1, source_target_pairs={{0,4},{4,0},{8,12},{12,8},{16,20},{20,16},{24,28},{28,24},{1,5},{5... | collective-permute-start | bytes 393224 | tf_op jit(solution)/shard_map/ppermute | solution.py:324
  95.9 8.0 %collective-permute-start.35 = (bf16[2,32,1024]{2,1,0:T(8,128)(2,1)S(1)}, bf16[2,32,1024]{2,1,0:T(8,128)(2,1)S(1)}, u32[]{:S(2)}, u32[]{:S(2)}) collective-permute-start(bf16[2,32,1024]{2,1,0:T(8,128)(2,1)S(1)} %get-tuple-element.74), channel_id=1, source_target_pairs={{0,8},{4,12},{8,0},{12,4},{16,24},{20,28},{24,16},{28,20},{1,9},{5... | collective-permute-start | bytes 393224 | tf_op jit(solution)/shard_map/ppermute | solution.py:324
  96.5 9.5 %collective-permute-start.36 = (bf16[2,32,1024]{2,1,0:T(8,128)(2,1)S(1)}, bf16[2,32,1024]{2,1,0:T(8,128)(2,1)S(1)}, u32[]{:S(2)}, u32[]{:S(2)}) collective-permute-start(bf16[2,32,1024]{2,1,0:T(8,128)(2,1)S(1)} %get-tuple-element.75), channel_id=1, source_target_pairs={{0,12},{4,8},{8,4},{12,0},{16,28},{20,24},{24,20},{28,16},{1,13},{... | collective-permute-start | bytes 393224 | tf_op jit(solution)/shard_map/ppermute | solution.py:324
  99.4 8.2 %collective-permute-start.40 = (bf16[2,32,1024]{2,1,0:T(8,128)(2,1)S(1)}, bf16[2,32,1024]{2,1,0:T(8,128)(2,1)S(1)}, u32[]{:S(2)}, u32[]{:S(2)}) collective-permute-start(bf16[2,32,1024]{2,1,0:T(8,128)(2,1)S(1)} %get-tuple-element.79), channel_id=1, source_target_pairs={{0,24},{4,28},{8,16},{12,20},{16,8},{20,12},{24,0},{28,4},{1,25},{... | collective-permute-start | bytes 393224 | tf_op jit(solution)/shard_map/ppermute | solution.py:324
  101.6 8.2 %collective-permute-start.41 = (bf16[2,32,1024]{2,1,0:T(8,128)(2,1)S(1)}, bf16[2,32,1024]{2,1,0:T(8,128)(2,1)S(1)}, u32[]{:S(2)}, u32[]{:S(2)}) collective-permute-start(bf16[2,32,1024]{2,1,0:T(8,128)(2,1)S(1)} %get-tuple-element.80), channel_id=1, source_target_pairs={{0,28},{4,24},{8,20},{12,16},{16,12},{20,8},{24,4},{28,0},{1,29},{... | collective-permute-start | bytes 393224 | tf_op jit(solution)/shard_map/ppermute | solution.py:324
  110.1 2.0 %collective-permute-start.42 = (f32[128,1024]{1,0:T(8,128)S(1)}, f32[128,1024]{1,0:T(8,128)S(1)}, u32[]{:S(2)}, u32[]{:S(2)}) collective-permute-start(f32[128,1024]{1,0:T(8,128)S(1)} %get-tuple-element.82), channel_id=1, source_target_pairs={{0,1},{1,0},{2,3},{3,2},{4,5},{5,4},{6,7},{7,6},{8,9},{9,8},{10,11... | collective-permute-start | bytes 1572872 | tf_op jit(solution)/shard_map/ppermute | solution.py:324
  (5 other events, 19.5 us)

commit v4 on v3

--- a/solution.py
+++ b/solution.py
@@ -88,23 +88,31 @@
         copy.wait()
 
 
-def lay_kernel(at_ref, *refs):
+def lay_kernel(at_ref, own_gate, own_up, *refs):
+    own_ref, sems = refs[6:]
+    copies = []
+    for i, src in enumerate((own_gate, own_up)):
+        cols = pl.ds(i * src.shape[1], src.shape[1])
+        copies.append(pltpu.make_async_copy(src, own_ref.at[:, cols], sems.at[i]))
+        copies[-1].start()
     for i, (ref, out) in enumerate(zip(refs[:4], refs[4:5] * 2 + refs[5:6] * 2)):
         value = ref[at_ref[4]] if i < 2 else ref[...]
         width = value.shape[1]
         out[:, i % 2 * width : (i % 2 + 1) * width] = value
+    for copy in copies:
+        copy.wait()
 
 
 def attention_kernel(at_ref, *refs, heads, group):
     blocks = heads * group
-    weights, refs = refs[:5], refs[5:]
-    ins, q_ins, outs = refs[:blocks], refs[blocks : blocks + heads], refs[blocks + heads : -8]
-    w_ref, laid_ref, shared_ref, kv_ref, q_ref, acc_ref, carry_ref, sems = refs[-8:]
+    weights, refs = refs[:3], refs[3:]
+    ins, q_ins, outs = refs[:blocks], refs[blocks : blocks + heads], refs[blocks + heads : -7]
+    w_ref, laid_ref, kv_ref, q_ref, acc_ref, carry_ref, sems = refs[-7:]
     e = at_ref[4]
     moves = [(weights[0], w_ref)]
-    for i, src in enumerate((weights[1].at[e], weights[2].at[e], *weights[3:])):
-        cols = pl.ds(i % 2 * src.shape[1], src.shape[1])
-        moves.append((src, (laid_ref if i < 2 else shared_ref).at[:, cols]))
+    for i, src in enumerate((weights[1].at[e], weights[2].at[e])):
+        cols = pl.ds(i * src.shape[1], src.shape[1])
+        moves.append((src, laid_ref.at[:, cols]))
     fetches = [pltpu.make_async_copy(a, b, sems.at[i]) for i, (a, b) in enumerate(moves)]
     for fetch in fetches:
         fetch.start()
@@ -310,11 +318,11 @@
         if outs == 1:
             out_refs[0][side] = total
         else:
-            out_refs[side][...] = total
+            out_refs[side][...] = total.astype(out_refs[side].dtype)
 
 
 def final_kernel(a_ref, b_ref, out_ref):
-    out_ref[...] = (a_ref[...] + b_ref[...]).astype(BF)
+    out_ref[...] = (a_ref[...] + b_ref[...].astype(F32)).astype(BF)
 
 
 def swap(x, axis, bit):
@@ -375,21 +383,26 @@
     hid_s = shared_gate.shape[1]
     width = 2 * gate_proj.shape[2]
     wide = (array(feats, width), array(feats, 2 * hid_s))
-    laid_other, shared_other = call(lay_kernel, wide, [smem()] + [vmem()] * 4)(at, *others[1:5])
-    *attended, out_w, laid_own, shared_own = call(
+    laid_other, shared_other, shared_own = call(
+        lay_kernel,
+        wide + wide[1:],
+        [smem()] + [hbm()] * 2 + [vmem()] * 4,
+        [pltpu.SemaphoreType.DMA((2,))],
+    )(at, in_hbm(shared_gate), in_hbm(shared_up), *others[1:5])
+    *attended, out_w, laid_own = call(
         functools.partial(attention_kernel, heads=heads, group=group),
-        (array(tok, hd),) * heads + (array(*out_proj.shape),) + wide,
-        [smem()] + [hbm()] * 5 + [vmem()] * (blocks + heads),
+        (array(tok, hd),) * heads + (array(*out_proj.shape),) + wide[:1],
+        [smem()] + [hbm()] * 3 + [vmem()] * (blocks + heads),
         [
             pltpu.VMEM((blocks, kv_rows, hd), BF),
             pltpu.VMEM((heads * tok, hd), BF),
             pltpu.VMEM((heads * tok, hd), F32),
             pltpu.VMEM((heads * tok, tok), F32),
-            pltpu.SemaphoreType.DMA((5,)),
+            pltpu.SemaphoreType.DMA((3,)),
         ],
     )(
         at,
-        *[in_hbm(x) for x in (out_proj, gate_proj, up_proj, shared_gate, shared_up)],
+        *[in_hbm(x) for x in (out_proj, gate_proj, up_proj)],
         *kv,
         *q,
     )
@@ -471,7 +484,7 @@
         one = jax.ShapeDtypeStruct((tok, feats), F32)
         total = call(
             functools.partial(combine_kernel, outs=2 if last else 1),
-            (one, one) if last else jax.ShapeDtypeStruct((2, tok, feats), F32),
+            (one, array(tok, feats)) if last else jax.ShapeDtypeStruct((2, tok, feats), F32),
             [vmem()] * (2 + len(ms)),
         )(total, picks[i], *[back[m] for m in ms])
     return call(final_kernel, array(tok, feats), [vmem()] * 2)(total[0], swap(total[1], "tp", 1))

time: 113 us -> 112 us (level)
  transfers between devices with their start and end apart: 43 -> 43, of which waited for: 19 -> 19; matrix products, arithmetic and copies ran while one was open for 0% -> 0% of each run, Pallas kernels for 10% -> 11%
where the time goes in v4:
time: 112 us
  starting transfers between devices  51.2 us (46%)
  waiting for transfers between devices  41.5 us (37%)
  Pallas kernels  18.8 us (17%)
    ppermute x43, starting transfers between devices, swap(): return lax.ppermute(x, axis, [(i, i ^ bit) for i in range(count)])  51.2 us
    ppermute x43, waiting for transfers between devices, swap(): return lax.ppermute(x, axis, [(i, i ^ bit) for i in range(count)])  41.5 us
    pallas_call x1, Pallas kernels, layer(): call(functools.partial(attention_kernel, heads=heads, group=group), (arra...  3.53 us
    pallas_call x3, Pallas kernels, layer(): call(functools.partial(down_kernel, width=width, features=features), (arr...  3.28 us
  transfers between devices with their start and end apart: 43, of which 19 were waited for; matrix products, arithmetic and copies ran while one was open for 0% of the time, Pallas kernels for 11%

profile of v4, /device:TPU:0, one launch (start us, length us, event | category | flops | bytes accessed | tf_op | source)
XLA Modules:
  0.0 111.9 jit_solution(16554371602921898024)
XLA Ops:
  0.1 1.6 %shard_map.145 = (bf16[272,128]{1,0:T(8,128)(2,1)S(1)}, bf16[272,128]{1,0:T(8,128)(2,1)S(1)}, bf16[272,128]{1,0:T(8,128)(2,1)S(1)}, bf16[272,128]{1,0:T(8,128)(2...) custom-call(s32[5]{0:T(128)S(1)} %stack.23.at_ref, ...), custom_call_target="tpu_custom_call" | custom-call | tf_op jit(solution)/shard_map/pallas_call | solution.py:374
  1.7 3.1 %collective-permute-start.1 = (bf16[272,128]{1,0:T(8,128)(2,1)S(1)}, bf16[272,128]{1,0:T(8,128)(2,1)S(1)}, u32[]{:S(2)}, u32[]{:S(2)}) collective-permute-start(bf16[272,128]{1,0:T(8,128)(2,1)S(1)} %get-tuple-element.45), channel_id=1, source_target_pairs={{0,8},{4,12},{8,0},{12,4},{16,24},{20,28},{24,16},{28,20},{1,9},{5... | collective-permute-start | bytes 208904 | tf_op jit(solution)/shard_map/ppermute | solution.py:332
  4.8 2.6 %collective-permute-start.3 = (bf16[272,128]{1,0:T(8,128)(2,1)S(1)}, bf16[272,128]{1,0:T(8,128)(2,1)S(1)}, u32[]{:S(2)}, u32[]{:S(2)}) collective-permute-start(bf16[272,128]{1,0:T(8,128)(2,1)S(1)} %get-tuple-element.46), channel_id=1, source_target_pairs={{0,16},{4,20},{8,24},{12,28},{16,0},{20,4},{24,8},{28,12},{1,17},{... | collective-permute-start | bytes 208904 | tf_op jit(solution)/shard_map/ppermute | solution.py:332
  7.4 0.9 collective-permute-start.7
  8.3 1.5 %collective-permute-start = (bf16[272,128]{1,0:T(8,128)(2,1)S(1)}, bf16[272,128]{1,0:T(8,128)(2,1)S(1)}, u32[]{:S(2)}, u32[]{:S(2)}) collective-permute-start(bf16[272,128]{1,0:T(8,128)(2,1)S(1)} %get-tuple-element.44.refs_3_), channel_id=1, source_target_pairs={{0,4},{4,0},{8,12},{12,8},{16,20},{20,16},{24,28},{28,24},{1,5},{5... | collective-permute-start | bytes 208904 | tf_op jit(solution)/shard_map/ppermute | solution.py:332
  10.3 2.0 %collective-permute-done.3.refs_7_ = bf16[272,128]{1,0:T(8,128)(2,1)S(1)} collective-permute-done((bf16[272,128]{1,0:T(8,128)(2,1)S(1)}, bf16[272,128]{1,0:T(8,128)(2,1)S(1)}, u32[]{:S(2)}, u32[]{:S(2)}) %collective-permute-start.3) | collective-permute-done | bytes 69664 | tf_op jit(solution)/shard_map/ppermute | solution.py:332
  12.3 1.5 %collective-permute-start.4 = (bf16[272,128]{1,0:T(8,128)(2,1)S(1)}, bf16[272,128]{1,0:T(8,128)(2,1)S(1)}, u32[]{:S(2)}, u32[]{:S(2)}) collective-permute-start(bf16[272,128]{1,0:T(8,128)(2,1)S(1)} %collective-permute-done.3.refs_7_), channel_id=1, source_target_pairs={{0,4},{4,0},{8,12},{12,8},{16,20},{20,16},{24,28},{28,24},{1,5},{5... | collective-permute-start | bytes 208904 | tf_op jit(solution)/shard_map/ppermute | solution.py:332
  13.8 1.3 %collective-permute-start.6 = (bf16[272,128]{1,0:T(8,128)(2,1)S(1)}, bf16[272,128]{1,0:T(8,128)(2,1)S(1)}, u32[]{:S(2)}, u32[]{:S(2)}) collective-permute-start(bf16[272,128]{1,0:T(8,128)(2,1)S(1)} %collective-permute-done.5.refs_9_), channel_id=1, source_target_pairs={{0,4},{4,0},{8,12},{12,8},{16,20},{20,16},{24,28},{28,24},{1,5},{5... | collective-permute-start | bytes 208904 | tf_op jit(solution)/shard_map/ppermute | solution.py:332
  15.1 1.8 %collective-permute-start.8 = (bf16[128,128]{1,0:T(8,128)(2,1)S(1)}, bf16[128,128]{1,0:T(8,128)(2,1)S(1)}, u32[]{:S(2)}, u32[]{:S(2)}) collective-permute-start(bf16[128,128]{1,0:T(8,128)(2,1)S(1)} %get-tuple-element.50), channel_id=1, source_target_pairs={{0,16},{4,20},{8,24},{12,28},{16,0},{20,4},{24,8},{28,12},{1,17},{... | collective-permute-start | bytes 98312 | tf_op jit(solution)/shard_map/ppermute | solution.py:332
  16.9 3.4 %collective-permute-done.8.refs_13_ = bf16[128,128]{1,0:T(8,128)(2,1)S(1)} collective-permute-done((bf16[128,128]{1,0:T(8,128)(2,1)S(1)}, bf16[128,128]{1,0:T(8,128)(2,1)S(1)}, u32[]{:S(2)}, u32[]{:S(2)}) %collective-permute-start.8) | collective-permute-done | bytes 32800 | tf_op jit(solution)/shard_map/ppermute | solution.py:332
  20.3 3.2 %collective-permute-start.9 = (bf16[128,128]{1,0:T(8,128)(2,1)S(1)}, bf16[128,128]{1,0:T(8,128)(2,1)S(1)}, u32[]{:S(2)}, u32[]{:S(2)}) collective-permute-start(bf16[128,128]{1,0:T(8,128)(2,1)S(1)} %get-tuple-element.51), channel_id=1, source_target_pairs={{0,24},{4,28},{8,16},{12,20},{16,8},{20,12},{24,0},{28,4},{1,25},{... | collective-permute-start | bytes 98312 | tf_op jit(solution)/shard_map/ppermute | solution.py:332
  23.5 2.5 %collective-permute-done.9.refs_14_ = bf16[128,128]{1,0:T(8,128)(2,1)S(1)} collective-permute-done((bf16[128,128]{1,0:T(8,128)(2,1)S(1)}, bf16[128,128]{1,0:T(8,128)(2,1)S(1)}, u32[]{:S(2)}, u32[]{:S(2)}) %collective-permute-start.9) | collective-permute-done | bytes 32800 | tf_op jit(solution)/shard_map/ppermute | solution.py:332
  26.1 3.5 %shard_map.146 = (bf16[128,128]{1,0:T(8,128)(2,1)S(1)}, bf16[128,128]{1,0:T(8,128)(2,1)S(1)}, bf16[128,128]{1,0:T(8,128)(2,1)S(1)}, bf16[128,128]{1,0:T(8,128)(2...) custom-call(s32[5]{0:T(128)S(1)} %stack.23.at_ref, bf16[2048,1024]{1,0:T(8,128)(2,1)} %refs_0_.1, ...), custom_call_target="tpu_custom_call" | custom-call | tf_op jit(solution)/shard_map/pallas_call | solution.py:392
  29.7 3.8 %collective-permute-start.11 = (bf16[128,128]{1,0:T(8,128)(2,1)S(1)}, bf16[128,128]{1,0:T(8,128)(2,1)S(1)}, u32[]{:S(2)}, u32[]{:S(2)}) collective-permute-start(bf16[128,128]{1,0:T(8,128)(2,1)S(1)} %get-tuple-element.54), channel_id=1, source_target_pairs={{0,16},{4,20},{8,24},{12,28},{16,0},{20,4},{24,8},{28,12},{1,17},{... | collective-permute-start | bytes 98312 | tf_op jit(solution)/shard_map/ppermute | solution.py:332
  34.6 0.8 collective-permute-done.11.refs_2_
  35.4 3.8 %collective-permute-done.12.refs_3_ = bf16[128,128]{1,0:T(8,128)(2,1)S(1)} collective-permute-done((bf16[128,128]{1,0:T(8,128)(2,1)S(1)}, bf16[128,128]{1,0:T(8,128)(2,1)S(1)}, u32[]{:S(2)}, u32[]{:S(2)}) %collective-permute-start.12) | collective-permute-done | bytes 32800 | tf_op jit(solution)/shard_map/ppermute | solution.py:332
  39.2 1.6 %collective-permute-start.13 = (bf16[4,128,128]{2,1,0:T(8,128)(2,1)S(1)}, bf16[4,128,128]{2,1,0:T(8,128)(2,1)S(1)}, u32[]{:S(2)}, u32[]{:S(2)}) collective-permute-start(bf16[4,128,128]{2,1,0:T(8,128)(2,1)S(1)} %shard_map.147.refs_0_), channel_id=1, source_target_pairs={{0,2},{1,3},{2,0},{3,1},{4,6},{5,7},{6,4},{7,5},{8,10},{9,11},{10,... | collective-permute-start | bytes 393224 | tf_op jit(solution)/shard_map/ppermute | solution.py:332
  41.3 2.9 %collective-permute-done.13.refs_1_ = bf16[4,128,128]{2,1,0:T(8,128)(2,1)S(1)} collective-permute-done((bf16[4,128,128]{2,1,0:T(8,128)(2,1)S(1)}, bf16[4,128,128]{2,1,0:T(8,128)(2,1)S(1)}, u32[]{:S(2)}, u32[]{:S(2)}) %collective-permute-start.13) | collective-permute-done | bytes 131104 | tf_op jit(solution)/shard_map/ppermute | solution.py:332
  44.4 1.2 %collective-permute-done.15.refs_3_ = bf16[4,128,128]{2,1,0:T(8,128)(2,1)S(1)} collective-permute-done((bf16[4,128,128]{2,1,0:T(8,128)(2,1)S(1)}, bf16[4,128,128]{2,1,0:T(8,128)(2,1)S(1)}, u32[]{:S(2)}, u32[]{:S(2)}) %collective-permute-start.15) | collective-permute-done | bytes 131104 | tf_op jit(solution)/shard_map/ppermute | solution.py:332
  45.6 1.4 %shard_map.148.own_ref.mixed_ref = bf16[128,1024]{1,0:T(8,128)(2,1)S(1)} custom-call(s32[5]{0:T(128)S(1)} %stack.23.at_ref, bf16[4,128,128]{2,1,0:T(8,128)(2,1)S(1)} %shard_map.147.refs_0_, bf16[4,128,128]{2,1,0:T(8,128)(2,1)S(1)} %collective-permute-done.13.refs_1_, bf16[4,128,128]{2,1,0:T(8,128)(2,1)S(1)} %collective-permute-done.14.refs_2_, ...), custom_call_target="tpu_custom_call" | custom-call | tf_op jit(solution)/shard_map/pallas_call | solution.py:422
  47.6 1.0 collective-permute-done.17.refs_1_
  49.2 1.1 shard_map.153
  50.9 1.1 %collective-permute-done.21.refs_3_ = bf16[1024,384]{1,0:T(8,128)(2,1)S(1)} collective-permute-done((bf16[1024,384]{1,0:T(8,128)(2,1)S(1)}, bf16[1024,384]{1,0:T(8,128)(2,1)S(1)}, u32[]{:S(2)}, u32[]{:S(2)}) %collective-permute-start.21) | collective-permute-done | bytes 786464 | tf_op jit(solution)/shard_map/ppermute | solution.py:332
  52.1 1.9 %collective-permute-start.25 = (bf16[2,32,1024]{2,1,0:T(8,128)(2,1)S(1)}, bf16[2,32,1024]{2,1,0:T(8,128)(2,1)S(1)}, u32[]{:S(2)}, u32[]{:S(2)}) collective-permute-start(bf16[2,32,1024]{2,1,0:T(8,128)(2,1)S(1)} %get-tuple-element.64), channel_id=1, source_target_pairs={{0,20},{4,16},{8,28},{12,24},{16,4},{20,0},{24,12},{28,8},{1,21},{... | collective-permute-start | bytes 393224 | tf_op jit(solution)/shard_map/ppermute | solution.py:332
  54.0 7.0 %collective-permute-done.24.refs_4_ = bf16[2,32,1024]{2,1,0:T(8,128)(2,1)S(1)} collective-permute-done((bf16[2,32,1024]{2,1,0:T(8,128)(2,1)S(1)}, bf16[2,32,1024]{2,1,0:T(8,128)(2,1)S(1)}, u32[]{:S(2)}, u32[]{:S(2)}) %collective-permute-start.24) | collective-permute-done | bytes 131104 | tf_op jit(solution)/shard_map/ppermute | solution.py:332
  61.7 2.0 %collective-permute-done.25.refs_5_ = bf16[2,32,1024]{2,1,0:T(8,128)(2,1)S(1)} collective-permute-done((bf16[2,32,1024]{2,1,0:T(8,128)(2,1)S(1)}, bf16[2,32,1024]{2,1,0:T(8,128)(2,1)S(1)}, u32[]{:S(2)}, u32[]{:S(2)}) %collective-permute-start.25) | collective-permute-done | bytes 131104 | tf_op jit(solution)/shard_map/ppermute | solution.py:332
  63.7 2.8 %collective-permute-done.30.refs_5_ = bf16[2,32,1024]{2,1,0:T(8,128)(2,1)S(1)} collective-permute-done((bf16[2,32,1024]{2,1,0:T(8,128)(2,1)S(1)}, bf16[2,32,1024]{2,1,0:T(8,128)(2,1)S(1)}, u32[]{:S(2)}, u32[]{:S(2)}) %collective-permute-start.30) | collective-permute-done | bytes 131104 | tf_op jit(solution)/shard_map/ppermute | solution.py:332
  66.8 2.6 %collective-permute-start.37 = (bf16[2,32,1024]{2,1,0:T(8,128)(2,1)S(1)}, bf16[2,32,1024]{2,1,0:T(8,128)(2,1)S(1)}, u32[]{:S(2)}, u32[]{:S(2)}) collective-permute-start(bf16[2,32,1024]{2,1,0:T(8,128)(2,1)S(1)} %get-tuple-element.77), channel_id=1, source_target_pairs={{0,24},{4,28},{8,16},{12,20},{16,8},{20,12},{24,0},{28,4},{1,25},{... | collective-permute-start | bytes 393224 | tf_op jit(solution)/shard_map/ppermute | solution.py:332
  69.4 1.9 %collective-permute-start.38 = (bf16[2,32,1024]{2,1,0:T(8,128)(2,1)S(1)}, bf16[2,32,1024]{2,1,0:T(8,128)(2,1)S(1)}, u32[]{:S(2)}, u32[]{:S(2)}) collective-permute-start(bf16[2,32,1024]{2,1,0:T(8,128)(2,1)S(1)} %get-tuple-element.78), channel_id=1, source_target_pairs={{0,28},{4,24},{8,20},{12,16},{16,12},{20,8},{24,4},{28,0},{1,29},{... | collective-permute-start | bytes 393224 | tf_op jit(solution)/shard_map/ppermute | solution.py:332
  71.3 1.9 %shard_map.149 = (bf16[1024,768]{1,0:T(8,128)(2,1)S(1)}, bf16[1024,768]{1,0:T(8,128)(2,1)S(1)}, bf16[1024,768]{1,0:T(8,128)(2,1)S(1)}) custom-call(s32[5]{0:T(128)S(1)} %stack.23.at_ref, bf16[1024,384]{1,0:T(8,128)(2,1)} %own_gate.1, bf16[1024,384]{1,0:T(8,128)(2,1)} %own_up.1, bf16[2,1024,384]{2,1,0:T(8,128)(2,1)S(1)} %collective-permute-done.18.refs_0_, ...), custom_call_target="tpu_custom_call" | custom-call | tf_op jit(solution)/shard_map/pallas_call | solution.py:386
  73.9 1.6 %collective-permute-start.26 = (bf16[64,896]{1,0:T(8,128)(2,1)S(1)}, bf16[64,896]{1,0:T(8,128)(2,1)S(1)}, u32[]{:S(2)}, u32[]{:S(2)}) collective-permute-start(bf16[64,896]{1,0:T(8,128)(2,1)S(1)} %shard_map.154.a_ref), channel_id=1, source_target_pairs={{0,2},{1,3},{2,0},{3,1},{4,6},{5,7},{6,4},{7,5},{8,10},{9,11},{10,... | collective-permute-start | bytes 344072 | tf_op jit(solution)/shard_map/ppermute | solution.py:332
  76.7 1.2 %shard_map.150.a_ref = bf16[64,896]{1,0:T(8,128)(2,1)S(1)} custom-call(s32[5]{0:T(128)S(1)} %stack.23.at_ref, bf16[128,1024]{1,0:T(8,128)(2,1)S(1)} %shard_map.148.own_ref.mixed_ref, bf16[128,1024]{1,0:T(8,128)(2,1)S(1)} %collective-permute-done.16.other_ref, f32[1,1024]{1,0:T(1,128)S(1)} %bitcast.12, f32[1,1024]{1,0:T(1,128)S(1)} %collective-permute-done.17.refs_1_, ...), custom_call_target="tpu_custom_call" | custom-call | tf_op jit(solution)/shard_map/pallas_call | solution.py:440
  78.0 1.6 %collective-permute-start.22 = (bf16[64,896]{1,0:T(8,128)(2,1)S(1)}, bf16[64,896]{1,0:T(8,128)(2,1)S(1)}, u32[]{:S(2)}, u32[]{:S(2)}) collective-permute-start(bf16[64,896]{1,0:T(8,128)(2,1)S(1)} %shard_map.150.a_ref), channel_id=1, source_target_pairs={{0,2},{1,3},{2,0},{3,1},{4,6},{5,7},{6,4},{7,5},{8,10},{9,11},{10,... | collective-permute-start | bytes 344072 | tf_op jit(solution)/shard_map/ppermute | solution.py:332
  79.6 1.1 shard_map.155
  80.7 3.2 %collective-permute-start.28 = (bf16[2,32,1024]{2,1,0:T(8,128)(2,1)S(1)}, bf16[2,32,1024]{2,1,0:T(8,128)(2,1)S(1)}, u32[]{:S(2)}, u32[]{:S(2)}) collective-permute-start(bf16[2,32,1024]{2,1,0:T(8,128)(2,1)S(1)} %get-tuple-element.65), channel_id=1, source_target_pairs={{0,16},{4,20},{8,24},{12,28},{16,0},{20,4},{24,8},{28,12},{1,17},{... | collective-permute-start | bytes 393224 | tf_op jit(solution)/shard_map/ppermute | solution.py:332
  83.9 3.6 %collective-permute-start.29 = (bf16[2,32,1024]{2,1,0:T(8,128)(2,1)S(1)}, bf16[2,32,1024]{2,1,0:T(8,128)(2,1)S(1)}, u32[]{:S(2)}, u32[]{:S(2)}) collective-permute-start(bf16[2,32,1024]{2,1,0:T(8,128)(2,1)S(1)} %get-tuple-element.66), channel_id=1, source_target_pairs={{0,20},{4,16},{8,28},{12,24},{16,4},{20,0},{24,12},{28,8},{1,21},{... | collective-permute-start | bytes 393224 | tf_op jit(solution)/shard_map/ppermute | solution.py:332
  88.2 1.6 %collective-permute-start.39 = (bf16[64,896]{1,0:T(8,128)(2,1)S(1)}, bf16[64,896]{1,0:T(8,128)(2,1)S(1)}, u32[]{:S(2)}, u32[]{:S(2)}) collective-permute-start(bf16[64,896]{1,0:T(8,128)(2,1)S(1)} %shard_map.160.a_ref), channel_id=1, source_target_pairs={{0,2},{1,3},{2,0},{3,1},{4,6},{5,7},{6,4},{7,5},{8,10},{9,11},{10,... | collective-permute-start | bytes 344072 | tf_op jit(solution)/shard_map/ppermute | solution.py:332
  90.1 3.0 %collective-permute-done.39.b_ref = bf16[64,896]{1,0:T(8,128)(2,1)S(1)} collective-permute-done((bf16[64,896]{1,0:T(8,128)(2,1)S(1)}, bf16[64,896]{1,0:T(8,128)(2,1)S(1)}, u32[]{:S(2)}, u32[]{:S(2)}) %collective-permute-start.39) | collective-permute-done | bytes 114720 | tf_op jit(solution)/shard_map/ppermute | solution.py:332
  93.1 1.1 shard_map.161
  94.2 1.1 %shard_map.158 = (bf16[2,32,1024]{2,1,0:T(8,128)(2,1)S(1)}, bf16[2,32,1024]{2,1,0:T(8,128)(2,1)S(1)}, bf16[2,32,1024]{2,1,0:T(8,128)(2,1)S(1)}, bf16[2,32,1024]{2,1,0:T(8,128)(2,1)S(1)}) custom-call(s32[5]{0:T(128)S(1)} %stack.23.at_ref, bf16[128,896]{1,0:T(8,128)(2,1)S(1)} %shard_map.157.a_ref, bf16[128,896]{1,0:T(8,128)(2,1)S(1)} %collective-permute-done.33.b_ref, ...), custom_call_target="tpu_custom_call" | custom-call | tf_op jit(solution)/shard_map/pallas_call | solution.py:469
  96.0 2.9 %collective-permute-start.36 = (bf16[2,32,1024]{2,1,0:T(8,128)(2,1)S(1)}, bf16[2,32,1024]{2,1,0:T(8,128)(2,1)S(1)}, u32[]{:S(2)}, u32[]{:S(2)}) collective-permute-start(bf16[2,32,1024]{2,1,0:T(8,128)(2,1)S(1)} %get-tuple-element.75), channel_id=1, source_target_pairs={{0,12},{4,8},{8,4},{12,0},{16,28},{20,24},{24,20},{28,16},{1,13},{... | collective-permute-start | bytes 393224 | tf_op jit(solution)/shard_map/ppermute | solution.py:332
  98.9 2.2 %collective-permute-start.40 = (bf16[2,32,1024]{2,1,0:T(8,128)(2,1)S(1)}, bf16[2,32,1024]{2,1,0:T(8,128)(2,1)S(1)}, u32[]{:S(2)}, u32[]{:S(2)}) collective-permute-start(bf16[2,32,1024]{2,1,0:T(8,128)(2,1)S(1)} %get-tuple-element.79), channel_id=1, source_target_pairs={{0,24},{4,28},{8,16},{12,20},{16,8},{20,12},{24,0},{28,4},{1,25},{... | collective-permute-start | bytes 393224 | tf_op jit(solution)/shard_map/ppermute | solution.py:332
  101.0 1.2 %collective-permute-start.41 = (bf16[2,32,1024]{2,1,0:T(8,128)(2,1)S(1)}, bf16[2,32,1024]{2,1,0:T(8,128)(2,1)S(1)}, u32[]{:S(2)}, u32[]{:S(2)}) collective-permute-start(bf16[2,32,1024]{2,1,0:T(8,128)(2,1)S(1)} %get-tuple-element.80), channel_id=1, source_target_pairs={{0,28},{4,24},{8,20},{12,16},{16,12},{20,8},{24,4},{28,0},{1,29},{... | collective-permute-start | bytes 393224 | tf_op jit(solution)/shard_map/ppermute | solution.py:332
  102.2 0.9 shard_map.152
  103.4 2.1 %collective-permute-done.36.refs_3_ = bf16[2,32,1024]{2,1,0:T(8,128)(2,1)S(1)} collective-permute-done((bf16[2,32,1024]{2,1,0:T(8,128)(2,1)S(1)}, bf16[2,32,1024]{2,1,0:T(8,128)(2,1)S(1)}, u32[]{:S(2)}, u32[]{:S(2)}) %collective-permute-start.36) | collective-permute-done | bytes 131104 | tf_op jit(solution)/shard_map/ppermute | solution.py:332
  105.8 1.2 %collective-permute-done.40.refs_0_ = bf16[2,32,1024]{2,1,0:T(8,128)(2,1)S(1)} collective-permute-done((bf16[2,32,1024]{2,1,0:T(8,128)(2,1)S(1)}, bf16[2,32,1024]{2,1,0:T(8,128)(2,1)S(1)}, u32[]{:S(2)}, u32[]{:S(2)}) %collective-permute-start.40) | collective-permute-done | bytes 131104 | tf_op jit(solution)/shard_map/ppermute | solution.py:332
  107.1 2.1 %collective-permute-done.41.refs_1_ = bf16[2,32,1024]{2,1,0:T(8,128)(2,1)S(1)} collective-permute-done((bf16[2,32,1024]{2,1,0:T(8,128)(2,1)S(1)}, bf16[2,32,1024]{2,1,0:T(8,128)(2,1)S(1)}, u32[]{:S(2)}, u32[]{:S(2)}) %collective-permute-start.41) | collective-permute-done | bytes 131104 | tf_op jit(solution)/shard_map/ppermute | solution.py:332
  109.6 1.5 %collective-permute-done.42.b_ref = bf16[128,1024]{1,0:T(8,128)(2,1)S(1)} collective-permute-done((bf16[128,1024]{1,0:T(8,128)(2,1)S(1)}, bf16[128,1024]{1,0:T(8,128)(2,1)S(1)}, u32[]{:S(2)}, u32[]{:S(2)}) %collective-permute-start.42) | collective-permute-done | bytes 262176 | tf_op jit(solution)/shard_map/ppermute | solution.py:332
  (78 shorter events, 10.6 us)
Async XLA Ops:
  1.7 8.1 %collective-permute-start.1 = (bf16[272,128]{1,0:T(8,128)(2,1)S(1)}, bf16[272,128]{1,0:T(8,128)(2,1)S(1)}, u32[]{:S(2)}, u32[]{:S(2)}) collective-permute-start(bf16[272,128]{1,0:T(8,128)(2,1)S(1)} %get-tuple-element.45), channel_id=1, source_target_pairs={{0,8},{4,12},{8,0},{12,4},{16,24},{20,28},{24,16},{28,20},{1,9},{5... | collective-permute-start | bytes 208904 | tf_op jit(solution)/shard_map/ppermute | solution.py:332
  4.8 7.5 %collective-permute-start.3 = (bf16[272,128]{1,0:T(8,128)(2,1)S(1)}, bf16[272,128]{1,0:T(8,128)(2,1)S(1)}, u32[]{:S(2)}, u32[]{:S(2)}) collective-permute-start(bf16[272,128]{1,0:T(8,128)(2,1)S(1)} %get-tuple-element.46), channel_id=1, source_target_pairs={{0,16},{4,20},{8,24},{12,28},{16,0},{20,4},{24,8},{28,12},{1,17},{... | collective-permute-start | bytes 208904 | tf_op jit(solution)/shard_map/ppermute | solution.py:332
  7.4 6.4 %collective-permute-start.5 = (bf16[272,128]{1,0:T(8,128)(2,1)S(1)}, bf16[272,128]{1,0:T(8,128)(2,1)S(1)}, u32[]{:S(2)}, u32[]{:S(2)}) collective-permute-start(bf16[272,128]{1,0:T(8,128)(2,1)S(1)} %get-tuple-element.47), channel_id=1, source_target_pairs={{0,24},{4,28},{8,16},{12,20},{16,8},{20,12},{24,0},{28,4},{1,25},{... | collective-permute-start | bytes 208904 | tf_op jit(solution)/shard_map/ppermute | solution.py:332
  7.4 7.7 %collective-permute-start.7 = (bf16[128,128]{1,0:T(8,128)(2,1)S(1)}, bf16[128,128]{1,0:T(8,128)(2,1)S(1)}, u32[]{:S(2)}, u32[]{:S(2)}) collective-permute-start(bf16[128,128]{1,0:T(8,128)(2,1)S(1)} %get-tuple-element.49), channel_id=1, source_target_pairs={{0,8},{4,12},{8,0},{12,4},{16,24},{20,28},{24,16},{28,20},{1,9},{5... | collective-permute-start | bytes 98312 | tf_op jit(solution)/shard_map/ppermute | solution.py:332
  8.3 17.7 %collective-permute-start = (bf16[272,128]{1,0:T(8,128)(2,1)S(1)}, bf16[272,128]{1,0:T(8,128)(2,1)S(1)}, u32[]{:S(2)}, u32[]{:S(2)}) collective-permute-start(bf16[272,128]{1,0:T(8,128)(2,1)S(1)} %get-tuple-element.44.refs_3_), channel_id=1, source_target_pairs={{0,4},{4,0},{8,12},{12,8},{16,20},{20,16},{24,28},{28,24},{1,5},{5... | collective-permute-start | bytes 208904 | tf_op jit(solution)/shard_map/ppermute | solution.py:332
  9.8 16.2 %collective-permute-start.2 = (bf16[272,128]{1,0:T(8,128)(2,1)S(1)}, bf16[272,128]{1,0:T(8,128)(2,1)S(1)}, u32[]{:S(2)}, u32[]{:S(2)}) collective-permute-start(bf16[272,128]{1,0:T(8,128)(2,1)S(1)} %collective-permute-done.1.refs_5_), channel_id=1, source_target_pairs={{0,4},{4,0},{8,12},{12,8},{16,20},{20,16},{24,28},{28,24},{1,5},{5... | collective-permute-start | bytes 208904 | tf_op jit(solution)/shard_map/ppermute | solution.py:332
  12.3 13.7 %collective-permute-start.4 = (bf16[272,128]{1,0:T(8,128)(2,1)S(1)}, bf16[272,128]{1,0:T(8,128)(2,1)S(1)}, u32[]{:S(2)}, u32[]{:S(2)}) collective-permute-start(bf16[272,128]{1,0:T(8,128)(2,1)S(1)} %collective-permute-done.3.refs_7_), channel_id=1, source_target_pairs={{0,4},{4,0},{8,12},{12,8},{16,20},{20,16},{24,28},{28,24},{1,5},{5... | collective-permute-start | bytes 208904 | tf_op jit(solution)/shard_map/ppermute | solution.py:332
  13.8 12.2 %collective-permute-start.6 = (bf16[272,128]{1,0:T(8,128)(2,1)S(1)}, bf16[272,128]{1,0:T(8,128)(2,1)S(1)}, u32[]{:S(2)}, u32[]{:S(2)}) collective-permute-start(bf16[272,128]{1,0:T(8,128)(2,1)S(1)} %collective-permute-done.5.refs_9_), channel_id=1, source_target_pairs={{0,4},{4,0},{8,12},{12,8},{16,20},{20,16},{24,28},{28,24},{1,5},{5... | collective-permute-start | bytes 208904 | tf_op jit(solution)/shard_map/ppermute | solution.py:332
  15.1 5.2 %collective-permute-start.8 = (bf16[128,128]{1,0:T(8,128)(2,1)S(1)}, bf16[128,128]{1,0:T(8,128)(2,1)S(1)}, u32[]{:S(2)}, u32[]{:S(2)}) collective-permute-start(bf16[128,128]{1,0:T(8,128)(2,1)S(1)} %get-tuple-element.50), channel_id=1, source_target_pairs={{0,16},{4,20},{8,24},{12,28},{16,0},{20,4},{24,8},{28,12},{1,17},{... | collective-permute-start | bytes 98312 | tf_op jit(solution)/shard_map/ppermute | solution.py:332
  20.3 5.7 %collective-permute-start.9 = (bf16[128,128]{1,0:T(8,128)(2,1)S(1)}, bf16[128,128]{1,0:T(8,128)(2,1)S(1)}, u32[]{:S(2)}, u32[]{:S(2)}) collective-permute-start(bf16[128,128]{1,0:T(8,128)(2,1)S(1)} %get-tuple-element.51), channel_id=1, source_target_pairs={{0,24},{4,28},{8,16},{12,20},{16,8},{20,12},{24,0},{28,4},{1,25},{... | collective-permute-start | bytes 98312 | tf_op jit(solution)/shard_map/ppermute | solution.py:332
  26.0 8.0 %copy-start.6 = (bf16[2,1024,384]{2,1,0:T(8,128)(2,1)S(1)}, bf16[2,1024,384]{2,1,0:T(8,128)(2,1)}, u32[]{:S(2)}) copy-start(bf16[2,1024,384]{2,1,0:T(8,128)(2,1)} %refs_1_.1) | copy-start | bytes 4718596
  26.1 14.7 %copy-start = (bf16[2,384,1024]{2,1,0:T(8,128)(2,1)S(1)}, bf16[2,384,1024]{2,1,0:T(8,128)(2,1)}, u32[]{:S(2)}) copy-start(bf16[2,384,1024]{2,1,0:T(8,128)(2,1)} %own_ref.5) | copy-start | bytes 4718596
  26.1 19.5 %copy-start.2 = (bf16[128,1024]{1,0:T(8,128)(2,1)S(1)}, bf16[128,1024]{1,0:T(8,128)(2,1)}, u32[]{:S(2)}) copy-start(bf16[128,1024]{1,0:T(8,128)(2,1)} %refs_5_.1) | copy-start | bytes 786436
  29.6 5.0 %collective-permute-start.10 = (bf16[128,128]{1,0:T(8,128)(2,1)S(1)}, bf16[128,128]{1,0:T(8,128)(2,1)S(1)}, u32[]{:S(2)}, u32[]{:S(2)}) collective-permute-start(bf16[128,128]{1,0:T(8,128)(2,1)S(1)} %get-tuple-element.53), channel_id=1, source_target_pairs={{0,8},{4,12},{8,0},{12,4},{16,24},{20,28},{24,16},{28,20},{1,9},{5... | collective-permute-start | bytes 98312 | tf_op jit(solution)/shard_map/ppermute | solution.py:332
  29.7 5.7 %collective-permute-start.11 = (bf16[128,128]{1,0:T(8,128)(2,1)S(1)}, bf16[128,128]{1,0:T(8,128)(2,1)S(1)}, u32[]{:S(2)}, u32[]{:S(2)}) collective-permute-start(bf16[128,128]{1,0:T(8,128)(2,1)S(1)} %get-tuple-element.54), channel_id=1, source_target_pairs={{0,16},{4,20},{8,24},{12,28},{16,0},{20,4},{24,8},{28,12},{1,17},{... | collective-permute-start | bytes 98312 | tf_op jit(solution)/shard_map/ppermute | solution.py:332
  33.5 5.7 %collective-permute-start.12 = (bf16[128,128]{1,0:T(8,128)(2,1)S(1)}, bf16[128,128]{1,0:T(8,128)(2,1)S(1)}, u32[]{:S(2)}, u32[]{:S(2)}) collective-permute-start(bf16[128,128]{1,0:T(8,128)(2,1)S(1)} %get-tuple-element.55), channel_id=1, source_target_pairs={{0,24},{4,28},{8,16},{12,20},{16,8},{20,12},{24,0},{28,4},{1,25},{... | collective-permute-start | bytes 98312 | tf_op jit(solution)/shard_map/ppermute | solution.py:332
  34.1 32.7 %collective-permute-start.18 = (bf16[2,1024,384]{2,1,0:T(8,128)(2,1)S(1)}, bf16[2,1024,384]{2,1,0:T(8,128)(2,1)S(1)}, u32[]{:S(2)}, u32[]{:S(2)}) collective-permute-start(bf16[2,1024,384]{2,1,0:T(8,128)(2,1)S(1)} %copy-done.6), channel_id=1, source_target_pairs={{0,1},{1,0},{2,3},{3,2},{4,5},{5,4},{6,7},{7,6},{8,9},{9,8},{10,11... | collective-permute-start | bytes 4718600 | tf_op jit(solution)/shard_map/ppermute | solution.py:332
  34.1 35.3 %collective-permute-start.19 = (bf16[2,1024,384]{2,1,0:T(8,128)(2,1)S(1)}, bf16[2,1024,384]{2,1,0:T(8,128)(2,1)S(1)}, u32[]{:S(2)}, u32[]{:S(2)}) collective-permute-start(bf16[2,1024,384]{2,1,0:T(8,128)(2,1)S(1)} %copy-done.7), channel_id=1, source_target_pairs={{0,1},{1,0},{2,3},{3,2},{4,5},{5,4},{6,7},{7,6},{8,9},{9,8},{10,11... | collective-permute-start | bytes 4718600 | tf_op jit(solution)/shard_map/ppermute | solution.py:332
  39.2 5.0 %collective-permute-start.13 = (bf16[4,128,128]{2,1,0:T(8,128)(2,1)S(1)}, bf16[4,128,128]{2,1,0:T(8,128)(2,1)S(1)}, u32[]{:S(2)}, u32[]{:S(2)}) collective-permute-start(bf16[4,128,128]{2,1,0:T(8,128)(2,1)S(1)} %shard_map.147.refs_0_), channel_id=1, source_target_pairs={{0,2},{1,3},{2,0},{3,1},{4,6},{5,7},{6,4},{7,5},{8,10},{9,11},{10,... | collective-permute-start | bytes 393224 | tf_op jit(solution)/shard_map/ppermute | solution.py:332
  40.8 37.2 %collective-permute-start.27 = (bf16[2,384,1024]{2,1,0:T(8,128)(2,1)S(1)}, bf16[2,384,1024]{2,1,0:T(8,128)(2,1)S(1)}, u32[]{:S(2)}, u32[]{:S(2)}) collective-permute-start(bf16[2,384,1024]{2,1,0:T(8,128)(2,1)S(1)} %copy-done), channel_id=1, source_target_pairs={{0,1},{1,0},{2,3},{3,2},{4,5},{5,4},{6,7},{7,6},{8,9},{9,8},{10,11... | collective-permute-start | bytes 4718600 | tf_op jit(solution)/shard_map/ppermute | solution.py:332
  40.8 3.6 %collective-permute-start.14 = (bf16[4,128,128]{2,1,0:T(8,128)(2,1)S(1)}, bf16[4,128,128]{2,1,0:T(8,128)(2,1)S(1)}, u32[]{:S(2)}, u32[]{:S(2)}) collective-permute-start(bf16[4,128,128]{2,1,0:T(8,128)(2,1)S(1)} %shard_map.147.refs_0_), channel_id=1, source_target_pairs={{0,1},{1,0},{2,3},{3,2},{4,5},{5,4},{6,7},{7,6},{8,9},{9,8},{10,11... | collective-permute-start | bytes 393224 | tf_op jit(solution)/shard_map/ppermute | solution.py:332
  44.2 1.3 %collective-permute-start.15 = (bf16[4,128,128]{2,1,0:T(8,128)(2,1)S(1)}, bf16[4,128,128]{2,1,0:T(8,128)(2,1)S(1)}, u32[]{:S(2)}, u32[]{:S(2)}) collective-permute-start(bf16[4,128,128]{2,1,0:T(8,128)(2,1)S(1)} %collective-permute-done.13.refs_1_), channel_id=1, source_target_pairs={{0,1},{1,0},{2,3},{3,2},{4,5},{5,4},{6,7},{7,6},{8,9},{9,8},{10,11... | collective-permute-start | bytes 393224 | tf_op jit(solution)/shard_map/ppermute | solution.py:332
  47.0 1.8 %collective-permute-start.16 = (bf16[128,1024]{1,0:T(8,128)(2,1)S(1)}, bf16[128,1024]{1,0:T(8,128)(2,1)S(1)}, u32[]{:S(2)}, u32[]{:S(2)}) collective-permute-start(bf16[128,1024]{1,0:T(8,128)(2,1)S(1)} %shard_map.148.own_ref.mixed_ref), channel_id=1, source_target_pairs={{0,1},{1,0},{2,3},{3,2},{4,5},{5,4},{6,7},{7,6},{8,9},{9,8},{10,11... | collective-permute-start | bytes 786440 | tf_op jit(solution)/shard_map/ppermute | solution.py:332
  47.3 1.4 %collective-permute-start.17 = (f32[1,1024]{1,0:T(1,128)S(1)}, f32[1,1024]{1,0:T(1,128)S(1)}, u32[]{:S(2)}, u32[]{:S(2)}) collective-permute-start(f32[1,1024]{1,0:T(1,128)S(1)} %bitcast.9), channel_id=1, source_target_pairs={{0,1},{1,0},{2,3},{3,2},{4,5},{5,4},{6,7},{7,6},{8,9},{9,8},{10,11... | collective-permute-start | bytes 12296 | tf_op jit(solution)/shard_map/ppermute | solution.py:332
  48.6 2.3 %collective-permute-start.20 = (bf16[1024,384]{1,0:T(8,128)(2,1)S(1)}, bf16[1024,384]{1,0:T(8,128)(2,1)S(1)}, u32[]{:S(2)}, u32[]{:S(2)}) collective-permute-start(bf16[1024,384]{1,0:T(8,128)(2,1)S(1)} %copy-done.8), channel_id=1, source_target_pairs={{0,1},{1,0},{2,3},{3,2},{4,5},{5,4},{6,7},{7,6},{8,9},{9,8},{10,11... | collective-permute-start | bytes 2359304 | tf_op jit(solution)/shard_map/ppermute | solution.py:332
  48.8 3.3 %collective-permute-start.21 = (bf16[1024,384]{1,0:T(8,128)(2,1)S(1)}, bf16[1024,384]{1,0:T(8,128)(2,1)S(1)}, u32[]{:S(2)}, u32[]{:S(2)}) collective-permute-start(bf16[1024,384]{1,0:T(8,128)(2,1)S(1)} %copy-done.9), channel_id=1, source_target_pairs={{0,1},{1,0},{2,3},{3,2},{4,5},{5,4},{6,7},{7,6},{8,9},{9,8},{10,11... | collective-permute-start | bytes 2359304 | tf_op jit(solution)/shard_map/ppermute | solution.py:332
  50.9 10.1 %collective-permute-start.24 = (bf16[2,32,1024]{2,1,0:T(8,128)(2,1)S(1)}, bf16[2,32,1024]{2,1,0:T(8,128)(2,1)S(1)}, u32[]{:S(2)}, u32[]{:S(2)}) collective-permute-start(bf16[2,32,1024]{2,1,0:T(8,128)(2,1)S(1)} %get-tuple-element.63), channel_id=1, source_target_pairs={{0,16},{4,20},{8,24},{12,28},{16,0},{20,4},{24,8},{28,12},{1,17},{... | collective-permute-start | bytes 393224 | tf_op jit(solution)/shard_map/ppermute | solution.py:332
  52.1 11.6 %collective-permute-start.25 = (bf16[2,32,1024]{2,1,0:T(8,128)(2,1)S(1)}, bf16[2,32,1024]{2,1,0:T(8,128)(2,1)S(1)}, u32[]{:S(2)}, u32[]{:S(2)}) collective-permute-start(bf16[2,32,1024]{2,1,0:T(8,128)(2,1)S(1)} %get-tuple-element.64), channel_id=1, source_target_pairs={{0,20},{4,16},{8,28},{12,24},{16,4},{20,0},{24,12},{28,8},{1,21},{... | collective-permute-start | bytes 393224 | tf_op jit(solution)/shard_map/ppermute | solution.py:332
  61.0 5.5 %collective-permute-start.30 = (bf16[2,32,1024]{2,1,0:T(8,128)(2,1)S(1)}, bf16[2,32,1024]{2,1,0:T(8,128)(2,1)S(1)}, u32[]{:S(2)}, u32[]{:S(2)}) collective-permute-start(bf16[2,32,1024]{2,1,0:T(8,128)(2,1)S(1)} %get-tuple-element.69), channel_id=1, source_target_pairs={{0,4},{4,0},{8,12},{12,8},{16,20},{20,16},{24,28},{28,24},{1,5},{5... | collective-permute-start | bytes 393224 | tf_op jit(solution)/shard_map/ppermute | solution.py:332
  63.7 10.3 %collective-permute-start.31 = (bf16[2,32,1024]{2,1,0:T(8,128)(2,1)S(1)}, bf16[2,32,1024]{2,1,0:T(8,128)(2,1)S(1)}, u32[]{:S(2)}, u32[]{:S(2)}) collective-permute-start(bf16[2,32,1024]{2,1,0:T(8,128)(2,1)S(1)} %get-tuple-element.70), channel_id=1, source_target_pairs={{0,8},{4,12},{8,0},{12,4},{16,24},{20,28},{24,16},{28,20},{1,9},{5... | collective-permute-start | bytes 393224 | tf_op jit(solution)/shard_map/ppermute | solution.py:332
  66.5 9.0 %collective-permute-start.32 = (bf16[2,32,1024]{2,1,0:T(8,128)(2,1)S(1)}, bf16[2,32,1024]{2,1,0:T(8,128)(2,1)S(1)}, u32[]{:S(2)}, u32[]{:S(2)}) collective-permute-start(bf16[2,32,1024]{2,1,0:T(8,128)(2,1)S(1)} %get-tuple-element.71), channel_id=1, source_target_pairs={{0,12},{4,8},{8,4},{12,0},{16,28},{20,24},{24,20},{28,16},{1,13},{... | collective-permute-start | bytes 393224 | tf_op jit(solution)/shard_map/ppermute | solution.py:332
  66.8 17.1 %collective-permute-start.37 = (bf16[2,32,1024]{2,1,0:T(8,128)(2,1)S(1)}, bf16[2,32,1024]{2,1,0:T(8,128)(2,1)S(1)}, u32[]{:S(2)}, u32[]{:S(2)}) collective-permute-start(bf16[2,32,1024]{2,1,0:T(8,128)(2,1)S(1)} %get-tuple-element.77), channel_id=1, source_target_pairs={{0,24},{4,28},{8,16},{12,20},{16,8},{20,12},{24,0},{28,4},{1,25},{... | collective-permute-start | bytes 393224 | tf_op jit(solution)/shard_map/ppermute | solution.py:332
  69.4 18.1 %collective-permute-start.38 = (bf16[2,32,1024]{2,1,0:T(8,128)(2,1)S(1)}, bf16[2,32,1024]{2,1,0:T(8,128)(2,1)S(1)}, u32[]{:S(2)}, u32[]{:S(2)}) collective-permute-start(bf16[2,32,1024]{2,1,0:T(8,128)(2,1)S(1)} %get-tuple-element.78), channel_id=1, source_target_pairs={{0,28},{4,24},{8,20},{12,16},{16,12},{20,8},{24,4},{28,0},{1,29},{... | collective-permute-start | bytes 393224 | tf_op jit(solution)/shard_map/ppermute | solution.py:332
  73.9 5.7 %collective-permute-start.26 = (bf16[64,896]{1,0:T(8,128)(2,1)S(1)}, bf16[64,896]{1,0:T(8,128)(2,1)S(1)}, u32[]{:S(2)}, u32[]{:S(2)}) collective-permute-start(bf16[64,896]{1,0:T(8,128)(2,1)S(1)} %shard_map.154.a_ref), channel_id=1, source_target_pairs={{0,2},{1,3},{2,0},{3,1},{4,6},{5,7},{6,4},{7,5},{8,10},{9,11},{10,... | collective-permute-start | bytes 344072 | tf_op jit(solution)/shard_map/ppermute | solution.py:332
  76.2 18.0 %collective-permute-start.33 = (bf16[128,896]{1,0:T(8,128)(2,1)S(1)}, bf16[128,896]{1,0:T(8,128)(2,1)S(1)}, u32[]{:S(2)}, u32[]{:S(2)}) collective-permute-start(bf16[128,896]{1,0:T(8,128)(2,1)S(1)} %shard_map.157.a_ref), channel_id=1, source_target_pairs={{0,2},{1,3},{2,0},{3,1},{4,6},{5,7},{6,4},{7,5},{8,10},{9,11},{10,... | collective-permute-start | bytes 688136 | tf_op jit(solution)/shard_map/ppermute | solution.py:332
  78.0 11.8 %collective-permute-start.22 = (bf16[64,896]{1,0:T(8,128)(2,1)S(1)}, bf16[64,896]{1,0:T(8,128)(2,1)S(1)}, u32[]{:S(2)}, u32[]{:S(2)}) collective-permute-start(bf16[64,896]{1,0:T(8,128)(2,1)S(1)} %shard_map.150.a_ref), channel_id=1, source_target_pairs={{0,2},{1,3},{2,0},{3,1},{4,6},{5,7},{6,4},{7,5},{8,10},{9,11},{10,... | collective-permute-start | bytes 344072 | tf_op jit(solution)/shard_map/ppermute | solution.py:332
  80.7 18.2 %collective-permute-start.28 = (bf16[2,32,1024]{2,1,0:T(8,128)(2,1)S(1)}, bf16[2,32,1024]{2,1,0:T(8,128)(2,1)S(1)}, u32[]{:S(2)}, u32[]{:S(2)}) collective-permute-start(bf16[2,32,1024]{2,1,0:T(8,128)(2,1)S(1)} %get-tuple-element.65), channel_id=1, source_target_pairs={{0,16},{4,20},{8,24},{12,28},{16,0},{20,4},{24,8},{28,12},{1,17},{... | collective-permute-start | bytes 393224 | tf_op jit(solution)/shard_map/ppermute | solution.py:332
  83.9 17.1 %collective-permute-start.29 = (bf16[2,32,1024]{2,1,0:T(8,128)(2,1)S(1)}, bf16[2,32,1024]{2,1,0:T(8,128)(2,1)S(1)}, u32[]{:S(2)}, u32[]{:S(2)}) collective-permute-start(bf16[2,32,1024]{2,1,0:T(8,128)(2,1)S(1)} %get-tuple-element.66), channel_id=1, source_target_pairs={{0,20},{4,16},{8,28},{12,24},{16,4},{20,0},{24,12},{28,8},{1,21},{... | collective-permute-start | bytes 393224 | tf_op jit(solution)/shard_map/ppermute | solution.py:332
  88.2 4.9 %collective-permute-start.39 = (bf16[64,896]{1,0:T(8,128)(2,1)S(1)}, bf16[64,896]{1,0:T(8,128)(2,1)S(1)}, u32[]{:S(2)}, u32[]{:S(2)}) collective-permute-start(bf16[64,896]{1,0:T(8,128)(2,1)S(1)} %shard_map.160.a_ref), channel_id=1, source_target_pairs={{0,2},{1,3},{2,0},{3,1},{4,6},{5,7},{6,4},{7,5},{8,10},{9,11},{10,... | collective-permute-start | bytes 344072 | tf_op jit(solution)/shard_map/ppermute | solution.py:332
  90.0 6.0 %collective-permute-start.23 = (bf16[64,384]{1,0:T(8,128)(2,1)S(1)}, bf16[64,384]{1,0:T(8,128)(2,1)S(1)}, u32[]{:S(2)}, u32[]{:S(2)}) collective-permute-start(bf16[64,384]{1,0:T(8,128)(2,1)S(1)} %shard_map.151.mine_ref), channel_id=1, source_target_pairs={{0,1},{1,0},{2,3},{3,2},{4,5},{5,4},{6,7},{7,6},{8,9},{9,8},{10,11... | collective-permute-start | bytes 147464 | tf_op jit(solution)/shard_map/ppermute | solution.py:332
  94.1 8.1 %copy-start.1 = (bf16[384,1024]{1,0:T(8,128)(2,1)S(1)}, bf16[384,1024]{1,0:T(8,128)(2,1)}, u32[]{:S(2)}) copy-start(bf16[384,1024]{1,0:T(8,128)(2,1)} %down_ref.1) | copy-start | bytes 2359300
  94.1 8.1 %copy-start.5 = (f32[128,2]{0,1:T(2,128)S(1)}, f32[128,2]{0,1:T(2,128)}, u32[]{:S(2)}) copy-start(f32[128,2]{0,1:T(2,128)} %param.23) | copy-start | bytes 3076
  95.3 8.1 %collective-permute-start.34 = (bf16[2,32,1024]{2,1,0:T(8,128)(2,1)S(1)}, bf16[2,32,1024]{2,1,0:T(8,128)(2,1)S(1)}, u32[]{:S(2)}, u32[]{:S(2)}) collective-permute-start(bf16[2,32,1024]{2,1,0:T(8,128)(2,1)S(1)} %get-tuple-element.73), channel_id=1, source_target_pairs={{0,4},{4,0},{8,12},{12,8},{16,20},{20,16},{24,28},{28,24},{1,5},{5... | collective-permute-start | bytes 393224 | tf_op jit(solution)/shard_map/ppermute | solution.py:332
  95.4 8.0 %collective-permute-start.35 = (bf16[2,32,1024]{2,1,0:T(8,128)(2,1)S(1)}, bf16[2,32,1024]{2,1,0:T(8,128)(2,1)S(1)}, u32[]{:S(2)}, u32[]{:S(2)}) collective-permute-start(bf16[2,32,1024]{2,1,0:T(8,128)(2,1)S(1)} %get-tuple-element.74), channel_id=1, source_target_pairs={{0,8},{4,12},{8,0},{12,4},{16,24},{20,28},{24,16},{28,20},{1,9},{5... | collective-permute-start | bytes 393224 | tf_op jit(solution)/shard_map/ppermute | solution.py:332
  96.0 9.6 %collective-permute-start.36 = (bf16[2,32,1024]{2,1,0:T(8,128)(2,1)S(1)}, bf16[2,32,1024]{2,1,0:T(8,128)(2,1)S(1)}, u32[]{:S(2)}, u32[]{:S(2)}) collective-permute-start(bf16[2,32,1024]{2,1,0:T(8,128)(2,1)S(1)} %get-tuple-element.75), channel_id=1, source_target_pairs={{0,12},{4,8},{8,4},{12,0},{16,28},{20,24},{24,20},{28,16},{1,13},{... | collective-permute-start | bytes 393224 | tf_op jit(solution)/shard_map/ppermute | solution.py:332
  98.9 8.2 %collective-permute-start.40 = (bf16[2,32,1024]{2,1,0:T(8,128)(2,1)S(1)}, bf16[2,32,1024]{2,1,0:T(8,128)(2,1)S(1)}, u32[]{:S(2)}, u32[]{:S(2)}) collective-permute-start(bf16[2,32,1024]{2,1,0:T(8,128)(2,1)S(1)} %get-tuple-element.79), channel_id=1, source_target_pairs={{0,24},{4,28},{8,16},{12,20},{16,8},{20,12},{24,0},{28,4},{1,25},{... | collective-permute-start | bytes 393224 | tf_op jit(solution)/shard_map/ppermute | solution.py:332
  101.0 8.2 %collective-permute-start.41 = (bf16[2,32,1024]{2,1,0:T(8,128)(2,1)S(1)}, bf16[2,32,1024]{2,1,0:T(8,128)(2,1)S(1)}, u32[]{:S(2)}, u32[]{:S(2)}) collective-permute-start(bf16[2,32,1024]{2,1,0:T(8,128)(2,1)S(1)} %get-tuple-element.80), channel_id=1, source_target_pairs={{0,28},{4,24},{8,20},{12,16},{16,12},{20,8},{24,4},{28,0},{1,29},{... | collective-permute-start | bytes 393224 | tf_op jit(solution)/shard_map/ppermute | solution.py:332
  109.5 1.6 %collective-permute-start.42 = (bf16[128,1024]{1,0:T(8,128)(2,1)S(1)}, bf16[128,1024]{1,0:T(8,128)(2,1)S(1)}, u32[]{:S(2)}, u32[]{:S(2)}) collective-permute-start(bf16[128,1024]{1,0:T(8,128)(2,1)S(1)} %get-tuple-element.82), channel_id=1, source_target_pairs={{0,1},{1,0},{2,3},{3,2},{4,5},{5,4},{6,7},{7,6},{8,9},{9,8},{10,11... | collective-permute-start | bytes 786440 | tf_op jit(solution)/shard_map/ppermute | solution.py:332
  (5 other events, 19.5 us)
